TPU v7x, 512 devices: a whole 4x4x16 slice. The times are simulated.
512 devices in a mesh: ep: 16 (over y, x), tp: 32 (over z, core).
Axes of the slice: x: 4, y: 4, z: 16, core: 2. Of those that a mesh axis runs over, the one named last changes fastest.
Arguments:
- tokens: bfloat16 [2048, 2048], P('ep'), may hold values from -32 to 32
- routes: int32 [2048, 2], P('ep'), may hold values from 0 to 15, all different within a row; in each aligned block of 128 rows (0 to 127, 128 to 255, ...) at most 24 rows name the same one
- gates: float32 [2048, 2], P('ep'), may hold values from 0.05 to 0.6
- cotangent: bfloat16 [2048, 2048], P('ep'), may hold values from -6 to 6
- w_glu: bfloat16 [16, 2048, 1024], P('ep', None, 'tp'), may hold values from -0.125 to 0.125
- w_lin: bfloat16 [16, 2048, 1024], P('ep', None, 'tp'), may hold values from -0.125 to 0.125
- w_down: bfloat16 [16, 1024, 2048], P('ep', 'tp'), may hold values from -0.1875 to 0.1875
Outputs:
- d_tokens: bfloat16 [2048, 2048], P('ep', 'tp')
- d_gates: float32 [2048, 2], P('ep')
- glu_wgrad: float32 [16, 2048, 1024], P('ep', None, 'tp')
- lin_wgrad: float32 [16, 2048, 1024], P('ep', None, 'tp')
- down_wgrad: float32 [16, 1024, 2048], P('ep', 'tp')
- glu_norms: float32 [16, 2048], P('ep')
- lin_norms: float32 [16, 2048], P('ep')
- down_norms: float32 [16, 1024], P('ep', 'tp')
Inputs may be any that keep to these rules, and one draw needn't show every extreme that they name: `routes`: each row names 2 different experts. Among the 128 tokens of one aligned block no expert is named more than 24 times, and in every draw some expert is named exactly 24 times in some block.
All inputs are finite; a program needn't handle non-finite values.
Results may differ from a plain program's by a relative error of at most 0.024.
Values may be sent and summed in bfloat16 or wider, within the bound.
No kernel may reach another device: no remote copies, remote signals or barrier semaphores. Data moves between devices by JAX's collectives and lax.ppermute only.
A program may use at most 64 MiB of HBM per device.

v0:
```python
import jax
import jax.numpy as jnp
from jax import lax
from jax.sharding import Mesh
from jax.sharding import PartitionSpec as P

TP = ("tp_0", "tp_1")


clamp_limit = 7.0
sigmoid_scale = 1.702


def side_by_side(arrays, axis, split_dim, concat_dim, along):
    both = jnp.concatenate(arrays, axis=along)
    filled, at, outs = (
        lax.all_to_all(both, axis, split_axis=split_dim, concat_axis=concat_dim, tiled=True),
        0,
        [],
    )
    for a in arrays:
        outs.append(lax.slice_in_dim(filled, at, at + a.shape[along], axis=along))
        at += a.shape[along]
    return tuple(outs)


def reduced_to_own(tiles, axes, sequence):
    inside = tiles.shape[1:]
    tiles = tiles.reshape(*(lax.axis_size(a) for a in axes), *inside)
    tiles = jnp.moveaxis(tiles, sequence, range(len(axes))).reshape(-1, *inside)
    for k in sequence:
        tiles = lax.psum_scatter(tiles, axes[k], scatter_dimension=0, tiled=True)
    return tiles[0]


def in_blocks(shard, dim, devices):
    before, after = (shard.shape[:dim], shard.shape[dim + 1 :])
    return jnp.moveaxis(shard.reshape(*before, devices, -1, *after), dim, 0)


def scatter_axes(shard, axes, sequence, dim):
    devices = lax.axis_size(axes)
    return reduced_to_own(in_blocks(shard, dim, devices), axes, sequence)


def copy_for_each(shard, axis):
    devices = lax.axis_size(axis)
    return lax.all_to_all(
        jnp.broadcast_to(shard[None], (devices, *shard.shape)), axis, 0, 0, tiled=True
    )


def taken_together(shard, axis):
    everything = copy_for_each(shard, axis)
    return jnp.sum(everything, axis=0)


def packed_total(arrays, axis):
    flat, at, outs = (jnp.concatenate([a.reshape(-1) for a in arrays]), 0, [])
    subtotal = taken_together(flat, axis)
    for a in arrays:
        outs.append(subtotal[at : at + a.size].reshape(a.shape))
        at += a.size
    return tuple(outs)


def slot_rank(pair_expert, all_experts):
    onehot = (pair_expert[:, None] == jnp.arange(all_experts, dtype=jnp.int32)[None, :]).astype(
        jnp.int32
    )
    return jnp.sum(jnp.cumsum(onehot, axis=0) * onehot, axis=1) - 1


def clamp_backward(glu_pre, lin_pre, back_proj, gate_col):
    glu_clip = jnp.minimum(glu_pre, clamp_limit)
    lin_clip = jnp.clip(lin_pre, -clamp_limit, clamp_limit)
    sig_val = jax.nn.sigmoid(sigmoid_scale * glu_clip)
    glu_act = glu_clip * sig_val
    hidden = glu_act * (lin_clip + 1.0)
    hid_grad = gate_col * back_proj
    act_slope = sig_val + sigmoid_scale * glu_clip * sig_val * (1.0 - sig_val)
    glu_grad = jnp.where(glu_pre < clamp_limit, hid_grad * (lin_clip + 1.0) * act_slope, 0.0)
    lin_grad = jnp.where(jnp.abs(lin_pre) < clamp_limit, hid_grad * glu_act, 0.0)
    return (hidden, glu_grad.astype(jnp.bfloat16), lin_grad.astype(jnp.bfloat16))


def pick_rows(source_rows, slot_token, local_experts, slot_total):
    padded = jnp.concatenate(
        [source_rows, jnp.zeros((1, source_rows.shape[1]), source_rows.dtype)], axis=0
    )
    return padded[slot_token].reshape(local_experts, slot_total, source_rows.shape[1])


def shards(tokens, routes, gates, cotangent, w_glu, w_lin, w_down):
    ep_count = lax.axis_size("ep")
    tp_count = lax.axis_size(TP)
    tok_rows, top_count = routes.shape
    local_experts = w_glu.shape[0]
    model_width = w_glu.shape[1]
    all_experts = local_experts * ep_count
    slot_cap = 3 * tok_rows * top_count // (2 * all_experts)
    slot_total = ep_count * slot_cap
    pair_count = tok_rows * top_count
    col_width = model_width // tp_count
    pair_expert = routes.reshape(-1)
    pair_slot = (
        pair_expert % local_experts * slot_total
        + pair_expert // local_experts * slot_cap
        + slot_rank(pair_expert, all_experts)
    )
    slot_pair = (
        jnp.full((local_experts * slot_total,), pair_count, jnp.int32)
        .at[pair_slot]
        .set(jnp.arange(pair_count, dtype=jnp.int32))
    )
    slot_token = slot_pair // top_count
    gate_send = jnp.concatenate([gates.reshape(-1), jnp.zeros((1,), jnp.float32)])[slot_pair]
    gate_rows = lax.all_to_all(
        gate_send.reshape(local_experts, slot_total), "ep", split_axis=1, concat_axis=1, tiled=True
    )
    tok_send = pick_rows(tokens, slot_token, local_experts, slot_total)
    cot_send = pick_rows(cotangent, slot_token, local_experts, slot_total)
    tok_recv, cot_recv = side_by_side((tok_send, cot_send), "ep", 1, 1, 0)
    glu_pre = jnp.einsum("erd,edf->erf", tok_recv, w_glu, preferred_element_type=jnp.float32)
    lin_pre = jnp.einsum("erd,edf->erf", tok_recv, w_lin, preferred_element_type=jnp.float32)
    back_proj = jnp.einsum("erd,efd->erf", cot_recv, w_down, preferred_element_type=jnp.float32)
    gate_col = gate_rows[:, :, None]
    hidden, glu_bf, lin_bf = clamp_backward(glu_pre, lin_pre, back_proj, gate_col)
    gate_part = jnp.sum(back_proj * hidden, axis=2)
    hidden_gated = (gate_col * hidden).astype(jnp.bfloat16)
    down_wgrad = jnp.einsum(
        "erf,erd->efd", hidden_gated, cot_recv, preferred_element_type=jnp.float32
    )
    glu_wgrad = jnp.einsum("erd,erf->edf", tok_recv, glu_bf, preferred_element_type=jnp.float32)
    lin_wgrad = jnp.einsum("erd,erf->edf", tok_recv, lin_bf, preferred_element_type=jnp.float32)
    input_part = jnp.dot(glu_bf[0], w_glu[0].T, preferred_element_type=jnp.float32)
    input_part = input_part + jnp.dot(lin_bf[0], w_lin[0].T, preferred_element_type=jnp.float32)
    grad_pieces = [
        scatter_axes(input_part.astype(jnp.bfloat16), TP, (1, 0), 1)
        .astype(jnp.float32)
        .astype(jnp.bfloat16)
    ]
    back_grads = lax.all_to_all(
        jnp.stack(grad_pieces), "ep", split_axis=1, concat_axis=1, tiled=True
    )
    gate_sums, glu_norms, lin_norms = packed_total(
        (gate_part, jnp.sum(glu_wgrad * glu_wgrad, axis=2), jnp.sum(lin_wgrad * lin_wgrad, axis=2)),
        TP,
    )
    gate_back = lax.all_to_all(gate_sums, "ep", split_axis=1, concat_axis=1, tiled=True)
    pair_grads = back_grads.reshape(-1, col_width)[pair_slot].astype(jnp.float32)
    d_tokens = jnp.sum(pair_grads.reshape(tok_rows, top_count, col_width), axis=1).astype(
        jnp.bfloat16
    )
    d_gates = gate_back.reshape(-1)[pair_slot].reshape(tok_rows, top_count)
    down_norms = jnp.sum(down_wgrad * down_wgrad, axis=2)
    return (d_tokens, d_gates, glu_wgrad, lin_wgrad, down_wgrad, glu_norms, lin_norms, down_norms)


def solution(mesh):
    split = Mesh(mesh.devices.reshape(mesh.shape["ep"], 16, 2), ("ep", "tp_0", "tp_1"))
    placed = (
        P("ep", None),
        P("ep", None),
        P("ep", None),
        P("ep", None),
        P("ep", None, TP),
        P("ep", None, TP),
        P("ep", TP, None),
    )
    return jax.shard_map(
        shards,
        mesh=split,
        in_specs=placed,
        out_specs=(
            P("ep", TP),
            P("ep", None),
            P("ep", None, TP),
            P("ep", None, TP),
            P("ep", TP, None),
            P("ep", None),
            P("ep", None),
            P("ep", TP),
        ),
        check_vma=False,
    )
```

profile of v0, /device:TPU:2, one launch (start us, length us, event | category | flops | bytes accessed | tf_op | source)
XLA Modules:
  0.0 224.1 jit_solution(12297283659354821836)
XLA Ops:
  7.2 0.9 copy.79
  8.3 0.7 broadcast_multiply_fusion
  9.0 0.6 reduce-window.6
  10.2 1.4 scatter_custom_fusion
  11.6 0.8 copy.84
  12.6 2.8 %gather_fusion.2 = f32[384]{0:T(512)S(1)} fusion(f32[257]{0:T(512)S(1)} %pad_maximum_fusion.2, s32[1024]{0:T(1024)S(1)} %get-tuple-element.72), kind=kCustom, calls=%fused_computation.2 | custom fusion | bytes 4608 | tf_op jit(solution)/shard_map/gather | solution.py:117
  15.4 0.7 all_to_all.23
  16.1 9.1 %all-to-all-start.1 = ((f32[1,16,24]{2,0,1:T(1,128)}), f32[1,16,24]{2,0,1:T(1,128)S(1)}, u32[]{:S(2)}, u32[]{:S(2)}) async-start(f32[1,16,24]{2,0,1:T(1,128)} %all_to_all.23), calls=%async_computation.1 | async-start | bytes 16384 | tf_op jit(solution)/shard_map/all_to_all | solution.py:118
  25.4 2.5 %gather_fusion = bf16[384,2048]{1,0:T(8,128)(2,1)S(1)} fusion(bf16[129,2048]{1,0:T(8,128)(2,1)S(1)} %concatenate.15, s32[1024]{0:T(1024)S(1)} %get-tuple-element.73), kind=kCustom, calls=%fused_computation | custom fusion | bytes 3147264 | tf_op jit(solution)/shard_map/gather | solution.py:91
  27.8 3.1 %gather_fusion.1 = bf16[384,2048]{1,0:T(8,128)(2,1)} fusion(bf16[129,2048]{1,0:T(8,128)(2,1)S(1)} %concatenate.16, s32[1024]{0:T(1024)S(1)} %get-tuple-element.73), kind=kCustom, calls=%fused_computation.1 | custom fusion | bytes 3147264 | tf_op jit(solution)/shard_map/gather | solution.py:91
  31.0 1.7 pad_maximum_fusion
  32.7 4.9 %copy.82 = bf16[2,384,2048]{2,0,1:T(2,128)(2,1)} copy(bf16[2,384,2048]{2,1,0:T(8,128)(2,1)S(1)} %pad_maximum_fusion) | data formatting | bytes 6291456 | tf_op jit(solution)/shard_map/concatenate | solution.py:15
  37.6 7.3 %all-to-all-start = ((bf16[2,384,2048]{2,0,1:T(2,128)(2,1)}), bf16[2,384,2048]{2,0,1:T(2,128)(2,1)S(1)}, u32[]{:S(2)}, u32[]{:S(2)}) async-start(bf16[2,384,2048]{2,0,1:T(2,128)(2,1)} %copy.82), calls=%async_computation | async-start | bytes 6291456 | tf_op jit(solution)/shard_map/all_to_all | solution.py:17
  45.1 0.5 broadcast.204
  45.6 0.7 reduce.18
  46.3 35.8 %all-to-all-done = bf16[2,384,2048]{2,0,1:T(2,128)(2,1)S(1)} async-done(((bf16[2,384,2048]{2,0,1:T(2,128)(2,1)}), bf16[2,384,2048]{2,0,1:T(2,128)(2,1)S(1)}, u32[]{:S(2)}, u32[]{:S(2)}) %all-to-all-start) | async-done | bytes 3145760 | tf_op jit(solution)/shard_map/all_to_all | solution.py:17
  82.2 4.4 %fusion.23 = (bf16[1,384,2048]{2,0,1:T(2,128)(2,1)S(1)}, bf16[1,384,2048]{2,0,1:T(2,128)(2,1)S(1)}) fusion(bf16[2,384,2048]{2,0,1:T(2,128)(2,1)S(1)} %all-to-all-done), kind=kLoop, calls=%fused_computation.64 | loop fusion | bytes 6291456 | tf_op jit(solution)/shard_map/slice | solution.py:22
  86.6 1.0 copy.110
  87.7 0.6 fusion.8
  88.7 0.9 fusion.1
  89.6 0.6 select_convert_fusion
  90.2 0.6 fusion.6
  90.8 1.7 add_convert_fusion
  92.6 1.9 copy.86
  94.4 1.3 copy.87
  95.8 1.1 multiply_reduce_fusion.2
  96.9 1.1 multiply_reduce_fusion.1
  98.0 1.1 broadcast_in_dim.30
  99.1 17.5 %all-to-all-start.3 = ((f32[32,1,4480]{2,1,0:T(1,128)}), f32[32,1,4480]{2,1,0:T(1,128)}, u32[]{:S(2)}, u32[]{:S(2)}) async-start(f32[32,1,4480]{2,1,0:T(1,128)} %broadcast_in_dim.30), calls=%async_computation.5 | async-start | bytes 1146880 | tf_op jit(solution)/shard_map/all_to_all | solution.py:48
  116.7 6.3 %reduce-scatter.3.cloned.1.call-done = bf16[16,384,64]{1,2,0:T(8,128)(2,1)} async-done(((bf16[32,384,64]{1,2,0:T(8,128)(2,1)}), bf16[16,384,64]{1,2,0:T(8,128)(2,1)}) %reduce-scatter.3.cloned.1.call-update) | async-done | bytes 786448 | tf_op jit(solution)/shard_map/reduce_scatter | solution.py:32
  123.0 29.6 %all-to-all-done.3 = f32[32,1,4480]{2,1,0:T(1,128)} async-done(((f32[32,1,4480]{2,1,0:T(1,128)}), f32[32,1,4480]{2,1,0:T(1,128)}, u32[]{:S(2)}, u32[]{:S(2)}) %all-to-all-start.3) | async-done | bytes 573472 | tf_op jit(solution)/shard_map/all_to_all | solution.py:48
  152.5 1.4 reduce_sum.73
  154.0 0.7 all_to_all.27
  154.7 8.8 %all-to-all-start.4 = ((f32[1,16,24]{2,0,1:T(1,128)}), f32[1,16,24]{2,0,1:T(1,128)S(1)}, u32[]{:S(2)}, u32[]{:S(2)}) async-start(f32[1,16,24]{2,0,1:T(1,128)} %all_to_all.27), calls=%async_computation.6 | async-start | bytes 16384 | tf_op jit(solution)/shard_map/all_to_all | solution.py:150
  163.5 2.3 %multiply_reduce_fusion = (f32[32]{0:T(128)}, f32[32,2048]{1,0:T(8,128)}) fusion(bf16[1,384,2048]{2,0,1:T(2,128)(2,1)S(1)} %copy-done.2, f32[384]{0:T(512)S(1)} %mul.93, f32[384,32]{0,1:T(8,128)S(1)} %get-tuple-element.65, f32[384,32]{0,1:T(8,128)S(1)} %fusion.8), kind=kOutput, calls=%fused_computation.12 | convolution fusion | flops 50597856 | bytes 1934976 | tf_op jit(solution)/shard_map/erf,erd->efd/dot_general | solution.py:131
  165.8 32.1 %reduce-scatter.5.cloned.1.call-done = bf16[1,384,64]{1,2,0:T(8,128)(2,1)} async-done(((bf16[16,384,64]{1,2,0:T(8,128)(2,1)}), bf16[1,384,64]{1,2,0:T(8,128)(2,1)}) %reduce-scatter.5.cloned.1.call-update) | async-done | bytes 49168 | tf_op jit(solution)/shard_map/reduce_scatter | solution.py:32
  197.9 1.0 copy.88
  198.9 0.5 broadcast.213
  199.4 1.2 reduce.20
  200.6 0.7 reshape.284
  201.4 7.7 %all-to-all-start.2 = ((bf16[16,2,768]{2,1,0:T(2,128)(2,1)}), bf16[16,2,768]{2,1,0:T(2,128)(2,1)S(1)}, u32[]{:S(2)}, u32[]{:S(2)}) async-start(bf16[16,2,768]{2,1,0:T(2,128)(2,1)} %reshape.284), calls=%async_computation.4 | async-start | bytes 98304 | tf_op jit(solution)/shard_map/all_to_all | solution.py:143
  209.1 0.6 fusion.24
  209.7 0.7 reduce.19
  210.5 1.9 gather_fusion.4
  212.6 0.6 copy.93
  213.2 2.1 all-to-all-done.2
  215.5 0.9 gather_fusion.3
  216.5 0.7 copy.92
  (47 shorter events, 2.6 us)
Async XLA Ops:
  7.2 82.5 %copy-start = (bf16[1,2048,32]{1,2,0:T(8,128)(2,1)S(1)}, bf16[1,2048,32]{1,2,0:T(8,128)(2,1)}, u32[]{:S(2)}) copy-start(bf16[1,2048,32]{1,2,0:T(8,128)(2,1)} %param.12) | copy-start | bytes 393220
  7.2 18.1 %copy-start.3 = (bf16[128,2048]{1,0:T(8,128)(2,1)S(1)}, bf16[128,2048]{1,0:T(8,128)(2,1)}, u32[]{:S(2)}) copy-start(bf16[128,2048]{1,0:T(8,128)(2,1)} %param.7) | copy-start | bytes 1572868
  12.6 12.7 %copy-start.4 = (bf16[128,2048]{1,0:T(8,128)(2,1)S(1)}, bf16[128,2048]{1,0:T(8,128)(2,1)}, u32[]{:S(2)}) copy-start(bf16[128,2048]{1,0:T(8,128)(2,1)} %param.10) | copy-start | bytes 1572868
  16.1 21.5 %all-to-all-start.1 = ((f32[1,16,24]{2,0,1:T(1,128)}), f32[1,16,24]{2,0,1:T(1,128)S(1)}, u32[]{:S(2)}, u32[]{:S(2)}) async-start(f32[1,16,24]{2,0,1:T(1,128)} %all_to_all.23), calls=%async_computation.1 | async-start | bytes 16384 | tf_op jit(solution)/shard_map/all_to_all | solution.py:118
  37.6 44.6 %all-to-all-start = ((bf16[2,384,2048]{2,0,1:T(2,128)(2,1)}), bf16[2,384,2048]{2,0,1:T(2,128)(2,1)S(1)}, u32[]{:S(2)}, u32[]{:S(2)}) async-start(bf16[2,384,2048]{2,0,1:T(2,128)(2,1)} %copy.82), calls=%async_computation | async-start | bytes 6291456 | tf_op jit(solution)/shard_map/all_to_all | solution.py:17
  44.8 78.1 %reduce-scatter.3.cloned.1.call-start = ((), (), s32[]{:S(2)}) async-start(), calls=%async_computation.7 | async-start | bytes 2359296 | tf_op jit(solution)/shard_map/reduce_scatter | solution.py:32
  86.6 1.7 copy-start.1
  86.6 1.0 copy-start.5
  87.6 1.1 copy-start.6
  98.0 65.5 %copy-start.2 = (bf16[1,384,2048]{2,0,1:T(2,128)(2,1)S(1)}, bf16[1,384,2048]{2,0,1:T(2,128)(2,1)}, u32[]{:S(2)}) copy-start(bf16[1,384,2048]{2,0,1:T(2,128)(2,1)} %copy-done.1) | copy-start | bytes 4718596
  99.1 53.4 %all-to-all-start.3 = ((f32[32,1,4480]{2,1,0:T(1,128)}), f32[32,1,4480]{2,1,0:T(1,128)}, u32[]{:S(2)}, u32[]{:S(2)}) async-start(f32[32,1,4480]{2,1,0:T(1,128)} %broadcast_in_dim.30), calls=%async_computation.5 | async-start | bytes 1146880 | tf_op jit(solution)/shard_map/all_to_all | solution.py:48
  116.6 81.3 %reduce-scatter.5.cloned.1.call-start = ((), (), s32[]{:S(2)}) async-start(), calls=%async_computation.8 | async-start | bytes 835584 | tf_op jit(solution)/shard_map/reduce_scatter | solution.py:32
  154.7 46.7 %all-to-all-start.4 = ((f32[1,16,24]{2,0,1:T(1,128)}), f32[1,16,24]{2,0,1:T(1,128)S(1)}, u32[]{:S(2)}, u32[]{:S(2)}) async-start(f32[1,16,24]{2,0,1:T(1,128)} %all_to_all.27), calls=%async_computation.6 | async-start | bytes 16384 | tf_op jit(solution)/shard_map/all_to_all | solution.py:150
  201.4 14.0 %all-to-all-start.2 = ((bf16[16,2,768]{2,1,0:T(2,128)(2,1)}), bf16[16,2,768]{2,1,0:T(2,128)(2,1)S(1)}, u32[]{:S(2)}, u32[]{:S(2)}) async-start(bf16[16,2,768]{2,1,0:T(2,128)(2,1)} %reshape.284), calls=%async_computation.4 | async-start | bytes 98304 | tf_op jit(solution)/shard_map/all_to_all | solution.py:143
Sparse Core Ops, SparseCore 0:
  95.9 26.9 reduce-scatter.2
  125.7 72.1 reduce-scatter.4
where the time goes:
time: 225 us; the launch traced here: 224 us
  waiting for transfers between devices  106 us (47%)
  starting transfers between devices  50.8 us (23%)
  local copies, waits for them, and re-layouts  36.8 us (16%)
  between operations  14.3 us (6%)
  matrix products  8.95 us (4%)
  other arithmetic  7.3 us (3%)
    reduce_scatter x2, waiting for transfers between devices, reduced_to_own(): tiles = lax.psum_scatter(tiles, axes[k], scatter_dimension=0, tiled=True)  38.3 us
    all_to_all x1, waiting for transfers between devices, side_by_side(): lax.all_to_all(both, axis, split_axis=split_dim, concat_axis=concat_dim,...  35.8 us
    all_to_all x1, waiting for transfers between devices, copy_for_each(): lax.all_to_all(jnp.broadcast_to(shard[None], (devices, *shard.shape)), ax...  29.6 us
    all_to_all x1, starting transfers between devices, copy_for_each(): lax.all_to_all(jnp.broadcast_to(shard[None], (devices, *shard.shape)), ax...  17.5 us
    all_to_all x1, starting transfers between devices, shards(): lax.all_to_all(gate_send.reshape(local_experts, slot_total), 'ep', split_...  9.14 us
    all_to_all x1, starting transfers between devices, shards(): lax.all_to_all(gate_sums, 'ep', split_axis=1, concat_axis=1, tiled=True)  8.84 us
    all_to_all x1, starting transfers between devices, shards(): lax.all_to_all(jnp.stack(grad_pieces), 'ep', split_axis=1, concat_axis=1,...  7.74 us
    all_to_all x1, starting transfers between devices, side_by_side(): lax.all_to_all(both, axis, split_axis=split_dim, concat_axis=concat_dim,...  7.28 us
  transfers between devices with their start and end apart: 7, of which 5 were waited for; matrix products, arithmetic and copies ran while one was open for 13% of the time, Pallas kernels for 0%

commit v1 on v0

v1 whole, which is shorter than its diff:
```python
import functools

import jax
import jax.numpy as jnp
from jax import lax
from jax.experimental import pallas as pl
from jax.experimental.pallas import tpu as pltpu
from jax.sharding import Mesh
from jax.sharding import PartitionSpec as P

clamp_limit = 7.0
sigmoid_scale = 1.702
HALF = 12
ROWS = 24
f32 = jnp.float32
bf16 = jnp.bfloat16

VMEM = pl.BlockSpec(memory_space=pltpu.VMEM)
SMEM = pl.BlockSpec(memory_space=pltpu.SMEM)


def nt(a, b):
    return lax.dot_general(a, b, (((1,), (1,)), ((), ())), preferred_element_type=f32)


def tn(a, b):
    return lax.dot_general(a, b, (((0,), (0,)), ((), ())), preferred_element_type=f32)


def iota(shape, dim):
    return lax.broadcasted_iota(jnp.int32, shape, dim)


def slot_keys(routes, experts):
    tok = routes.shape[1]
    e = iota((experts, tok), 0)
    first = jnp.broadcast_to(routes[0:1, :], (experts, tok)) == e
    second = jnp.broadcast_to(routes[1:2, :], (experts, tok)) == e
    named = jnp.where(first | second, 1.0, 0.0)
    before = jnp.where(iota((tok, tok), 0) < iota((tok, tok), 1), 1.0, 0.0).astype(bf16)
    rank = jnp.dot(named.astype(bf16), before, preferred_element_type=f32)
    return jnp.where(named > 0.0, rank, -1.0), first


def slot_target(tok, first_slot):
    r = iota((ROWS, 2 * tok), 0)
    h = jnp.where(iota((ROWS, 2 * tok), 1) >= tok, 1, 0)
    mine = jnp.where(r >= HALF, 1, 0) == h
    return jnp.where(mine, (first_slot + r - HALF * h).astype(f32), -2.0)


def pack_kernel(core_ref, routes_ref, gates_ref, tok_ref, cot_ref, out_ref, pick_ref, scale_ref):
    experts = out_ref.shape[0] // ROWS
    tok, width = tok_ref.shape
    key, first = slot_keys(routes_ref[...], experts)
    gate = jnp.where(
        first,
        jnp.broadcast_to(gates_ref[0:1, :], key.shape),
        jnp.broadcast_to(gates_ref[1:2, :], key.shape),
    )
    key2 = jnp.concatenate([key, key], axis=1)
    gate2 = jnp.concatenate([jnp.ones_like(gate), gate], axis=1)
    target = slot_target(tok, core_ref[0] * HALF)
    picks = jnp.concatenate(
        [jnp.where(target == key2[e : e + 1, :], 1.0, 0.0) for e in range(experts)], axis=0
    )
    scales = jnp.concatenate(
        [jnp.broadcast_to(gate2[e : e + 1, :], (ROWS, 2 * tok)) for e in range(experts)], axis=0
    )
    scale_ref[...] = jnp.broadcast_to(
        jnp.sum(picks * scales, axis=1, keepdims=True), scale_ref.shape
    )
    pick_ref[...] = picks.astype(bf16)
    step = min(512, width)

    @pl.loop(0, width // step)
    def _(n):
        cols = pl.ds(pl.multiple_of(n * step, step), step)
        both = jnp.concatenate([tok_ref[:, cols], cot_ref[:, cols]], axis=0)
        rows = jnp.dot(pick_ref[...], both, preferred_element_type=f32)
        scale = jnp.concatenate([scale_ref[...]] * (step // 128), axis=1)
        out_ref[:, cols] = (rows * scale).astype(bf16)


def pack_rows(core, routes, gates, tokens, cotangent, experts):
    tok, width = tokens.shape
    return pl.pallas_call(
        pack_kernel,
        out_shape=jax.ShapeDtypeStruct((experts * ROWS, width), bf16),
        in_specs=[SMEM, VMEM, VMEM, VMEM, VMEM],
        out_specs=VMEM,
        scratch_shapes=[
            pltpu.VMEM((experts * ROWS, 2 * tok), bf16),
            pltpu.VMEM((experts * ROWS, 128), f32),
        ],
        name="pack_rows",
    )(core, routes, gates, tokens, cotangent)


def unit_kernel(rows_ref, wall_ref, wret_ref, grads_ref, msg_ref):
    count = rows_ref.shape[0]
    sources = count // ROWS
    units = wall_ref.shape[0] // 3
    pre = nt(rows_ref[...], wall_ref[...])
    glu_pre = pre[:, :units]
    lin_pre = pre[:, units : 2 * units]
    hid_grad = jnp.roll(pre[:, 2 * units :], -HALF, axis=0)
    keep = lax.rem(iota((count, units), 0), ROWS) < HALF
    glu_clip = jnp.minimum(glu_pre, clamp_limit)
    lin_clip = jnp.clip(lin_pre, -clamp_limit, clamp_limit)
    sig = jax.nn.sigmoid(sigmoid_scale * glu_clip)
    glu_act = glu_clip * sig
    hidden = glu_act * (lin_clip + 1.0)
    slope = sig + sigmoid_scale * glu_clip * sig * (1.0 - sig)
    glu_grad = jnp.where(
        keep & (glu_pre < clamp_limit), hid_grad * (lin_clip + 1.0) * slope, 0.0
    )
    lin_grad = jnp.where(keep & (jnp.abs(lin_pre) < clamp_limit), hid_grad * glu_act, 0.0)
    hidden = jnp.where(keep, hidden, 0.0)
    gate_part = jnp.sum(hid_grad * hidden, axis=1, keepdims=True)
    both = jnp.concatenate([glu_grad, lin_grad], axis=1)
    down = jnp.roll(hidden, HALF, axis=0)
    grads_ref[...] = jnp.concatenate([both, down], axis=1).astype(bf16)
    shifted = jnp.roll(both, HALF, axis=0)
    left = jnp.concatenate([both, shifted], axis=1).astype(bf16)
    lanes = iota((count, 128), 1) == lax.rem(iota((count, 128), 0), ROWS)
    spread = jnp.where(lanes, gate_part, 0.0).reshape(sources, ROWS, 128)
    parts = jnp.sum(spread, axis=1, keepdims=True)
    high = parts.astype(bf16).astype(f32)
    row = iota((sources, 8, 128), 1)
    tail = jnp.where(row == 0, high, jnp.where(row == 1, parts - high, 0.0)).astype(bf16)
    blocks = wret_ref.shape[2] // 128
    for core in range(2):
        part = jnp.dot(left, wret_ref[core], preferred_element_type=f32).astype(bf16)
        for q in range(blocks):
            msg_ref[:, core, q * ROWS : (q + 1) * ROWS, :] = part[
                :, q * 128 : (q + 1) * 128
            ].reshape(sources, ROWS, 128)
        msg_ref[:, core, blocks * ROWS :, :] = tail


def units(rows, wall, wret):
    count = rows.shape[0]
    height = wret.shape[2] // 128 * ROWS + 8
    return pl.pallas_call(
        unit_kernel,
        out_shape=(
            jax.ShapeDtypeStruct((count, wall.shape[0]), bf16),
            jax.ShapeDtypeStruct((count // ROWS, 2, height, 128), bf16),
        ),
        in_specs=[VMEM, VMEM, VMEM],
        out_specs=(VMEM, VMEM),
        name="units",
    )(rows, wall, wret)


def wgrad_kernel(grads_ref, rows_ref, own_ref, other_ref):
    step = min(512, rows_ref.shape[1])

    @pl.loop(0, rows_ref.shape[1] // step)
    def _(n):
        cols = pl.ds(pl.multiple_of(n * step, step), step)
        part = tn(grads_ref[...], rows_ref[:, cols])
        for k in range(3):
            own_ref[k, :, cols] = part[64 * k : 64 * k + 32, :]
            other_ref[k, :, cols] = part[64 * k + 32 : 64 * k + 64, :]


def wgrads(grads, rows):
    shape = jax.ShapeDtypeStruct((3, 32, rows.shape[1]), f32)
    return pl.pallas_call(
        wgrad_kernel,
        out_shape=(shape, shape),
        in_specs=[VMEM, VMEM],
        out_specs=(VMEM, VMEM),
        name="wgrads",
    )(grads, rows)


def total_kernel(own_ref, got_ref, glu_ref, lin_ref, down_ref, norms_ref, down_norms_ref):
    glu = own_ref[0] + got_ref[0]
    lin = own_ref[1] + got_ref[1]
    down = own_ref[2] + got_ref[2]
    glu_ref[...] = glu
    lin_ref[...] = lin
    down_ref[...] = down
    norms_ref[0:1, :] = jnp.sum(glu * glu, axis=0, keepdims=True)
    norms_ref[1:2, :] = jnp.sum(lin * lin, axis=0, keepdims=True)
    each = jnp.sum(down * down, axis=1, keepdims=True)
    spread = jnp.where(iota((32, 128), 0) == iota((32, 128), 1), each, 0.0)
    down_norms_ref[...] = jnp.sum(spread, axis=0, keepdims=True)


def totals(own, got):
    width = own.shape[2]
    shape = jax.ShapeDtypeStruct((32, width), f32)
    return pl.pallas_call(
        total_kernel,
        out_shape=(
            shape,
            shape,
            shape,
            jax.ShapeDtypeStruct((2, width), f32),
            jax.ShapeDtypeStruct((1, 128), f32),
        ),
        in_specs=[VMEM, VMEM],
        out_specs=(VMEM,) * 5,
        name="totals",
    )(own, got)


def combine_kernel(routes_ref, back_ref, norms_ref, got_ref, msg_ref):
    experts = back_ref.shape[0]
    height = back_ref.shape[2]
    blocks = (height - 8) // ROWS
    tok = routes_ref.shape[1]
    depth = msg_ref.shape[0]
    key, first = slot_keys(routes_ref[...], experts)
    key2 = jnp.concatenate([key, key], axis=1)
    targets = [slot_target(tok, core * HALF) for core in range(2)]
    picks = jnp.concatenate(
        [
            jnp.where(targets[core] == key2[e : e + 1, :], 1.0, 0.0)
            for e in range(experts)
            for core in range(2)
        ],
        axis=0,
    )
    pick = picks.astype(bf16)
    for q in range(blocks):
        rows = back_ref[:, :, q * ROWS : (q + 1) * ROWS, :].reshape(experts * 2 * ROWS, 128)
        sums = tn(rows, pick).astype(bf16)
        for h in range(2):
            for b in range(2):
                msg_ref[h * (depth // 2) + 2 * q + b, 0:64, :] = sums[
                    64 * b : 64 * b + 64, h * tok : (h + 1) * tok
                ]
    tail = back_ref[:, :, blocks * ROWS :, :].astype(f32).reshape(experts * 2, 8, 128)
    parts = tail[:, 0:1, :] + tail[:, 1:2, :]
    spread = jnp.broadcast_to(parts, (experts * 2, ROWS, 128)).reshape(experts * 2 * ROWS, 128)
    shape = spread.shape
    lanes = iota(shape, 1) == lax.rem(iota(shape, 0), ROWS)
    column = jnp.sum(jnp.where(lanes, spread, 0.0), axis=1, keepdims=True)
    placed = (picks[:, :tok] * column).reshape(experts, 2 * ROWS, tok)
    each = jnp.sum(placed, axis=1)
    named_first = jnp.sum(jnp.where(first, each, 0.0), axis=0, keepdims=True)
    named_second = jnp.sum(jnp.where(first, 0.0, each), axis=0, keepdims=True)
    high_first = named_first.astype(bf16).astype(f32)
    high_second = named_second.astype(bf16).astype(f32)
    row = iota((8, 128), 0)
    gate_rows = jnp.where(row == 0, high_first, jnp.where(row == 1, high_second, 0.0))
    gate_rows = jnp.where(row == 2, named_first - high_first, gate_rows)
    gate_rows = jnp.where(row == 3, named_second - high_second, gate_rows)
    normed = norms_ref[...] + got_ref[...]
    count = normed.shape[1] // 128
    lines = jnp.concatenate(
        [normed[k : k + 1, n * 128 : (n + 1) * 128] for k in range(2) for n in range(count)], axis=0
    )
    extra = jnp.concatenate([lines, gate_rows], axis=0).astype(bf16)
    for z in range(depth):
        msg_ref[z, 64:, :] = extra


def combine(routes, back, norms, got, depth):
    height = 64 + 2 * norms.shape[1] // 128 + 8
    return pl.pallas_call(
        combine_kernel,
        out_shape=jax.ShapeDtypeStruct((depth, height, 128), bf16),
        in_specs=[VMEM] * 4,
        out_specs=VMEM,
        name="combine",
    )(routes, back, norms, got)


def finish_kernel(parts_ref, gates_ref, tok_ref, gate_ref, norms_ref):
    total = jnp.sum(parts_ref[...].astype(f32), axis=0)
    lines = norms_ref.shape[0]
    tok_ref[...] = total[:64, :].astype(bf16)
    norms_ref[...] = total[64 : 64 + lines, :]
    tail = total[64 + lines :, :]
    gate_ref[...] = (tail[0:2, :] + tail[2:4, :]) / gates_ref[...]


def finish(parts, gates):
    lines = parts.shape[1] - 72
    return pl.pallas_call(
        finish_kernel,
        out_shape=(
            jax.ShapeDtypeStruct((64, 128), bf16),
            jax.ShapeDtypeStruct((2, 128), f32),
            jax.ShapeDtypeStruct((lines, 128), f32),
        ),
        in_specs=[VMEM] * 2,
        out_specs=(VMEM,) * 3,
        name="finish",
    )(parts, gates)


def swap(x):
    return lax.ppermute(x, "tp_1", [(0, 1), (1, 0)])


def shards(tokens, routes, gates, cotangent, w_glu, w_lin, w_down):
    experts = lax.axis_size("ep")
    depth = lax.axis_size("tp_0")
    tok, width = tokens.shape
    core = lax.axis_index("tp_1").astype(jnp.int32).reshape(1)
    routes_t, gates_t = routes.T, gates.T
    glu_t, lin_t, down = w_glu[0].T, w_lin[0].T, w_down[0]

    packed = pack_rows(core, routes_t, gates_t, tokens, cotangent, experts)
    rows = lax.all_to_all(packed.reshape(experts, ROWS, width), "ep", 0, 0, tiled=True)
    rows = rows.reshape(experts * ROWS, width)

    glu_o, lin_o, down_o = swap(glu_t), swap(lin_t), swap(down)
    wall = jnp.concatenate([glu_t, glu_o, lin_t, lin_o, down, down_o], axis=0)
    inner = wall[:128].reshape(128, 2, depth // 2, 2, 64)
    wret = inner.transpose(3, 1, 0, 2, 4).reshape(2, 256, width // 4)

    grads, msg = units(rows, wall, wret)
    msg = msg.reshape(experts * 2, *msg.shape[2:])
    back = lax.all_to_all(msg, ("ep", "tp_1"), 0, 0, tiled=True)
    back = back.reshape(experts, 2, *msg.shape[1:])

    own, other = wgrads(grads, rows)
    glu_wg, lin_wg, down_wg, norms, down_norms = totals(own, swap(other))
    msg = combine(routes_t, back, norms, swap(norms), depth)
    parts = lax.all_to_all(msg, "tp_0", 0, 0, tiled=True)
    tok_t, gate_t, lines = finish(parts, gates_t)
    lines = lines.reshape(2, width)
    return (
        tok_t.T,
        gate_t.T,
        glu_wg.T[None],
        lin_wg.T[None],
        down_wg[None],
        lines[0:1],
        lines[1:2],
        down_norms[:, :32],
    )


def solution(mesh):
    depth = mesh.shape["tp"] // 2
    split = Mesh(mesh.devices.reshape(mesh.shape["ep"], depth, 2), ("ep", "tp_0", "tp_1"))
    tp = ("tp_0", "tp_1")
    return jax.shard_map(
        shards,
        mesh=split,
        in_specs=(
            P("ep", None),
            P("ep", None),
            P("ep", None),
            P("ep", None),
            P("ep", None, tp),
            P("ep", None, tp),
            P("ep", tp, None),
        ),
        out_specs=(
            P("ep", tp),
            P("ep", None),
            P("ep", None, tp),
            P("ep", None, tp),
            P("ep", tp, None),
            P("ep", None),
            P("ep", None),
            P("ep", tp),
        ),
        check_vma=False,
    )
```

time: 225 us -> 108 us (0.48)
  waiting for transfers between devices: 106 us -> 11 us
  blocking collectives: 0 us -> 41.9 us
  local copies, waits for them, and re-layouts: 36.8 us -> 10.5 us
  starting transfers between devices: 50.8 us -> 25.3 us
  Pallas kernels: 0 us -> 18.2 us
  between operations: 14.3 us -> 0.74 us
  matrix products: 8.95 us -> 0 us
  other arithmetic: 7.3 us -> 0.04 us
    all_to_all x5 -> x2, waiting for transfers between devices: 67.5 us -> 7.41 us  [the longest x1 7.41 us: shards(): lax.all_to_all(packed.reshape(experts, ROWS, width), 'ep', 0, 0, tiled=True)]
    all_to_all x0 -> x1, blocking collectives: none -> 41.9 us  [shards(): parts = lax.all_to_all(msg, 'tp_0', 0, 0, tiled=True)]
    reduce_scatter x2 -> x0, waiting for transfers between devices: 38.3 us -> none  [reduced_to_own(): tiles = lax.psum_scatter(tiles, axes[k], scatter_dimension=0, tiled=True)]
    all_to_all x5 -> x2, starting transfers between devices: 50.5 us -> 15 us  [the longest x1 9.51 us: shards(): lax.all_to_all(packed.reshape(experts, ROWS, width), 'ep', 0, 0, tiled=True)]
    pallas_call x0 -> x6, Pallas kernels: none -> 18.2 us  [the longest x1 4.12 us: units(): pl.pallas_call(unit_kernel, out_shape=(jax.ShapeDtypeStruct((count, wall....]
    gather x5 -> x0, local copies, waits for them, and re-layouts: 11.2 us -> none  [the longest x2 5.59 us: pick_rows(): padded[slot_token].reshape(local_experts, slot_total, source_rows.shape[1])]
    ppermute x0 -> x5, starting transfers between devices: none -> 10.3 us  [swap(): return lax.ppermute(x, 'tp_1', [(0, 1), (1, 0)])]
    dot_general x8 -> x0, matrix products: 8.95 us -> none  [the longest x1 2.33 us: shards(): jnp.einsum('erf,erd->efd', hidden_gated, cot_recv, preferred_element_type...]
  transfers between devices with their start and end apart: 7 -> 7, of which waited for: 5 -> 3; matrix products, arithmetic and copies ran while one was open for 13% -> 6% of each run, Pallas kernels for 0% -> 6%
where the time goes in v1:
time: 108 us
  blocking collectives  41.9 us (39%)
  starting transfers between devices  25.3 us (23%)
  Pallas kernels  18.2 us (17%)
  waiting for transfers between devices  11 us (10%)
  local copies, waits for them, and re-layouts  10.5 us (10%)
    all_to_all x1, blocking collectives, shards(): parts = lax.all_to_all(msg, 'tp_0', 0, 0, tiled=True)  41.9 us
    ppermute x5, starting transfers between devices, swap(): return lax.ppermute(x, 'tp_1', [(0, 1), (1, 0)])  10.3 us
    all_to_all x1, starting transfers between devices, shards(): lax.all_to_all(packed.reshape(experts, ROWS, width), 'ep', 0, 0, tiled=True)  9.51 us
    all_to_all x1, waiting for transfers between devices, shards(): lax.all_to_all(packed.reshape(experts, ROWS, width), 'ep', 0, 0, tiled=True)  7.41 us
    unnamed x19, local copies, waits for them, and re-layouts  6.27 us
    all_to_all x1, starting transfers between devices, shards(): back = lax.all_to_all(msg, ('ep', 'tp_1'), 0, 0, tiled=True)  5.48 us
    pallas_call x1, Pallas kernels, units(): pl.pallas_call(unit_kernel, out_shape=(jax.ShapeDtypeStruct((count, wall....  4.12 us
    pallas_call x1, Pallas kernels, wgrads(): pl.pallas_call(wgrad_kernel, out_shape=(shape, shape), in_specs=[VMEM, VM...  3.83 us
  transfers between devices with their start and end apart: 7, of which 3 were waited for; matrix products, arithmetic and copies ran while one was open for 6% of the time, Pallas kernels for 6%

profile of v1, /device:TPU:2, one launch (start us, length us, event | category | flops | bytes accessed | tf_op | source)
XLA Modules:
  0.0 107.6 jit_solution(16334621178363178001)
XLA Ops:
  0.6 3.8 %pack_rows.1 = bf16[384,2048]{1,0:T(8,128)(2,1)} custom-call(s32[1]{0:T(128)} %bitcast.1.core_ref, s32[2,128]{1,0:T(2,128)} %bitcast.49, f32[2,128]{1,0:T(2,128)} %bitcast.47, bf16[128,2048]{1,0:T(8,128)(2,1)} %tok_ref.1, bf16[128,2048]{1,0:T(8,128)(2,1)} %cot_ref.1), custom_call_target="tpu_custom_call" | custom-call | tf_op jit(solution)/shard_map/pack_rows/pallas_call | solution.py:87
  4.4 0.0 copy-start.3
  4.4 0.0 copy-start.4
  4.4 0.0 copy-start.5
  4.4 9.5 %all-to-all-start = ((bf16[16,24,2048]{2,1,0:T(8,128)(2,1)}), bf16[16,24,2048]{2,1,0:T(8,128)(2,1)S(1)}, u32[]{:S(2)}, u32[]{:S(2)}) async-start(bf16[16,24,2048]{2,1,0:T(8,128)(2,1)} %bitcast.36), calls=%async_computation | async-start | bytes 3145728 | tf_op jit(solution)/shard_map/all_to_all | solution.py:312
  13.9 0.0 copy-done.3
  13.9 1.9 %collective-permute-start = (bf16[32,2048]{1,0:T(8,128)(2,1)S(1)}, bf16[32,2048]{1,0:T(8,128)(2,1)S(1)}, u32[]{:S(2)}, u32[]{:S(2)}) collective-permute-start(bf16[32,2048]{1,0:T(8,128)(2,1)S(1)} %bitcast.40), channel_id=1, source_target_pairs={{0,1},{1,0},{2,3},{3,2},{4,5},{5,4},{6,7},{7,6},{8,9},{9,8},{10,11... | collective-permute-start | bytes 393224 | tf_op jit(solution)/shard_map/ppermute | solution.py:300
  15.8 0.0 copy-done.4
  15.8 2.4 %collective-permute-start.1 = (bf16[32,2048]{1,0:T(8,128)(2,1)S(1)}, bf16[32,2048]{1,0:T(8,128)(2,1)S(1)}, u32[]{:S(2)}, u32[]{:S(2)}) collective-permute-start(bf16[32,2048]{1,0:T(8,128)(2,1)S(1)} %bitcast.42), channel_id=1, source_target_pairs={{0,1},{1,0},{2,3},{3,2},{4,5},{5,4},{6,7},{7,6},{8,9},{9,8},{10,11... | collective-permute-start | bytes 393224 | tf_op jit(solution)/shard_map/ppermute | solution.py:300
  18.3 0.0 copy-done.5
  18.3 1.9 %collective-permute-start.2 = (bf16[32,2048]{1,0:T(8,128)(2,1)S(1)}, bf16[32,2048]{1,0:T(8,128)(2,1)S(1)}, u32[]{:S(2)}, u32[]{:S(2)}) collective-permute-start(bf16[32,2048]{1,0:T(8,128)(2,1)S(1)} %bitcast.44), channel_id=1, source_target_pairs={{0,1},{1,0},{2,3},{3,2},{4,5},{5,4},{6,7},{7,6},{8,9},{9,8},{10,11... | collective-permute-start | bytes 393224 | tf_op jit(solution)/shard_map/ppermute | solution.py:300
  20.2 0.7 constant_dynamic-update-slice_fusion.5
  20.9 0.0 collective-permute-done
  20.9 0.7 constant_dynamic-update-slice_fusion.4
  21.5 0.7 constant_dynamic-update-slice_fusion.3
  22.2 0.0 collective-permute-done.1
  22.2 0.7 constant_dynamic-update-slice_fusion.2
  22.9 0.7 constant_dynamic-update-slice_fusion.1
  23.6 0.3 copy.16
  23.8 0.6 copy.19
  24.4 1.4 %reshape.47.wret_ref = bf16[2,256,512]{2,1,0:T(8,128)(2,1)} reshape(bf16[2,2,128,8,64]{4,3,2,1,0:T(8,128)(2,1)S(1)} %copy.19) | data formatting | bytes 1048576 | tf_op jit(solution)/shard_map/reshape | solution.py:318
  25.8 0.0 collective-permute-done.2
  25.8 0.7 constant_dynamic-update-slice_fusion.wall_ref
  26.5 7.4 %all-to-all-done = bf16[16,24,2048]{2,1,0:T(8,128)(2,1)S(1)} async-done(((bf16[16,24,2048]{2,1,0:T(8,128)(2,1)}), bf16[16,24,2048]{2,1,0:T(8,128)(2,1)S(1)}, u32[]{:S(2)}, u32[]{:S(2)}) %all-to-all-start) | async-done | bytes 1572896 | tf_op jit(solution)/shard_map/all_to_all | solution.py:312
  33.9 0.0 copy-start
  33.9 1.2 %copy-done = bf16[16,24,2048]{2,1,0:T(8,128)(2,1)} copy-done((bf16[16,24,2048]{2,1,0:T(8,128)(2,1)}, bf16[16,24,2048]{2,1,0:T(8,128)(2,1)S(1)}, u32[]{:S(2)}) %copy-start) | copy-done | bytes 1572888
  35.1 4.1 %units.1 = (bf16[384,192]{1,0:T(8,128)(2,1)}, bf16[16,2,104,128]{3,2,1,0:T(8,128)(2,1)}) custom-call(bf16[384,2048]{1,0:T(8,128)(2,1)} %bitcast.34, bf16[192,2048]{1,0:T(8,128)(2,1)} %constant_dynamic-update-slice_fusion.wall_ref, bf16[2,256,512]{2,1,0:T(8,128)(2,1)} %reshape.47.wret_ref), custom_call_target="tpu_custom_call" | custom-call | tf_op jit(solution)/shard_map/units/pallas_call | solution.py:145
  39.2 5.5 %all-to-all-start.1 = ((bf16[32,104,128]{2,1,0:T(8,128)(2,1)}), bf16[32,104,128]{2,1,0:T(8,128)(2,1)S(1)}, u32[]{:S(2)}, u32[]{:S(2)}) async-start(bf16[32,104,128]{2,1,0:T(8,128)(2,1)} %bitcast.39), calls=%async_computation.1 | async-start | bytes 1703936 | tf_op jit(solution)/shard_map/all_to_all | solution.py:322
  44.7 3.8 %wgrads.1 = (f32[3,32,2048]{2,1,0:T(8,128)}, f32[3,32,2048]{2,1,0:T(8,128)}) custom-call(bf16[384,192]{1,0:T(8,128)(2,1)} %get-tuple-element.21.grads_ref, bf16[384,2048]{1,0:T(8,128)(2,1)} %bitcast.35), custom_call_target="tpu_custom_call" | custom-call | tf_op jit(solution)/shard_map/wgrads/pallas_call | solution.py:171
  48.5 2.0 %collective-permute-start.3 = (f32[3,32,2048]{2,1,0:T(8,128)}, f32[3,32,2048]{2,1,0:T(8,128)S(1)}, u32[]{:S(2)}, u32[]{:S(2)}) collective-permute-start(f32[3,32,2048]{2,1,0:T(8,128)} %get-tuple-element.23), channel_id=1, source_target_pairs={{0,1},{1,0},{2,3},{3,2},{4,5},{5,4},{6,7},{7,6},{8,9},{9,8},{10,11... | collective-permute-start | bytes 2359304 | tf_op jit(solution)/shard_map/ppermute | solution.py:300
  50.5 2.4 %collective-permute-done.3.got_ref = f32[3,32,2048]{2,1,0:T(8,128)S(1)} collective-permute-done((f32[3,32,2048]{2,1,0:T(8,128)}, f32[3,32,2048]{2,1,0:T(8,128)S(1)}, u32[]{:S(2)}, u32[]{:S(2)}) %collective-permute-start.3) | collective-permute-done | bytes 786464 | tf_op jit(solution)/shard_map/ppermute | solution.py:300
  52.9 0.0 copy-start.2
  52.9 0.9 copy-done.2
  53.8 2.3 %totals.1 = (f32[32,2048]{1,0:T(8,128)}, f32[32,2048]{1,0:T(8,128)}, f32[32,2048]{1,0:T(8,128)}, f32[2,2048]{1,0:T(2,128)}, f32[1,128]{1,0:T(1,128)}) custom-call(f32[3,32,2048]{2,1,0:T(8,128)} %get-tuple-element.22.own_ref, f32[3,32,2048]{2,1,0:T(8,128)} %copy-done.2), custom_call_target="tpu_custom_call" | custom-call | tf_op jit(solution)/shard_map/totals/pallas_call | solution.py:197
  56.1 2.0 %collective-permute-start.4 = (f32[2,2048]{1,0:T(2,128)}, f32[2,2048]{1,0:T(2,128)S(1)}, u32[]{:S(2)}, u32[]{:S(2)}) collective-permute-start(f32[2,2048]{1,0:T(2,128)} %get-tuple-element.24.norms_ref), channel_id=1, source_target_pairs={{0,1},{1,0},{2,3},{3,2},{4,5},{5,4},{6,7},{7,6},{8,9},{9,8},{10,11... | collective-permute-start | bytes 49160 | tf_op jit(solution)/shard_map/ppermute | solution.py:300
  58.1 1.2 %collective-permute-done.4.got_ref = f32[2,2048]{1,0:T(2,128)S(1)} collective-permute-done((f32[2,2048]{1,0:T(2,128)}, f32[2,2048]{1,0:T(2,128)S(1)}, u32[]{:S(2)}, u32[]{:S(2)}) %collective-permute-start.4) | collective-permute-done | bytes 16416 | tf_op jit(solution)/shard_map/ppermute | solution.py:300
  59.4 0.0 copy-start.6
  59.4 0.0 all-to-all-done.1
  59.4 0.0 copy-start.1
  59.4 0.6 copy-done.6
  59.9 0.3 copy-done.1
  60.3 2.5 %combine.1 = bf16[16,104,128]{2,1,0:T(8,128)(2,1)} custom-call(s32[2,128]{1,0:T(2,128)} %bitcast.50, bf16[16,2,104,128]{3,2,1,0:T(8,128)(2,1)} %bitcast.37, f32[2,2048]{1,0:T(2,128)} %get-tuple-element.24.norms_ref, f32[2,2048]{1,0:T(2,128)} %copy-done.6), custom_call_target="tpu_custom_call" | custom-call | tf_op jit(solution)/shard_map/combine/pallas_call | solution.py:266
  62.8 41.9 %all_to_all.15.parts_ref = bf16[16,104,128]{2,1,0:T(8,128)(2,1)} all-to-all(bf16[16,104,128]{2,1,0:T(8,128)(2,1)} %combine.1), channel_id=1, replica_groups=mesh['ep'=16,'tp_0'=16,'tp_1'=2] {'tp_0'}, dimensions={0} | all-to-all | bytes 851968 | tf_op jit(solution)/shard_map/all_to_all | solution.py:328
  104.6 1.7 %finish.1 = (bf16[64,128]{1,0:T(8,128)(2,1)}, f32[2,128]{1,0:T(2,128)}, f32[32,128]{1,0:T(8,128)}) custom-call(bf16[16,104,128]{2,1,0:T(8,128)(2,1)} %all_to_all.15.parts_ref, f32[2,128]{1,0:T(2,128)} %bitcast.48), custom_call_target="tpu_custom_call" | custom-call | tf_op jit(solution)/shard_map/finish/pallas_call | solution.py:286
  106.3 1.3 %fusion = (f32[16,128]{1,0:T(8,128)}, f32[16,128]{1,0:T(8,128)}) fusion(f32[32,128]{1,0:T(8,128)} %get-tuple-element.30), kind=kLoop, calls=%fused_computation.7 | loop fusion | bytes 32768 | tf_op jit(solution)/shard_map/slice | solution.py:338
  (1 shorter events, 0.0 us)
Async XLA Ops:
  4.4 9.5 %copy-start.3 = (bf16[1,2048,32]{1,2,0:T(8,128)(2,1)S(1)}, bf16[1,2048,32]{1,2,0:T(8,128)(2,1)}, u32[]{:S(2)}) copy-start(bf16[1,2048,32]{1,2,0:T(8,128)(2,1)} %param.11) | copy-start | bytes 393220
  4.4 11.4 %copy-start.4 = (bf16[1,2048,32]{1,2,0:T(8,128)(2,1)S(1)}, bf16[1,2048,32]{1,2,0:T(8,128)(2,1)}, u32[]{:S(2)}) copy-start(bf16[1,2048,32]{1,2,0:T(8,128)(2,1)} %param.12) | copy-start | bytes 393220
  4.4 13.9 %copy-start.5 = (bf16[1,32,2048]{2,1,0:T(8,128)(2,1)S(1)}, bf16[1,32,2048]{2,1,0:T(8,128)(2,1)}, u32[]{:S(2)}) copy-start(bf16[1,32,2048]{2,1,0:T(8,128)(2,1)} %param.13) | copy-start | bytes 393220
  4.4 29.5 %all-to-all-start = ((bf16[16,24,2048]{2,1,0:T(8,128)(2,1)}), bf16[16,24,2048]{2,1,0:T(8,128)(2,1)S(1)}, u32[]{:S(2)}, u32[]{:S(2)}) async-start(bf16[16,24,2048]{2,1,0:T(8,128)(2,1)} %bitcast.36), calls=%async_computation | async-start | bytes 3145728 | tf_op jit(solution)/shard_map/all_to_all | solution.py:312
  13.9 7.0 %collective-permute-start = (bf16[32,2048]{1,0:T(8,128)(2,1)S(1)}, bf16[32,2048]{1,0:T(8,128)(2,1)S(1)}, u32[]{:S(2)}, u32[]{:S(2)}) collective-permute-start(bf16[32,2048]{1,0:T(8,128)(2,1)S(1)} %bitcast.40), channel_id=1, source_target_pairs={{0,1},{1,0},{2,3},{3,2},{4,5},{5,4},{6,7},{7,6},{8,9},{9,8},{10,11... | collective-permute-start | bytes 393224 | tf_op jit(solution)/shard_map/ppermute | solution.py:300
  15.8 6.3 %collective-permute-start.1 = (bf16[32,2048]{1,0:T(8,128)(2,1)S(1)}, bf16[32,2048]{1,0:T(8,128)(2,1)S(1)}, u32[]{:S(2)}, u32[]{:S(2)}) collective-permute-start(bf16[32,2048]{1,0:T(8,128)(2,1)S(1)} %bitcast.42), channel_id=1, source_target_pairs={{0,1},{1,0},{2,3},{3,2},{4,5},{5,4},{6,7},{7,6},{8,9},{9,8},{10,11... | collective-permute-start | bytes 393224 | tf_op jit(solution)/shard_map/ppermute | solution.py:300
  18.3 7.5 %collective-permute-start.2 = (bf16[32,2048]{1,0:T(8,128)(2,1)S(1)}, bf16[32,2048]{1,0:T(8,128)(2,1)S(1)}, u32[]{:S(2)}, u32[]{:S(2)}) collective-permute-start(bf16[32,2048]{1,0:T(8,128)(2,1)S(1)} %bitcast.44), channel_id=1, source_target_pairs={{0,1},{1,0},{2,3},{3,2},{4,5},{5,4},{6,7},{7,6},{8,9},{9,8},{10,11... | collective-permute-start | bytes 393224 | tf_op jit(solution)/shard_map/ppermute | solution.py:300
  33.9 1.2 %copy-start = (bf16[16,24,2048]{2,1,0:T(8,128)(2,1)}, bf16[16,24,2048]{2,1,0:T(8,128)(2,1)S(1)}, u32[]{:S(2)}) copy-start(bf16[16,24,2048]{2,1,0:T(8,128)(2,1)S(1)} %all-to-all-done) | copy-start | bytes 4718596
  39.2 20.2 %all-to-all-start.1 = ((bf16[32,104,128]{2,1,0:T(8,128)(2,1)}), bf16[32,104,128]{2,1,0:T(8,128)(2,1)S(1)}, u32[]{:S(2)}, u32[]{:S(2)}) async-start(bf16[32,104,128]{2,1,0:T(8,128)(2,1)} %bitcast.39), calls=%async_computation.1 | async-start | bytes 1703936 | tf_op jit(solution)/shard_map/all_to_all | solution.py:322
  48.5 4.4 %collective-permute-start.3 = (f32[3,32,2048]{2,1,0:T(8,128)}, f32[3,32,2048]{2,1,0:T(8,128)S(1)}, u32[]{:S(2)}, u32[]{:S(2)}) collective-permute-start(f32[3,32,2048]{2,1,0:T(8,128)} %get-tuple-element.23), channel_id=1, source_target_pairs={{0,1},{1,0},{2,3},{3,2},{4,5},{5,4},{6,7},{7,6},{8,9},{9,8},{10,11... | collective-permute-start | bytes 2359304 | tf_op jit(solution)/shard_map/ppermute | solution.py:300
  52.9 0.9 copy-start.2
  56.1 3.3 %collective-permute-start.4 = (f32[2,2048]{1,0:T(2,128)}, f32[2,2048]{1,0:T(2,128)S(1)}, u32[]{:S(2)}, u32[]{:S(2)}) collective-permute-start(f32[2,2048]{1,0:T(2,128)} %get-tuple-element.24.norms_ref), channel_id=1, source_target_pairs={{0,1},{1,0},{2,3},{3,2},{4,5},{5,4},{6,7},{7,6},{8,9},{9,8},{10,11... | collective-permute-start | bytes 49160 | tf_op jit(solution)/shard_map/ppermute | solution.py:300
  59.4 0.6 copy-start.6
  59.4 0.9 copy-start.1

commit v2 on v1

--- a/solution.py
+++ b/solution.py
@@ -11,6 +11,7 @@
 clamp_limit = 7.0
 sigmoid_scale = 1.702
 HALF = 12
+LIMIT = 24 * 1024 * 1024
 ROWS = 24
 f32 = jnp.float32
 bf16 = jnp.bfloat16
@@ -150,6 +151,7 @@
         ),
         in_specs=[VMEM, VMEM, VMEM],
         out_specs=(VMEM, VMEM),
+        compiler_params=pltpu.CompilerParams(vmem_limit_bytes=LIMIT),
         name="units",
     )(rows, wall, wret)
 
@@ -173,6 +175,7 @@
         out_shape=(shape, shape),
         in_specs=[VMEM, VMEM],
         out_specs=(VMEM, VMEM),
+        compiler_params=pltpu.CompilerParams(vmem_limit_bytes=LIMIT),
         name="wgrads",
     )(grads, rows)
 
@@ -205,6 +208,7 @@
         ),
         in_specs=[VMEM, VMEM],
         out_specs=(VMEM,) * 5,
+        compiler_params=pltpu.CompilerParams(vmem_limit_bytes=LIMIT),
         name="totals",
     )(own, got)
 
@@ -268,30 +272,34 @@
         out_shape=jax.ShapeDtypeStruct((depth, height, 128), bf16),
         in_specs=[VMEM] * 4,
         out_specs=VMEM,
+        compiler_params=pltpu.CompilerParams(vmem_limit_bytes=LIMIT),
         name="combine",
     )(routes, back, norms, got)
 
 
-def finish_kernel(parts_ref, gates_ref, tok_ref, gate_ref, norms_ref):
+def finish_kernel(parts_ref, gates_ref, tok_ref, gate_ref, glu_ref, lin_ref):
     total = jnp.sum(parts_ref[...].astype(f32), axis=0)
-    lines = norms_ref.shape[0]
+    lines = glu_ref.shape[0]
     tok_ref[...] = total[:64, :].astype(bf16)
-    norms_ref[...] = total[64 : 64 + lines, :]
-    tail = total[64 + lines :, :]
+    glu_ref[...] = total[64 : 64 + lines, :]
+    lin_ref[...] = total[64 + lines : 64 + 2 * lines, :]
+    tail = total[64 + 2 * lines :, :]
     gate_ref[...] = (tail[0:2, :] + tail[2:4, :]) / gates_ref[...]
 
 
 def finish(parts, gates):
-    lines = parts.shape[1] - 72
+    lines = (parts.shape[1] - 72) // 2
     return pl.pallas_call(
         finish_kernel,
         out_shape=(
             jax.ShapeDtypeStruct((64, 128), bf16),
             jax.ShapeDtypeStruct((2, 128), f32),
             jax.ShapeDtypeStruct((lines, 128), f32),
+            jax.ShapeDtypeStruct((lines, 128), f32),
         ),
         in_specs=[VMEM] * 2,
-        out_specs=(VMEM,) * 3,
+        out_specs=(VMEM,) * 4,
+        compiler_params=pltpu.CompilerParams(vmem_limit_bytes=LIMIT),
         name="finish",
     )(parts, gates)
 
@@ -326,16 +334,15 @@
     glu_wg, lin_wg, down_wg, norms, down_norms = totals(own, swap(other))
     msg = combine(routes_t, back, norms, swap(norms), depth)
     parts = lax.all_to_all(msg, "tp_0", 0, 0, tiled=True)
-    tok_t, gate_t, lines = finish(parts, gates_t)
-    lines = lines.reshape(2, width)
+    tok_t, gate_t, glu_norms, lin_norms = finish(parts, gates_t)
     return (
         tok_t.T,
         gate_t.T,
         glu_wg.T[None],
         lin_wg.T[None],
         down_wg[None],
-        lines[0:1],
-        lines[1:2],
+        glu_norms.reshape(1, width),
+        lin_norms.reshape(1, width),
         down_norms[:, :32],
     )
 

time: 108 us -> 99.5 us (0.921)
  Pallas kernels: 18.2 us -> 8.55 us
  waiting for transfers between devices: 11 us -> 16.7 us
  local copies, waits for them, and re-layouts: 10.5 us -> 5.55 us
    unnamed x19 -> x17, local copies, waits for them, and re-layouts: 6.27 us -> 0.98 us
    all_to_all x1, waiting for transfers between devices: 0.01 us -> 4.61 us  [shards(): back = lax.all_to_all(msg, ('ep', 'tp_1'), 0, 0, tiled=True)]
    pallas_call x1, Pallas kernels: 3.83 us -> 1.16 us  [wgrads(): pl.pallas_call(wgrad_kernel, out_shape=(shape, shape), in_specs=[VMEM, VM...]
    pallas_call x1, Pallas kernels: 4.12 us -> 1.46 us  [units(): pl.pallas_call(unit_kernel, out_shape=(jax.ShapeDtypeStruct((count, wall....]
    pallas_call x1, Pallas kernels: 2.5 us -> 0.57 us  [combine(): pl.pallas_call(combine_kernel, out_shape=jax.ShapeDtypeStruct((depth, hei...]
    all_to_all x1, waiting for transfers between devices: 7.41 us -> 8.93 us  [shards(): lax.all_to_all(packed.reshape(experts, ROWS, width), 'ep', 0, 0, tiled=True)]
    reshape x2, local copies, waits for them, and re-layouts: 1.97 us -> 3.38 us  [shards(): wret = inner.transpose(3, 1, 0, 2, 4).reshape(2, 256, width // 4)]
    pallas_call x1, Pallas kernels: 2.31 us -> 0.95 us  [totals(): pl.pallas_call(total_kernel, out_shape=(shape, shape, shape, jax.ShapeDty...]
  transfers between devices with their start and end apart: 7 -> 7, of which waited for: 3 -> 4; matrix products, arithmetic and copies ran while one was open for 6% -> 5% of each run, Pallas kernels for 6% -> 2%
where the time goes in v2:
time: 99.5 us; the launch traced here: 99 us
  blocking collectives  42 us (42%)
  starting transfers between devices  25.3 us (25%)
  waiting for transfers between devices  16.7 us (17%)
  Pallas kernels  8.55 us (9%)
  local copies, waits for them, and re-layouts  5.55 us (6%)
    all_to_all x1, blocking collectives, shards(): parts = lax.all_to_all(msg, 'tp_0', 0, 0, tiled=True)  42 us
    ppermute x5, starting transfers between devices, swap(): return lax.ppermute(x, 'tp_1', [(0, 1), (1, 0)])  10.3 us
    all_to_all x1, starting transfers between devices, shards(): lax.all_to_all(packed.reshape(experts, ROWS, width), 'ep', 0, 0, tiled=True)  9.51 us
    all_to_all x1, waiting for transfers between devices, shards(): lax.all_to_all(packed.reshape(experts, ROWS, width), 'ep', 0, 0, tiled=True)  8.93 us
    all_to_all x1, starting transfers between devices, shards(): back = lax.all_to_all(msg, ('ep', 'tp_1'), 0, 0, tiled=True)  5.48 us
    all_to_all x1, waiting for transfers between devices, shards(): back = lax.all_to_all(msg, ('ep', 'tp_1'), 0, 0, tiled=True)  4.61 us
    pallas_call x1, Pallas kernels, pack_rows(): pl.pallas_call(pack_kernel, out_shape=jax.ShapeDtypeStruct((experts * ROW...  3.75 us
    reshape x2, local copies, waits for them, and re-layouts, shards(): wret = inner.transpose(3, 1, 0, 2, 4).reshape(2, 256, width // 4)  3.38 us
  transfers between devices with their start and end apart: 7, of which 4 were waited for; matrix products, arithmetic and copies ran while one was open for 5% of the time, Pallas kernels for 2%

profile of v2, /device:TPU:2, one launch (start us, length us, event | category | flops | bytes accessed | tf_op | source)
XLA Modules:
  0.0 99.0 jit_solution(17919892958041572502)
XLA Ops:
  0.6 3.8 %pack_rows.1 = bf16[384,2048]{1,0:T(8,128)(2,1)} custom-call(s32[1]{0:T(128)} %bitcast.1.core_ref, s32[2,128]{1,0:T(2,128)} %bitcast.40, f32[2,128]{1,0:T(2,128)} %bitcast.38, bf16[128,2048]{1,0:T(8,128)(2,1)} %tok_ref.1, bf16[128,2048]{1,0:T(8,128)(2,1)} %cot_ref.1), custom_call_target="tpu_custom_call" | custom-call | tf_op jit(solution)/shard_map/pack_rows/pallas_call | solution.py:88
  4.4 0.0 copy-start.3
  4.4 0.0 copy-start.4
  4.4 0.0 copy-start.5
  4.4 9.5 %all-to-all-start = ((bf16[16,24,2048]{2,1,0:T(8,128)(2,1)}), bf16[16,24,2048]{2,1,0:T(8,128)(2,1)S(1)}, u32[]{:S(2)}, u32[]{:S(2)}) async-start(bf16[16,24,2048]{2,1,0:T(8,128)(2,1)} %bitcast.42), calls=%async_computation | async-start | bytes 3145728 | tf_op jit(solution)/shard_map/all_to_all | solution.py:320
  13.9 0.0 copy-done.3
  13.9 1.9 %collective-permute-start = (bf16[32,2048]{1,0:T(8,128)(2,1)S(1)}, bf16[32,2048]{1,0:T(8,128)(2,1)S(1)}, u32[]{:S(2)}, u32[]{:S(2)}) collective-permute-start(bf16[32,2048]{1,0:T(8,128)(2,1)S(1)} %bitcast.44), channel_id=1, source_target_pairs={{0,1},{1,0},{2,3},{3,2},{4,5},{5,4},{6,7},{7,6},{8,9},{9,8},{10,11... | collective-permute-start | bytes 393224 | tf_op jit(solution)/shard_map/ppermute | solution.py:308
  15.8 0.0 copy-done.4
  15.8 2.4 %collective-permute-start.1 = (bf16[32,2048]{1,0:T(8,128)(2,1)S(1)}, bf16[32,2048]{1,0:T(8,128)(2,1)S(1)}, u32[]{:S(2)}, u32[]{:S(2)}) collective-permute-start(bf16[32,2048]{1,0:T(8,128)(2,1)S(1)} %bitcast.46), channel_id=1, source_target_pairs={{0,1},{1,0},{2,3},{3,2},{4,5},{5,4},{6,7},{7,6},{8,9},{9,8},{10,11... | collective-permute-start | bytes 393224 | tf_op jit(solution)/shard_map/ppermute | solution.py:308
  18.3 0.0 copy-done.5
  18.3 1.9 %collective-permute-start.2 = (bf16[32,2048]{1,0:T(8,128)(2,1)S(1)}, bf16[32,2048]{1,0:T(8,128)(2,1)}, u32[]{:S(2)}, u32[]{:S(2)}) collective-permute-start(bf16[32,2048]{1,0:T(8,128)(2,1)S(1)} %bitcast.48), channel_id=1, source_target_pairs={{0,1},{1,0},{2,3},{3,2},{4,5},{5,4},{6,7},{7,6},{8,9},{9,8},{10,11... | collective-permute-start | bytes 393224 | tf_op jit(solution)/shard_map/ppermute | solution.py:308
  20.2 0.0 collective-permute-done
  20.3 0.0 collective-permute-done.1
  20.4 0.3 copy.16
  20.6 1.5 %copy.19 = bf16[2,2,128,8,64]{4,3,2,1,0:T(8,128)(2,1)} copy(bf16[2,2,128,8,64]{2,4,0,3,1:T(8,128)(2,1)S(1)} %bitcast.43) | data formatting | bytes 1048576 | tf_op jit(solution)/shard_map/reshape | solution.py:326
  22.1 1.9 %reshape.52.wret_ref = bf16[2,256,512]{2,1,0:T(8,128)(2,1)S(1)} reshape(bf16[2,2,128,8,64]{4,3,2,1,0:T(8,128)(2,1)} %copy.19) | data formatting | bytes 1048576 | tf_op jit(solution)/shard_map/reshape | solution.py:326
  24.0 0.0 collective-permute-done.2
  24.0 0.9 constant_dynamic-update-slice_fusion.wall_ref
  25.0 8.9 %all-to-all-done = bf16[16,24,2048]{2,1,0:T(8,128)(2,1)S(1)} async-done(((bf16[16,24,2048]{2,1,0:T(8,128)(2,1)}), bf16[16,24,2048]{2,1,0:T(8,128)(2,1)S(1)}, u32[]{:S(2)}, u32[]{:S(2)}) %all-to-all-start) | async-done | bytes 1572896 | tf_op jit(solution)/shard_map/all_to_all | solution.py:320
  33.9 1.5 %units.1 = (bf16[384,192]{1,0:T(8,128)(2,1)S(1)}, bf16[16,2,104,128]{3,2,1,0:T(8,128)(2,1)S(1)}) custom-call(bf16[384,2048]{1,0:T(8,128)(2,1)S(1)} %bitcast.34, bf16[192,2048]{1,0:T(8,128)(2,1)S(1)} %constant_dynamic-update-slice_fusion.wall_ref, bf16[2,256,512]{2,1,0:T(8,128)(2,1)S(1)} %reshape.52.wret_ref), custom_call_target="tpu_custom_call" | custom-call | tf_op jit(solution)/shard_map/units/pallas_call | solution.py:146
  35.4 0.0 copy-start
  35.4 0.9 copy-done
  36.3 5.5 %all-to-all-start.1 = ((bf16[32,104,128]{2,1,0:T(8,128)(2,1)}), bf16[32,104,128]{2,1,0:T(8,128)(2,1)S(1)}, u32[]{:S(2)}, u32[]{:S(2)}) async-start(bf16[32,104,128]{2,1,0:T(8,128)(2,1)} %bitcast.37), calls=%async_computation.1 | async-start | bytes 1703936 | tf_op jit(solution)/shard_map/all_to_all | solution.py:330
  41.8 0.0 copy-start.2
  41.8 1.2 %wgrads.1 = (f32[3,32,2048]{2,1,0:T(8,128)S(1)}, f32[3,32,2048]{2,1,0:T(8,128)S(1)}) custom-call(bf16[384,192]{1,0:T(8,128)(2,1)S(1)} %get-tuple-element.22.grads_ref, bf16[384,2048]{1,0:T(8,128)(2,1)S(1)} %bitcast.35), custom_call_target="tpu_custom_call" | custom-call | tf_op jit(solution)/shard_map/wgrads/pallas_call | solution.py:173
  42.9 2.0 %collective-permute-start.3 = (f32[3,32,2048]{2,1,0:T(8,128)S(1)}, f32[3,32,2048]{2,1,0:T(8,128)S(1)}, u32[]{:S(2)}, u32[]{:S(2)}) collective-permute-start(f32[3,32,2048]{2,1,0:T(8,128)S(1)} %get-tuple-element.24), channel_id=1, source_target_pairs={{0,1},{1,0},{2,3},{3,2},{4,5},{5,4},{6,7},{7,6},{8,9},{9,8},{10,11... | collective-permute-start | bytes 2359304 | tf_op jit(solution)/shard_map/ppermute | solution.py:308
  45.0 2.1 %collective-permute-done.3.got_ref = f32[3,32,2048]{2,1,0:T(8,128)S(1)} collective-permute-done((f32[3,32,2048]{2,1,0:T(8,128)S(1)}, f32[3,32,2048]{2,1,0:T(8,128)S(1)}, u32[]{:S(2)}, u32[]{:S(2)}) %collective-permute-start.3) | collective-permute-done | bytes 786464 | tf_op jit(solution)/shard_map/ppermute | solution.py:308
  47.1 0.0 copy-start.1
  47.1 1.0 totals.1
  48.1 2.0 %collective-permute-start.4 = (f32[2,2048]{1,0:T(2,128)S(1)}, f32[2,2048]{1,0:T(2,128)S(1)}, u32[]{:S(2)}, u32[]{:S(2)}) collective-permute-start(f32[2,2048]{1,0:T(2,128)S(1)} %get-tuple-element.25.norms_ref), channel_id=1, source_target_pairs={{0,1},{1,0},{2,3},{3,2},{4,5},{5,4},{6,7},{7,6},{8,9},{9,8},{10,11... | collective-permute-start | bytes 49160 | tf_op jit(solution)/shard_map/ppermute | solution.py:308
  50.1 1.0 %collective-permute-done.4.got_ref = f32[2,2048]{1,0:T(2,128)S(1)} collective-permute-done((f32[2,2048]{1,0:T(2,128)S(1)}, f32[2,2048]{1,0:T(2,128)S(1)}, u32[]{:S(2)}, u32[]{:S(2)}) %collective-permute-start.4) | collective-permute-done | bytes 16416 | tf_op jit(solution)/shard_map/ppermute | solution.py:308
  51.1 4.6 %all-to-all-done.1 = bf16[32,104,128]{2,1,0:T(8,128)(2,1)S(1)} async-done(((bf16[32,104,128]{2,1,0:T(8,128)(2,1)}), bf16[32,104,128]{2,1,0:T(8,128)(2,1)S(1)}, u32[]{:S(2)}, u32[]{:S(2)}) %all-to-all-start.1) | async-done | bytes 852000 | tf_op jit(solution)/shard_map/all_to_all | solution.py:330
  55.8 0.0 copy-done.2
  55.8 0.6 combine.1
  56.3 42.0 %all_to_all.15.parts_ref = bf16[16,104,128]{2,1,0:T(8,128)(2,1)S(1)} all-to-all(bf16[16,104,128]{2,1,0:T(8,128)(2,1)S(1)} %combine.1), channel_id=1, replica_groups=mesh['ep'=16,'tp_0'=16,'tp_1'=2] {'tp_0'}, dimensions={0} | all-to-all | bytes 851968 | tf_op jit(solution)/shard_map/all_to_all | solution.py:336
  98.3 0.0 copy-done.1
  98.3 0.7 finish.1
  (6 shorter events, 0.1 us)
Async XLA Ops:
  4.4 9.5 %copy-start.3 = (bf16[1,2048,32]{1,2,0:T(8,128)(2,1)S(1)}, bf16[1,2048,32]{1,2,0:T(8,128)(2,1)}, u32[]{:S(2)}) copy-start(bf16[1,2048,32]{1,2,0:T(8,128)(2,1)} %param.11) | copy-start | bytes 393220
  4.4 11.4 %copy-start.4 = (bf16[1,2048,32]{1,2,0:T(8,128)(2,1)S(1)}, bf16[1,2048,32]{1,2,0:T(8,128)(2,1)}, u32[]{:S(2)}) copy-start(bf16[1,2048,32]{1,2,0:T(8,128)(2,1)} %param.12) | copy-start | bytes 393220
  4.4 13.9 %copy-start.5 = (bf16[1,32,2048]{2,1,0:T(8,128)(2,1)S(1)}, bf16[1,32,2048]{2,1,0:T(8,128)(2,1)}, u32[]{:S(2)}) copy-start(bf16[1,32,2048]{2,1,0:T(8,128)(2,1)} %param.13) | copy-start | bytes 393220
  4.4 29.5 %all-to-all-start = ((bf16[16,24,2048]{2,1,0:T(8,128)(2,1)}), bf16[16,24,2048]{2,1,0:T(8,128)(2,1)S(1)}, u32[]{:S(2)}, u32[]{:S(2)}) async-start(bf16[16,24,2048]{2,1,0:T(8,128)(2,1)} %bitcast.42), calls=%async_computation | async-start | bytes 3145728 | tf_op jit(solution)/shard_map/all_to_all | solution.py:320
  13.9 6.3 %collective-permute-start = (bf16[32,2048]{1,0:T(8,128)(2,1)S(1)}, bf16[32,2048]{1,0:T(8,128)(2,1)S(1)}, u32[]{:S(2)}, u32[]{:S(2)}) collective-permute-start(bf16[32,2048]{1,0:T(8,128)(2,1)S(1)} %bitcast.44), channel_id=1, source_target_pairs={{0,1},{1,0},{2,3},{3,2},{4,5},{5,4},{6,7},{7,6},{8,9},{9,8},{10,11... | collective-permute-start | bytes 393224 | tf_op jit(solution)/shard_map/ppermute | solution.py:308
  15.8 4.4 %collective-permute-start.1 = (bf16[32,2048]{1,0:T(8,128)(2,1)S(1)}, bf16[32,2048]{1,0:T(8,128)(2,1)S(1)}, u32[]{:S(2)}, u32[]{:S(2)}) collective-permute-start(bf16[32,2048]{1,0:T(8,128)(2,1)S(1)} %bitcast.46), channel_id=1, source_target_pairs={{0,1},{1,0},{2,3},{3,2},{4,5},{5,4},{6,7},{7,6},{8,9},{9,8},{10,11... | collective-permute-start | bytes 393224 | tf_op jit(solution)/shard_map/ppermute | solution.py:308
  18.3 5.8 %collective-permute-start.2 = (bf16[32,2048]{1,0:T(8,128)(2,1)S(1)}, bf16[32,2048]{1,0:T(8,128)(2,1)}, u32[]{:S(2)}, u32[]{:S(2)}) collective-permute-start(bf16[32,2048]{1,0:T(8,128)(2,1)S(1)} %bitcast.48), channel_id=1, source_target_pairs={{0,1},{1,0},{2,3},{3,2},{4,5},{5,4},{6,7},{7,6},{8,9},{9,8},{10,11... | collective-permute-start | bytes 393224 | tf_op jit(solution)/shard_map/ppermute | solution.py:308
  35.4 0.9 copy-start
  36.3 19.5 %all-to-all-start.1 = ((bf16[32,104,128]{2,1,0:T(8,128)(2,1)}), bf16[32,104,128]{2,1,0:T(8,128)(2,1)S(1)}, u32[]{:S(2)}, u32[]{:S(2)}) async-start(bf16[32,104,128]{2,1,0:T(8,128)(2,1)} %bitcast.37), calls=%async_computation.1 | async-start | bytes 1703936 | tf_op jit(solution)/shard_map/all_to_all | solution.py:330
  41.8 14.0 %copy-start.2 = (s32[128,2]{0,1:T(2,128)S(1)}, s32[128,2]{0,1:T(2,128)}, u32[]{:S(2)}) copy-start(s32[128,2]{0,1:T(2,128)} %param.8) | copy-start | bytes 3076
  42.9 4.2 %collective-permute-start.3 = (f32[3,32,2048]{2,1,0:T(8,128)S(1)}, f32[3,32,2048]{2,1,0:T(8,128)S(1)}, u32[]{:S(2)}, u32[]{:S(2)}) collective-permute-start(f32[3,32,2048]{2,1,0:T(8,128)S(1)} %get-tuple-element.24), channel_id=1, source_target_pairs={{0,1},{1,0},{2,3},{3,2},{4,5},{5,4},{6,7},{7,6},{8,9},{9,8},{10,11... | collective-permute-start | bytes 2359304 | tf_op jit(solution)/shard_map/ppermute | solution.py:308
  47.1 51.2 %copy-start.1 = (f32[128,2]{0,1:T(2,128)S(1)}, f32[128,2]{0,1:T(2,128)}, u32[]{:S(2)}) copy-start(f32[128,2]{0,1:T(2,128)} %param.9) | copy-start | bytes 3076
  48.1 3.1 %collective-permute-start.4 = (f32[2,2048]{1,0:T(2,128)S(1)}, f32[2,2048]{1,0:T(2,128)S(1)}, u32[]{:S(2)}, u32[]{:S(2)}) collective-permute-start(f32[2,2048]{1,0:T(2,128)S(1)} %get-tuple-element.25.norms_ref), channel_id=1, source_target_pairs={{0,1},{1,0},{2,3},{3,2},{4,5},{5,4},{6,7},{7,6},{8,9},{9,8},{10,11... | collective-permute-start | bytes 49160 | tf_op jit(solution)/shard_map/ppermute | solution.py:308

commit v3 on v2

--- a/solution.py
+++ b/solution.py
@@ -1,5 +1,3 @@
-import functools
-
 import jax
 import jax.numpy as jnp
 from jax import lax
@@ -30,6 +28,10 @@
 
 def iota(shape, dim):
     return lax.broadcasted_iota(jnp.int32, shape, dim)
+
+
+def block(j, side):
+    return pl.ds(pl.multiple_of((2 * j + side) * 128, 128), 128)
 
 
 def slot_keys(routes, experts):
@@ -50,9 +52,11 @@
     return jnp.where(mine, (first_slot + r - HALF * h).astype(f32), -2.0)
 
 
-def pack_kernel(core_ref, routes_ref, gates_ref, tok_ref, cot_ref, out_ref, pick_ref, scale_ref):
+def pack_kernel(place_ref, core_ref, routes_ref, gates_ref, tok_ref, cot_ref, out_ref, pick_ref, scale_ref):
     experts = out_ref.shape[0] // ROWS
-    tok, width = tok_ref.shape
+    tok = tok_ref.shape[0]
+    width = out_ref.shape[1]
+    side = place_ref[0]
     key, first = slot_keys(routes_ref[...], experts)
     gate = jnp.where(
         first,
@@ -72,40 +76,138 @@
         jnp.sum(picks * scales, axis=1, keepdims=True), scale_ref.shape
     )
     pick_ref[...] = picks.astype(bf16)
-    step = min(512, width)
-
-    @pl.loop(0, width // step)
+    wide = min(4, width // 128)
+
+    @pl.loop(0, width // (128 * wide))
     def _(n):
-        cols = pl.ds(pl.multiple_of(n * step, step), step)
-        both = jnp.concatenate([tok_ref[:, cols], cot_ref[:, cols]], axis=0)
+        both = jnp.concatenate(
+            [
+                jnp.concatenate([ref[:, block(n * wide + k, side)] for k in range(wide)], axis=1)
+                for ref in (tok_ref, cot_ref)
+            ],
+            axis=0,
+        )
         rows = jnp.dot(pick_ref[...], both, preferred_element_type=f32)
-        scale = jnp.concatenate([scale_ref[...]] * (step // 128), axis=1)
+        scale = jnp.concatenate([scale_ref[...]] * wide, axis=1)
+        cols = pl.ds(pl.multiple_of(n * 128 * wide, 128 * wide), 128 * wide)
         out_ref[:, cols] = (rows * scale).astype(bf16)
 
 
-def pack_rows(core, routes, gates, tokens, cotangent, experts):
+def pack_rows(place, core, routes, gates, tokens, cotangent, experts):
     tok, width = tokens.shape
     return pl.pallas_call(
         pack_kernel,
-        out_shape=jax.ShapeDtypeStruct((experts * ROWS, width), bf16),
-        in_specs=[SMEM, VMEM, VMEM, VMEM, VMEM],
+        out_shape=jax.ShapeDtypeStruct((experts * ROWS, width // 2), bf16),
+        in_specs=[SMEM, SMEM, VMEM, VMEM, VMEM, VMEM],
         out_specs=VMEM,
         scratch_shapes=[
             pltpu.VMEM((experts * ROWS, 2 * tok), bf16),
             pltpu.VMEM((experts * ROWS, 128), f32),
         ],
         name="pack_rows",
-    )(core, routes, gates, tokens, cotangent)
-
-
-def unit_kernel(rows_ref, wall_ref, wret_ref, grads_ref, msg_ref):
+    )(place, core, routes, gates, tokens, cotangent)
+
+
+def part_kernel(place_ref, glu_ref, lin_ref, down_ref, keep_ref, send_ref):
+    side = place_ref[0]
+    for k, ref in enumerate((glu_ref, lin_ref, down_ref)):
+        for j in range(keep_ref.shape[1] // 128):
+            cols = slice(128 * j, 128 * j + 128)
+            keep_ref[32 * k : 32 * k + 32, cols] = ref[:, block(j, side)]
+            send_ref[32 * k : 32 * k + 32, cols] = ref[:, block(j, 1 - side)]
+
+
+def part_weights(place, glu, lin, down):
+    shape = jax.ShapeDtypeStruct((96, glu.shape[1] // 2), bf16)
+    return pl.pallas_call(
+        part_kernel,
+        out_shape=(shape, shape),
+        in_specs=[SMEM, VMEM, VMEM, VMEM],
+        out_specs=(VMEM,) * 2,
+        compiler_params=pltpu.CompilerParams(vmem_limit_bytes=LIMIT),
+        name="part_weights",
+    )(place, glu, lin, down)
+
+
+def gather_kernel(place_ref, keep_ref, side_ref, core_ref, cross_ref, wall_ref, wret_ref):
+    def fill(order):
+        for k in range(3):
+            for n, ref in enumerate(order):
+                at = 128 * k + 32 * n
+                wall_ref[at : at + 32, :] = ref[32 * k : 32 * k + 32, :]
+
+    @pl.when(place_ref[0] == 0)
+    def _():
+        fill((keep_ref, side_ref, core_ref, cross_ref))
+
+    @pl.when(place_ref[0] == 1)
+    def _():
+        fill((side_ref, keep_ref, cross_ref, core_ref))
+
+    half = wall_ref.shape[1] // 2
+    low = iota((256, 128), 1) < 64
+    for h in range(2):
+        for q in range(half // 256):
+            at = h * half + q * 256
+            one = wall_ref[0:256, at : at + 128].astype(f32)
+            two = wall_ref[0:256, at + 128 : at + 256].astype(f32)
+            even = jnp.where(low, one, pltpu.roll(two, 64, 1))
+            odd = jnp.where(low, pltpu.roll(one, 64, 1), two)
+            cols = slice(128 * q, 128 * q + 128)
+            wret_ref[0, 256 * h : 256 * h + 256, cols] = even.astype(bf16)
+            wret_ref[1, 256 * h : 256 * h + 256, cols] = odd.astype(bf16)
+
+
+def gather_weights(place, keep, side, core, cross):
+    width = keep.shape[1]
+    return pl.pallas_call(
+        gather_kernel,
+        out_shape=(
+            jax.ShapeDtypeStruct((384, width), bf16),
+            jax.ShapeDtypeStruct((2, 512, width // 4), bf16),
+        ),
+        in_specs=[SMEM] + [VMEM] * 4,
+        out_specs=(VMEM,) * 2,
+        compiler_params=pltpu.CompilerParams(vmem_limit_bytes=LIMIT),
+        name="gather_weights",
+    )(place, keep, side, core, cross)
+
+
+def pre_kernel(rows_ref, wall_ref, out_ref):
     count = rows_ref.shape[0]
+    pre = nt(rows_ref[...], wall_ref[...])
+    upper = lax.rem(iota((count, 128), 0), ROWS) < HALF
+    out_ref[0:count, :] = jnp.where(upper, pre[:, :128], pre[:, 256:])
+    lin = pre[:, 128:256].reshape(count // (2 * ROWS), 2, ROWS, 128)
+    moved = jnp.roll(pre[:, 128:256], HALF, axis=0).reshape(lin.shape)
+    top = iota((count // (2 * ROWS), ROWS, 128), 1) < HALF
+    out_ref[count:, :] = jnp.where(top, lin[:, 0], moved[:, 1]).reshape(count // 2, 128)
+
+
+def pre_parts(rows, wall):
+    count = rows.shape[0]
+    return pl.pallas_call(
+        pre_kernel,
+        out_shape=jax.ShapeDtypeStruct((count + count // 2, 128), f32),
+        in_specs=[VMEM, VMEM],
+        out_specs=VMEM,
+        compiler_params=pltpu.CompilerParams(vmem_limit_bytes=LIMIT),
+        name="pre_parts",
+    )(rows, wall)
+
+
+def unit_kernel(mine_ref, got_ref, wret_ref, grads_ref, msg_ref):
+    count = grads_ref.shape[0]
     sources = count // ROWS
-    units = wall_ref.shape[0] // 3
-    pre = nt(rows_ref[...], wall_ref[...])
-    glu_pre = pre[:, :units]
-    lin_pre = pre[:, units : 2 * units]
-    hid_grad = jnp.roll(pre[:, 2 * units :], -HALF, axis=0)
+    units = 128
+    glu_pre = mine_ref[0:count, :] + got_ref[0:count, :]
+    hid_grad = jnp.roll(glu_pre, -HALF, axis=0)
+    lin = mine_ref[count:, :] + got_ref[count:, :]
+    moved = jnp.roll(lin, -HALF, axis=0)
+    lin_pre = jnp.concatenate(
+        [lin.reshape(sources // 2, 1, ROWS, units), moved.reshape(sources // 2, 1, ROWS, units)],
+        axis=1,
+    ).reshape(count, units)
     keep = lax.rem(iota((count, units), 0), ROWS) < HALF
     glu_clip = jnp.minimum(glu_pre, clamp_limit)
     lin_clip = jnp.clip(lin_pre, -clamp_limit, clamp_limit)
@@ -140,80 +242,106 @@
         msg_ref[:, core, blocks * ROWS :, :] = tail
 
 
-def units(rows, wall, wret):
-    count = rows.shape[0]
+def units(mine, got, wret):
+    count = mine.shape[0] // 3 * 2
     height = wret.shape[2] // 128 * ROWS + 8
     return pl.pallas_call(
         unit_kernel,
         out_shape=(
-            jax.ShapeDtypeStruct((count, wall.shape[0]), bf16),
+            jax.ShapeDtypeStruct((count, 384), bf16),
             jax.ShapeDtypeStruct((count // ROWS, 2, height, 128), bf16),
         ),
         in_specs=[VMEM, VMEM, VMEM],
         out_specs=(VMEM, VMEM),
         compiler_params=pltpu.CompilerParams(vmem_limit_bytes=LIMIT),
         name="units",
-    )(rows, wall, wret)
-
-
-def wgrad_kernel(grads_ref, rows_ref, own_ref, other_ref):
+    )(mine, got, wret)
+
+
+def wgrad_kernel(grads_ref, rows_ref, part_ref, down_ref):
     step = min(512, rows_ref.shape[1])
 
     @pl.loop(0, rows_ref.shape[1] // step)
     def _(n):
         cols = pl.ds(pl.multiple_of(n * step, step), step)
         part = tn(grads_ref[...], rows_ref[:, cols])
-        for k in range(3):
-            own_ref[k, :, cols] = part[64 * k : 64 * k + 32, :]
-            other_ref[k, :, cols] = part[64 * k + 32 : 64 * k + 64, :]
+        for k in range(4):
+            part_ref[k, :, cols] = part[64 * k : 64 * k + 64, :]
+        down_ref[:, cols] = part[256:320, :]
+        part_ref[4, :, cols] = part[320:384, :]
 
 
 def wgrads(grads, rows):
-    shape = jax.ShapeDtypeStruct((3, 32, rows.shape[1]), f32)
+    width = rows.shape[1]
     return pl.pallas_call(
         wgrad_kernel,
-        out_shape=(shape, shape),
+        out_shape=(
+            jax.ShapeDtypeStruct((5, 64, width), f32),
+            jax.ShapeDtypeStruct((64, width), f32),
+        ),
         in_specs=[VMEM, VMEM],
-        out_specs=(VMEM, VMEM),
+        out_specs=(VMEM,) * 2,
         compiler_params=pltpu.CompilerParams(vmem_limit_bytes=LIMIT),
         name="wgrads",
     )(grads, rows)
 
 
-def total_kernel(own_ref, got_ref, glu_ref, lin_ref, down_ref, norms_ref, down_norms_ref):
-    glu = own_ref[0] + got_ref[0]
-    lin = own_ref[1] + got_ref[1]
-    down = own_ref[2] + got_ref[2]
-    glu_ref[...] = glu
-    lin_ref[...] = lin
-    down_ref[...] = down
-    norms_ref[0:1, :] = jnp.sum(glu * glu, axis=0, keepdims=True)
-    norms_ref[1:2, :] = jnp.sum(lin * lin, axis=0, keepdims=True)
-    each = jnp.sum(down * down, axis=1, keepdims=True)
-    spread = jnp.where(iota((32, 128), 0) == iota((32, 128), 1), each, 0.0)
-    down_norms_ref[...] = jnp.sum(spread, axis=0, keepdims=True)
-
-
-def totals(own, got):
+def total_kernel(place_ref, own_ref, down_ref, got_ref, keep_ref, send_ref, norms_ref):
+    side = place_ref[0]
+    for k in range(3):
+        if k < 2:
+            mine = own_ref[2 * k] + got_ref[2 * k + 1]
+            other = own_ref[2 * k + 1] + got_ref[2 * k]
+            norms_ref[k : k + 1, :] = jnp.sum(mine * mine + other * other, axis=0, keepdims=True)
+        else:
+            mine = down_ref[...] + got_ref[4]
+        low, high = mine[:32, :], mine[32:, :]
+        keep_ref[k] = jnp.where(side == 0, low, high)
+        send_ref[k] = jnp.where(side == 0, high, low).astype(bf16)
+
+
+def totals(place, own, down, got):
     width = own.shape[2]
-    shape = jax.ShapeDtypeStruct((32, width), f32)
     return pl.pallas_call(
         total_kernel,
         out_shape=(
-            shape,
-            shape,
-            shape,
+            jax.ShapeDtypeStruct((3, 32, width), f32),
+            jax.ShapeDtypeStruct((3, 32, width), bf16),
             jax.ShapeDtypeStruct((2, width), f32),
-            jax.ShapeDtypeStruct((1, 128), f32),
-        ),
-        in_specs=[VMEM, VMEM],
-        out_specs=(VMEM,) * 5,
+        ),
+        in_specs=[SMEM, VMEM, VMEM, VMEM],
+        out_specs=(VMEM,) * 3,
         compiler_params=pltpu.CompilerParams(vmem_limit_bytes=LIMIT),
         name="totals",
-    )(own, got)
-
-
-def combine_kernel(routes_ref, back_ref, norms_ref, got_ref, msg_ref):
+    )(place, own, down, got)
+
+
+def place_kernel(place_ref, own_ref, got_ref, glu_ref, lin_ref, down_ref, norms_ref):
+    side = place_ref[0]
+    for k, ref in enumerate((glu_ref, lin_ref, down_ref)):
+        for j in range(own_ref.shape[2] // 128):
+            cols = slice(128 * j, 128 * j + 128)
+            ref[:, block(j, side)] = own_ref[k, :, cols]
+            ref[:, block(j, 1 - side)] = got_ref[k, :, cols].astype(f32)
+    down, got = own_ref[2], got_ref[2].astype(f32)
+    each = jnp.sum(down * down + got * got, axis=1, keepdims=True)
+    spread = jnp.where(iota((32, 128), 0) == iota((32, 128), 1), each, 0.0)
+    norms_ref[...] = jnp.sum(spread, axis=0, keepdims=True)
+
+
+def place_grads(place, own, got):
+    shape = jax.ShapeDtypeStruct((32, 2 * own.shape[2]), f32)
+    return pl.pallas_call(
+        place_kernel,
+        out_shape=(shape, shape, shape, jax.ShapeDtypeStruct((1, 128), f32)),
+        in_specs=[SMEM] + [VMEM] * 2,
+        out_specs=(VMEM,) * 4,
+        compiler_params=pltpu.CompilerParams(vmem_limit_bytes=LIMIT),
+        name="place_grads",
+    )(place, own, got)
+
+
+def combine_kernel(place_ref, routes_ref, back_ref, norms_ref, got_ref, msg_ref):
     experts = back_ref.shape[0]
     height = back_ref.shape[2]
     blocks = (height - 8) // ROWS
@@ -255,26 +383,30 @@
     gate_rows = jnp.where(row == 0, high_first, jnp.where(row == 1, high_second, 0.0))
     gate_rows = jnp.where(row == 2, named_first - high_first, gate_rows)
     gate_rows = jnp.where(row == 3, named_second - high_second, gate_rows)
-    normed = norms_ref[...] + got_ref[...]
-    count = normed.shape[1] // 128
-    lines = jnp.concatenate(
-        [normed[k : k + 1, n * 128 : (n + 1) * 128] for k in range(2) for n in range(count)], axis=0
-    )
+    count = norms_ref.shape[1] // 128
+    lines = []
+    for k in range(2):
+        for n in range(count):
+            own = norms_ref[k : k + 1, n * 128 : (n + 1) * 128]
+            got = got_ref[k : k + 1, n * 128 : (n + 1) * 128]
+            lines.append(jnp.where(place_ref[0] == 0, own, got))
+            lines.append(jnp.where(place_ref[0] == 0, got, own))
+    lines = jnp.concatenate(lines, axis=0)
     extra = jnp.concatenate([lines, gate_rows], axis=0).astype(bf16)
     for z in range(depth):
         msg_ref[z, 64:, :] = extra
 
 
-def combine(routes, back, norms, got, depth):
-    height = 64 + 2 * norms.shape[1] // 128 + 8
+def combine(place, routes, back, norms, got, depth):
+    height = 64 + 4 * norms.shape[1] // 128 + 8
     return pl.pallas_call(
         combine_kernel,
         out_shape=jax.ShapeDtypeStruct((depth, height, 128), bf16),
-        in_specs=[VMEM] * 4,
+        in_specs=[SMEM] + [VMEM] * 4,
         out_specs=VMEM,
         compiler_params=pltpu.CompilerParams(vmem_limit_bytes=LIMIT),
         name="combine",
-    )(routes, back, norms, got)
+    )(place, routes, back, norms, got)
 
 
 def finish_kernel(parts_ref, gates_ref, tok_ref, gate_ref, glu_ref, lin_ref):
@@ -304,36 +436,44 @@
     )(parts, gates)
 
 
-def swap(x):
-    return lax.ppermute(x, "tp_1", [(0, 1), (1, 0)])
-
-
-def shards(tokens, routes, gates, cotangent, w_glu, w_lin, w_down):
+def over_side(x):
+    return lax.ppermute(x, "side", [(0, 1), (1, 0)])
+
+
+def over_core(x):
+    return lax.ppermute(x, "core", [(0, 1), (1, 0)])
+
+
+def layer(tokens, routes, gates, cotangent, w_glu, w_lin, w_down):
     experts = lax.axis_size("ep")
-    depth = lax.axis_size("tp_0")
-    tok, width = tokens.shape
-    core = lax.axis_index("tp_1").astype(jnp.int32).reshape(1)
+    depth = lax.axis_size("team")
+    _, width = tokens.shape
+    place = lax.axis_index("side").astype(jnp.int32).reshape(1)
+    core = lax.axis_index("core").astype(jnp.int32).reshape(1)
     routes_t, gates_t = routes.T, gates.T
-    glu_t, lin_t, down = w_glu[0].T, w_lin[0].T, w_down[0]
-
-    packed = pack_rows(core, routes_t, gates_t, tokens, cotangent, experts)
-    rows = lax.all_to_all(packed.reshape(experts, ROWS, width), "ep", 0, 0, tiled=True)
-    rows = rows.reshape(experts * ROWS, width)
-
-    glu_o, lin_o, down_o = swap(glu_t), swap(lin_t), swap(down)
-    wall = jnp.concatenate([glu_t, glu_o, lin_t, lin_o, down, down_o], axis=0)
-    inner = wall[:128].reshape(128, 2, depth // 2, 2, 64)
-    wret = inner.transpose(3, 1, 0, 2, 4).reshape(2, 256, width // 4)
-
-    grads, msg = units(rows, wall, wret)
+
+    packed = pack_rows(place, core, routes_t, gates_t, tokens, cotangent, experts)
+    rows = lax.all_to_all(packed.reshape(experts, ROWS, width // 2), "ep", 0, 0, tiled=True)
+    rows = rows.reshape(experts * ROWS, width // 2)
+
+    keep, send = part_weights(place, w_glu[0].T, w_lin[0].T, w_down[0])
+    got = over_side(send)
+    wall, wret = gather_weights(place, keep, got, over_core(keep), over_core(got))
+
+    mine = pre_parts(rows, wall)
+    grads, msg = units(mine, over_side(mine), wret)
     msg = msg.reshape(experts * 2, *msg.shape[2:])
-    back = lax.all_to_all(msg, ("ep", "tp_1"), 0, 0, tiled=True)
+    back = lax.all_to_all(msg, ("ep", "core"), 0, 0, tiled=True)
     back = back.reshape(experts, 2, *msg.shape[1:])
 
-    own, other = wgrads(grads, rows)
-    glu_wg, lin_wg, down_wg, norms, down_norms = totals(own, swap(other))
-    msg = combine(routes_t, back, norms, swap(norms), depth)
-    parts = lax.all_to_all(msg, "tp_0", 0, 0, tiled=True)
+    part, down = wgrads(grads, rows)
+    own, other, norms = totals(place, part, down, over_core(part))
+    norms_got = over_side(norms)
+    msg = combine(place, routes_t, back, norms, norms_got, depth)
+    parts = lax.all_to_all(msg, "team", 0, 0, tiled=True)
+    other, msg = lax.optimization_barrier((other, msg))
+    got = over_side(other)
+    glu_wg, lin_wg, down_wg, down_norms = place_grads(place, own, got)
     tok_t, gate_t, glu_norms, lin_norms = finish(parts, gates_t)
     return (
         tok_t.T,
@@ -348,11 +488,13 @@
 
 
 def solution(mesh):
-    depth = mesh.shape["tp"] // 2
-    split = Mesh(mesh.devices.reshape(mesh.shape["ep"], depth, 2), ("ep", "tp_0", "tp_1"))
-    tp = ("tp_0", "tp_1")
+    teams = mesh.shape["tp"] // 4
+    split = Mesh(
+        mesh.devices.reshape(mesh.shape["ep"], teams, 2, 2), ("ep", "team", "side", "core")
+    )
+    tp = ("team", "side", "core")
     return jax.shard_map(
-        shards,
+        layer,
         mesh=split,
         in_specs=(
             P("ep", None),

time: 99.5 us -> 94.6 us (0.951)
  the two profiles are of different devices: /device:TPU:2 before, /device:TPU:32 now
where the time goes in v3:
time: 94.6 us; the launch traced here: 93.9 us
  starting transfers between devices  46.1 us (49%)
  waiting for transfers between devices  34.8 us (37%)
  Pallas kernels  8.28 us (9%)
  local copies, waits for them, and re-layouts  3.86 us (4%)
    ppermute x4, waiting for transfers between devices, over_side(): return lax.ppermute(x, 'side', [(0, 1), (1, 0)])  21.9 us
    all_to_all x1, starting transfers between devices, layer(): parts = lax.all_to_all(msg, 'team', 0, 0, tiled=True)  14.2 us
    ppermute x4, starting transfers between devices, over_side(): return lax.ppermute(x, 'side', [(0, 1), (1, 0)])  12.4 us
    all_to_all x1, starting transfers between devices, layer(): lax.all_to_all(packed.reshape(experts, ROWS, width // 2), 'ep', 0, 0, til...  7.04 us
    all_to_all x1, starting transfers between devices, layer(): back = lax.all_to_all(msg, ('ep', 'core'), 0, 0, tiled=True)  6.71 us
    ppermute x3, starting transfers between devices, over_core(): return lax.ppermute(x, 'core', [(0, 1), (1, 0)])  5.74 us
    all_to_all x1, waiting for transfers between devices, layer(): back = lax.all_to_all(msg, ('ep', 'core'), 0, 0, tiled=True)  4.61 us
    all_to_all x1, waiting for transfers between devices, layer(): parts = lax.all_to_all(msg, 'team', 0, 0, tiled=True)  4.43 us
  transfers between devices with their start and end apart: 10, of which 7 were waited for; matrix products, arithmetic and copies ran while one was open for 0% of the time, Pallas kernels for 2%

profile of v3, /device:TPU:32, one launch (start us, length us, event | category | flops | bytes accessed | tf_op | source)
XLA Modules:
  0.0 93.9 jit_solution(11709886415399136180)
XLA Ops:
  0.6 0.0 copy-start.5
  0.7 0.0 copy-start.6
  0.7 0.0 copy-start.7
  0.7 3.1 %pack_rows.1 = bf16[384,1024]{1,0:T(8,128)(2,1)} custom-call(s32[1]{0:T(128)} %bitcast.place_ref, s32[1]{0:T(128)} %bitcast.2.core_ref, s32[2,128]{1,0:T(2,128)} %bitcast.34, f32[2,128]{1,0:T(2,128)} %bitcast.36, bf16[128,2048]{1,0:T(8,128)(2,1)} %tok_ref.1, bf16[128,2048]{1,0:T(8,128)(2,1)} %cot_ref.1), custom_call_target="tpu_custom_call" | custom-call | tf_op jit(solution)/shard_map/pack_rows/pallas_call | solution.py:98
  3.7 7.0 %all-to-all-start = ((bf16[16,24,1024]{2,1,0:T(8,128)(2,1)}), bf16[16,24,1024]{2,1,0:T(8,128)(2,1)S(1)}, u32[]{:S(2)}, u32[]{:S(2)}) async-start(bf16[16,24,1024]{2,1,0:T(8,128)(2,1)} %bitcast.38), calls=%async_computation | async-start | bytes 1572864 | tf_op jit(solution)/shard_map/all_to_all | solution.py:456
  10.8 0.0 copy-done.5
  10.8 0.0 copy-done.6
  10.8 0.0 copy-done.7
  10.8 0.1 part_weights.1
  10.9 4.0 %collective-permute-start = (bf16[96,1024]{1,0:T(8,128)(2,1)S(1)}, bf16[96,1024]{1,0:T(8,128)(2,1)S(1)}, u32[]{:S(2)}, u32[]{:S(2)}) collective-permute-start(bf16[96,1024]{1,0:T(8,128)(2,1)S(1)} %get-tuple-element.29), channel_id=1, source_target_pairs={{0,2},{2,0},{1,3},{3,1},{4,6},{6,4},{5,7},{7,5},{8,10},{10,8},{9,1... | collective-permute-start | bytes 589832 | tf_op jit(solution)/shard_map/ppermute | solution.py:440
  14.9 1.9 %collective-permute-start.1 = (bf16[96,1024]{1,0:T(8,128)(2,1)S(1)}, bf16[96,1024]{1,0:T(8,128)(2,1)S(1)}, u32[]{:S(2)}, u32[]{:S(2)}) collective-permute-start(bf16[96,1024]{1,0:T(8,128)(2,1)S(1)} %get-tuple-element.28.keep_ref), channel_id=1, source_target_pairs={{0,1},{1,0},{2,3},{3,2},{4,5},{5,4},{6,7},{7,6},{8,9},{9,8},{10,11... | collective-permute-start | bytes 589832 | tf_op jit(solution)/shard_map/ppermute | solution.py:444
  16.8 2.4 %collective-permute-done.side_ref = bf16[96,1024]{1,0:T(8,128)(2,1)S(1)} collective-permute-done((bf16[96,1024]{1,0:T(8,128)(2,1)S(1)}, bf16[96,1024]{1,0:T(8,128)(2,1)S(1)}, u32[]{:S(2)}, u32[]{:S(2)}) %collective-permute-start) | collective-permute-done | bytes 196640 | tf_op jit(solution)/shard_map/ppermute | solution.py:440
  19.2 1.9 %collective-permute-start.2 = (bf16[96,1024]{1,0:T(8,128)(2,1)S(1)}, bf16[96,1024]{1,0:T(8,128)(2,1)S(1)}, u32[]{:S(2)}, u32[]{:S(2)}) collective-permute-start(bf16[96,1024]{1,0:T(8,128)(2,1)S(1)} %collective-permute-done.side_ref), channel_id=1, source_target_pairs={{0,1},{1,0},{2,3},{3,2},{4,5},{5,4},{6,7},{7,6},{8,9},{9,8},{10,11... | collective-permute-start | bytes 589832 | tf_op jit(solution)/shard_map/ppermute | solution.py:444
  21.1 0.0 collective-permute-done.1.core_ref
  21.1 1.4 %collective-permute-done.2.cross_ref = bf16[96,1024]{1,0:T(8,128)(2,1)S(1)} collective-permute-done((bf16[96,1024]{1,0:T(8,128)(2,1)S(1)}, bf16[96,1024]{1,0:T(8,128)(2,1)S(1)}, u32[]{:S(2)}, u32[]{:S(2)}) %collective-permute-start.2) | collective-permute-done | bytes 196640 | tf_op jit(solution)/shard_map/ppermute | solution.py:444
  22.5 0.3 gather_weights.1
  22.8 2.5 %all-to-all-done = bf16[16,24,1024]{2,1,0:T(8,128)(2,1)S(1)} async-done(((bf16[16,24,1024]{2,1,0:T(8,128)(2,1)}), bf16[16,24,1024]{2,1,0:T(8,128)(2,1)S(1)}, u32[]{:S(2)}, u32[]{:S(2)}) %all-to-all-start) | async-done | bytes 786464 | tf_op jit(solution)/shard_map/all_to_all | solution.py:456
  25.3 0.6 pre_parts.1.mine_ref
  25.9 2.0 %collective-permute-start.3 = (f32[576,128]{1,0:T(8,128)S(1)}, f32[576,128]{1,0:T(8,128)S(1)}, u32[]{:S(2)}, u32[]{:S(2)}) collective-permute-start(f32[576,128]{1,0:T(8,128)S(1)} %pre_parts.1.mine_ref), channel_id=1, source_target_pairs={{0,2},{2,0},{1,3},{3,1},{4,6},{6,4},{5,7},{7,5},{8,10},{10,8},{9,1... | collective-permute-start | bytes 884744 | tf_op jit(solution)/shard_map/ppermute | solution.py:440
  27.8 7.1 %collective-permute-done.3.got_ref = f32[576,128]{1,0:T(8,128)S(1)} collective-permute-done((f32[576,128]{1,0:T(8,128)S(1)}, f32[576,128]{1,0:T(8,128)S(1)}, u32[]{:S(2)}, u32[]{:S(2)}) %collective-permute-start.3) | collective-permute-done | bytes 294944 | tf_op jit(solution)/shard_map/ppermute | solution.py:440
  35.0 0.5 units.1
  35.5 0.0 copy-start
  35.5 0.8 copy-done
  36.2 0.8 wgrads.1
  37.0 0.0 copy-start.3
  37.0 0.7 copy-done.3
  37.7 1.9 %collective-permute-start.4 = (f32[5,64,1024]{2,1,0:T(8,128)S(1)}, f32[5,64,1024]{2,1,0:T(8,128)S(1)}, u32[]{:S(2)}, u32[]{:S(2)}) collective-permute-start(f32[5,64,1024]{2,1,0:T(8,128)S(1)} %get-tuple-element.34.own_ref), channel_id=1, source_target_pairs={{0,1},{1,0},{2,3},{3,2},{4,5},{5,4},{6,7},{7,6},{8,9},{9,8},{10,11... | collective-permute-start | bytes 3932168 | tf_op jit(solution)/shard_map/ppermute | solution.py:444
  39.7 6.7 %all-to-all-start.1 = ((bf16[32,56,128]{2,1,0:T(8,128)(2,1)}), bf16[32,56,128]{2,1,0:T(8,128)(2,1)S(1)}, u32[]{:S(2)}, u32[]{:S(2)}) async-start(bf16[32,56,128]{2,1,0:T(8,128)(2,1)} %bitcast.30), calls=%async_computation.1 | async-start | bytes 917504 | tf_op jit(solution)/shard_map/all_to_all | solution.py:466
  46.4 0.0 collective-permute-done.4.got_ref
  46.4 0.0 copy-start.4
  46.4 0.9 %copy-done.4 = f32[64,1024]{1,0:T(8,128)S(1)} copy-done((f32[64,1024]{1,0:T(8,128)S(1)}, f32[64,1024]{1,0:T(8,128)}, u32[]{:S(2)}) %copy-start.4) | copy-done | bytes 262168
  47.3 0.3 totals.1
  47.6 0.0 copy-start.1
  47.6 0.8 copy-done.1
  48.4 0.7 copy-done.10
  49.0 3.6 %collective-permute-start.5 = (f32[2,1024]{1,0:T(2,128)S(1)}, f32[2,1024]{1,0:T(2,128)S(1)}, u32[]{:S(2)}, u32[]{:S(2)}) collective-permute-start(f32[2,1024]{1,0:T(2,128)S(1)} %get-tuple-element.36.norms_ref), channel_id=1, source_target_pairs={{0,2},{2,0},{1,3},{3,1},{4,6},{6,4},{5,7},{7,5},{8,10},{10,8},{9,1... | collective-permute-start | bytes 24584 | tf_op jit(solution)/shard_map/ppermute | solution.py:440
  52.7 4.6 %all-to-all-done.1 = bf16[32,56,128]{2,1,0:T(8,128)(2,1)S(1)} async-done(((bf16[32,56,128]{2,1,0:T(8,128)(2,1)}), bf16[32,56,128]{2,1,0:T(8,128)(2,1)S(1)}, u32[]{:S(2)}, u32[]{:S(2)}) %all-to-all-start.1) | async-done | bytes 458784 | tf_op jit(solution)/shard_map/all_to_all | solution.py:466
  57.3 0.0 collective-permute-done.5.got_ref
  57.3 0.0 copy-done.8
  57.3 1.1 %combine.1 = bf16[8,104,128]{2,1,0:T(8,128)(2,1)} custom-call(s32[1]{0:T(128)} %bitcast.place_ref, s32[2,128]{1,0:T(2,128)S(1)} %bitcast.35, bf16[16,2,56,128]{3,2,1,0:T(8,128)(2,1)S(1)} %bitcast.29, f32[2,1024]{1,0:T(2,128)S(1)} %get-tuple-element.36.norms_ref, f32[2,1024]{1,0:T(2,128)S(1)} %collective-permute-done.5.got_ref), custom_call_target="tpu_custom_call" | custom-call | tf_op jit(solution)/shard_map/combine/pallas_call | solution.py:402
  58.4 14.2 %all-to-all-start.2 = ((bf16[8,104,128]{2,1,0:T(8,128)(2,1)}), bf16[8,104,128]{2,1,0:T(8,128)(2,1)S(1)}, u32[]{:S(2)}, u32[]{:S(2)}) async-start(bf16[8,104,128]{2,1,0:T(8,128)(2,1)} %combine.1), calls=%async_computation.2 | async-start | bytes 425984 | tf_op jit(solution)/shard_map/all_to_all | solution.py:473
  72.6 2.9 %collective-permute-start.6 = (bf16[3,32,1024]{2,1,0:T(8,128)(2,1)}, bf16[3,32,1024]{2,1,0:T(8,128)(2,1)S(1)}, u32[]{:S(2)}, u32[]{:S(2)}) collective-permute-start(bf16[3,32,1024]{2,1,0:T(8,128)(2,1)} %copy-done.10), channel_id=1, source_target_pairs={{0,2},{2,0},{1,3},{3,1},{4,6},{6,4},{5,7},{7,5},{8,10},{10,8},{9,1... | collective-permute-start | bytes 589832 | tf_op jit(solution)/shard_map/ppermute | solution.py:440
  75.5 12.4 %collective-permute-done.6.got_ref = bf16[3,32,1024]{2,1,0:T(8,128)(2,1)S(1)} collective-permute-done((bf16[3,32,1024]{2,1,0:T(8,128)(2,1)}, bf16[3,32,1024]{2,1,0:T(8,128)(2,1)S(1)}, u32[]{:S(2)}, u32[]{:S(2)}) %collective-permute-start.6) | collective-permute-done | bytes 196640 | tf_op jit(solution)/shard_map/ppermute | solution.py:440
  87.9 0.0 copy-done.2
  88.0 0.9 place_grads.1
  88.9 4.4 %all-to-all-done.2.parts_ref = bf16[8,104,128]{2,1,0:T(8,128)(2,1)S(1)} async-done(((bf16[8,104,128]{2,1,0:T(8,128)(2,1)}), bf16[8,104,128]{2,1,0:T(8,128)(2,1)S(1)}, u32[]{:S(2)}, u32[]{:S(2)}) %all-to-all-start.2) | async-done | bytes 213024 | tf_op jit(solution)/shard_map/all_to_all | solution.py:473
  93.3 0.0 copy-done.9
  93.3 0.6 finish.1
  (4 shorter events, 0.0 us)
Async XLA Ops:
  0.6 10.1 %copy-start.5 = (bf16[1,2048,32]{1,2,0:T(8,128)(2,1)S(1)}, bf16[1,2048,32]{1,2,0:T(8,128)(2,1)}, u32[]{:S(2)}) copy-start(bf16[1,2048,32]{1,2,0:T(8,128)(2,1)} %param.11) | copy-start | bytes 393220
  0.7 10.1 %copy-start.6 = (bf16[1,2048,32]{1,2,0:T(8,128)(2,1)S(1)}, bf16[1,2048,32]{1,2,0:T(8,128)(2,1)}, u32[]{:S(2)}) copy-start(bf16[1,2048,32]{1,2,0:T(8,128)(2,1)} %param.12) | copy-start | bytes 393220
  0.7 10.1 %copy-start.7 = (bf16[1,32,2048]{2,1,0:T(8,128)(2,1)S(1)}, bf16[1,32,2048]{2,1,0:T(8,128)(2,1)}, u32[]{:S(2)}) copy-start(bf16[1,32,2048]{2,1,0:T(8,128)(2,1)} %param.13) | copy-start | bytes 393220
  3.7 21.6 %all-to-all-start = ((bf16[16,24,1024]{2,1,0:T(8,128)(2,1)}), bf16[16,24,1024]{2,1,0:T(8,128)(2,1)S(1)}, u32[]{:S(2)}, u32[]{:S(2)}) async-start(bf16[16,24,1024]{2,1,0:T(8,128)(2,1)} %bitcast.38), calls=%async_computation | async-start | bytes 1572864 | tf_op jit(solution)/shard_map/all_to_all | solution.py:456
  10.9 8.3 %collective-permute-start = (bf16[96,1024]{1,0:T(8,128)(2,1)S(1)}, bf16[96,1024]{1,0:T(8,128)(2,1)S(1)}, u32[]{:S(2)}, u32[]{:S(2)}) collective-permute-start(bf16[96,1024]{1,0:T(8,128)(2,1)S(1)} %get-tuple-element.29), channel_id=1, source_target_pairs={{0,2},{2,0},{1,3},{3,1},{4,6},{6,4},{5,7},{7,5},{8,10},{10,8},{9,1... | collective-permute-start | bytes 589832 | tf_op jit(solution)/shard_map/ppermute | solution.py:440
  14.9 6.2 %collective-permute-start.1 = (bf16[96,1024]{1,0:T(8,128)(2,1)S(1)}, bf16[96,1024]{1,0:T(8,128)(2,1)S(1)}, u32[]{:S(2)}, u32[]{:S(2)}) collective-permute-start(bf16[96,1024]{1,0:T(8,128)(2,1)S(1)} %get-tuple-element.28.keep_ref), channel_id=1, source_target_pairs={{0,1},{1,0},{2,3},{3,2},{4,5},{5,4},{6,7},{7,6},{8,9},{9,8},{10,11... | collective-permute-start | bytes 589832 | tf_op jit(solution)/shard_map/ppermute | solution.py:444
  19.2 3.3 %collective-permute-start.2 = (bf16[96,1024]{1,0:T(8,128)(2,1)S(1)}, bf16[96,1024]{1,0:T(8,128)(2,1)S(1)}, u32[]{:S(2)}, u32[]{:S(2)}) collective-permute-start(bf16[96,1024]{1,0:T(8,128)(2,1)S(1)} %collective-permute-done.side_ref), channel_id=1, source_target_pairs={{0,1},{1,0},{2,3},{3,2},{4,5},{5,4},{6,7},{7,6},{8,9},{9,8},{10,11... | collective-permute-start | bytes 589832 | tf_op jit(solution)/shard_map/ppermute | solution.py:444
  25.9 9.1 %collective-permute-start.3 = (f32[576,128]{1,0:T(8,128)S(1)}, f32[576,128]{1,0:T(8,128)S(1)}, u32[]{:S(2)}, u32[]{:S(2)}) collective-permute-start(f32[576,128]{1,0:T(8,128)S(1)} %pre_parts.1.mine_ref), channel_id=1, source_target_pairs={{0,2},{2,0},{1,3},{3,1},{4,6},{6,4},{5,7},{7,5},{8,10},{10,8},{9,1... | collective-permute-start | bytes 884744 | tf_op jit(solution)/shard_map/ppermute | solution.py:440
  35.5 0.8 copy-start
  37.0 0.7 copy-start.3
  37.7 8.6 %collective-permute-start.4 = (f32[5,64,1024]{2,1,0:T(8,128)S(1)}, f32[5,64,1024]{2,1,0:T(8,128)S(1)}, u32[]{:S(2)}, u32[]{:S(2)}) collective-permute-start(f32[5,64,1024]{2,1,0:T(8,128)S(1)} %get-tuple-element.34.own_ref), channel_id=1, source_target_pairs={{0,1},{1,0},{2,3},{3,2},{4,5},{5,4},{6,7},{7,6},{8,9},{9,8},{10,11... | collective-permute-start | bytes 3932168 | tf_op jit(solution)/shard_map/ppermute | solution.py:444
  39.7 17.6 %all-to-all-start.1 = ((bf16[32,56,128]{2,1,0:T(8,128)(2,1)}), bf16[32,56,128]{2,1,0:T(8,128)(2,1)S(1)}, u32[]{:S(2)}, u32[]{:S(2)}) async-start(bf16[32,56,128]{2,1,0:T(8,128)(2,1)} %bitcast.30), calls=%async_computation.1 | async-start | bytes 917504 | tf_op jit(solution)/shard_map/all_to_all | solution.py:466
  46.4 1.0 %copy-start.4 = (f32[64,1024]{1,0:T(8,128)S(1)}, f32[64,1024]{1,0:T(8,128)}, u32[]{:S(2)}) copy-start(f32[64,1024]{1,0:T(8,128)} %copy-done.3) | copy-start | bytes 786436
  47.3 9.9 %copy-start.8 = (s32[128,2]{0,1:T(2,128)S(1)}, s32[128,2]{0,1:T(2,128)}, u32[]{:S(2)}) copy-start(s32[128,2]{0,1:T(2,128)} %param.8) | copy-start | bytes 3076
  47.6 0.8 copy-start.1
  48.4 0.7 copy-start.10
  49.0 44.3 %copy-start.9 = (f32[128,2]{0,1:T(2,128)S(1)}, f32[128,2]{0,1:T(2,128)}, u32[]{:S(2)}) copy-start(f32[128,2]{0,1:T(2,128)} %param.9) | copy-start | bytes 3076
  49.0 38.9 %copy-start.2 = (f32[3,32,1024]{2,1,0:T(8,128)S(1)}, f32[3,32,1024]{2,1,0:T(8,128)}, u32[]{:S(2)}) copy-start(f32[3,32,1024]{2,1,0:T(8,128)} %copy-done.1) | copy-start | bytes 1179652
  49.0 8.2 %collective-permute-start.5 = (f32[2,1024]{1,0:T(2,128)S(1)}, f32[2,1024]{1,0:T(2,128)S(1)}, u32[]{:S(2)}, u32[]{:S(2)}) collective-permute-start(f32[2,1024]{1,0:T(2,128)S(1)} %get-tuple-element.36.norms_ref), channel_id=1, source_target_pairs={{0,2},{2,0},{1,3},{3,1},{4,6},{6,4},{5,7},{7,5},{8,10},{10,8},{9,1... | collective-permute-start | bytes 24584 | tf_op jit(solution)/shard_map/ppermute | solution.py:440
  58.4 34.9 %all-to-all-start.2 = ((bf16[8,104,128]{2,1,0:T(8,128)(2,1)}), bf16[8,104,128]{2,1,0:T(8,128)(2,1)S(1)}, u32[]{:S(2)}, u32[]{:S(2)}) async-start(bf16[8,104,128]{2,1,0:T(8,128)(2,1)} %combine.1), calls=%async_computation.2 | async-start | bytes 425984 | tf_op jit(solution)/shard_map/all_to_all | solution.py:473
  72.6 15.3 %collective-permute-start.6 = (bf16[3,32,1024]{2,1,0:T(8,128)(2,1)}, bf16[3,32,1024]{2,1,0:T(8,128)(2,1)S(1)}, u32[]{:S(2)}, u32[]{:S(2)}) collective-permute-start(bf16[3,32,1024]{2,1,0:T(8,128)(2,1)} %copy-done.10), channel_id=1, source_target_pairs={{0,2},{2,0},{1,3},{3,1},{4,6},{6,4},{5,7},{7,5},{8,10},{10,8},{9,1... | collective-permute-start | bytes 589832 | tf_op jit(solution)/shard_map/ppermute | solution.py:440

commit v4 on v3

--- a/solution.py
+++ b/solution.py
@@ -28,6 +28,10 @@
 
 def iota(shape, dim):
     return lax.broadcasted_iota(jnp.int32, shape, dim)
+
+
+def first_team(teams):
+    return teams * 5 // 8
 
 
 def block(j, side):
@@ -364,7 +368,8 @@
         sums = tn(rows, pick).astype(bf16)
         for h in range(2):
             for b in range(2):
-                msg_ref[h * (depth // 2) + 2 * q + b, 0:64, :] = sums[
+                team = h * (depth // 2) + 2 * q + b
+                msg_ref[(team - first_team(depth)) % depth, 0:64, :] = sums[
                     64 * b : 64 * b + 64, h * tok : (h + 1) * tok
                 ]
     tail = back_ref[:, :, blocks * ROWS :, :].astype(f32).reshape(experts * 2, 8, 128)
@@ -470,8 +475,8 @@
     own, other, norms = totals(place, part, down, over_core(part))
     norms_got = over_side(norms)
     msg = combine(place, routes_t, back, norms, norms_got, depth)
-    parts = lax.all_to_all(msg, "team", 0, 0, tiled=True)
-    other, msg = lax.optimization_barrier((other, msg))
+    turned = [(n + first_team(depth)) % depth for n in range(depth)]
+    parts = lax.all_to_all(msg, "team", 0, 0, axis_index_groups=[turned], tiled=True)
     got = over_side(other)
     glu_wg, lin_wg, down_wg, down_norms = place_grads(place, own, got)
     tok_t, gate_t, glu_norms, lin_norms = finish(parts, gates_t)

time: 94.6 us -> 92.8 us (0.981)
  the two profiles are of different devices: /device:TPU:32 before, /device:TPU:1 now
where the time goes in v4:
time: 92.8 us; the launch traced here: 92.1 us
  starting transfers between devices  53.7 us (58%)
  waiting for transfers between devices  25.4 us (27%)
  Pallas kernels  8.3 us (9%)
  local copies, waits for them, and re-layouts  3.86 us (4%)
    ppermute x4, waiting for transfers between devices, over_side(): return lax.ppermute(x, 'side', [(0, 1), (1, 0)])  18.4 us
    all_to_all x1, starting transfers between devices, layer(): lax.all_to_all(msg, 'team', 0, 0, axis_index_groups=[turned], tiled=True)  14.6 us
    ppermute x3, starting transfers between devices, over_core(): return lax.ppermute(x, 'core', [(0, 1), (1, 0)])  13 us
    ppermute x4, starting transfers between devices, over_side(): return lax.ppermute(x, 'side', [(0, 1), (1, 0)])  11.2 us
    all_to_all x1, starting transfers between devices, layer(): lax.all_to_all(packed.reshape(experts, ROWS, width // 2), 'ep', 0, 0, til...  7.57 us
    all_to_all x1, starting transfers between devices, layer(): back = lax.all_to_all(msg, ('ep', 'core'), 0, 0, tiled=True)  7.33 us
    all_to_all x1, waiting for transfers between devices, layer(): back = lax.all_to_all(msg, ('ep', 'core'), 0, 0, tiled=True)  5.91 us
    unnamed x22, local copies, waits for them, and re-layouts  3.86 us
  transfers between devices with their start and end apart: 10, of which 5 were waited for; matrix products, arithmetic and copies ran while one was open for 0% of the time, Pallas kernels for 2%

profile of v4, /device:TPU:1, one launch (start us, length us, event | category | flops | bytes accessed | tf_op | source)
XLA Modules:
  0.0 92.1 jit_solution(5726799403932485390)
XLA Ops:
  0.6 0.0 copy-start.5
  0.7 0.0 copy-start.6
  0.7 0.0 copy-start.7
  0.7 3.1 %pack_rows.1 = bf16[384,1024]{1,0:T(8,128)(2,1)} custom-call(s32[1]{0:T(128)} %bitcast.place_ref, s32[1]{0:T(128)} %bitcast.2.core_ref, s32[2,128]{1,0:T(2,128)} %bitcast.34, f32[2,128]{1,0:T(2,128)} %bitcast.36, bf16[128,2048]{1,0:T(8,128)(2,1)} %tok_ref.1, bf16[128,2048]{1,0:T(8,128)(2,1)} %cot_ref.1), custom_call_target="tpu_custom_call" | custom-call | tf_op jit(solution)/shard_map/pack_rows/pallas_call | solution.py:102
  3.7 7.6 %all-to-all-start = ((bf16[16,24,1024]{2,1,0:T(8,128)(2,1)}), bf16[16,24,1024]{2,1,0:T(8,128)(2,1)S(1)}, u32[]{:S(2)}, u32[]{:S(2)}) async-start(bf16[16,24,1024]{2,1,0:T(8,128)(2,1)} %bitcast.38), calls=%async_computation | async-start | bytes 1572864 | tf_op jit(solution)/shard_map/all_to_all | solution.py:461
  11.3 0.0 copy-done.5
  11.3 0.0 copy-done.6
  11.3 0.0 copy-done.7
  11.4 0.1 part_weights.1
  11.5 3.5 %collective-permute-start = (bf16[96,1024]{1,0:T(8,128)(2,1)S(1)}, bf16[96,1024]{1,0:T(8,128)(2,1)S(1)}, u32[]{:S(2)}, u32[]{:S(2)}) collective-permute-start(bf16[96,1024]{1,0:T(8,128)(2,1)S(1)} %get-tuple-element.28), channel_id=1, source_target_pairs={{0,2},{2,0},{1,3},{3,1},{4,6},{6,4},{5,7},{7,5},{8,10},{10,8},{9,1... | collective-permute-start | bytes 589832 | tf_op jit(solution)/shard_map/ppermute | solution.py:445
  15.0 3.2 %collective-permute-start.1 = (bf16[96,1024]{1,0:T(8,128)(2,1)S(1)}, bf16[96,1024]{1,0:T(8,128)(2,1)S(1)}, u32[]{:S(2)}, u32[]{:S(2)}) collective-permute-start(bf16[96,1024]{1,0:T(8,128)(2,1)S(1)} %get-tuple-element.27.keep_ref), channel_id=1, source_target_pairs={{0,1},{1,0},{2,3},{3,2},{4,5},{5,4},{6,7},{7,6},{8,9},{9,8},{10,11... | collective-permute-start | bytes 589832 | tf_op jit(solution)/shard_map/ppermute | solution.py:449
  18.2 0.1 collective-permute-done.side_ref
  18.3 5.6 %collective-permute-start.2 = (bf16[96,1024]{1,0:T(8,128)(2,1)S(1)}, bf16[96,1024]{1,0:T(8,128)(2,1)S(1)}, u32[]{:S(2)}, u32[]{:S(2)}) collective-permute-start(bf16[96,1024]{1,0:T(8,128)(2,1)S(1)} %collective-permute-done.side_ref), channel_id=1, source_target_pairs={{0,1},{1,0},{2,3},{3,2},{4,5},{5,4},{6,7},{7,6},{8,9},{9,8},{10,11... | collective-permute-start | bytes 589832 | tf_op jit(solution)/shard_map/ppermute | solution.py:449
  23.8 0.0 collective-permute-done.1.core_ref
  23.8 1.0 %collective-permute-done.2.cross_ref = bf16[96,1024]{1,0:T(8,128)(2,1)S(1)} collective-permute-done((bf16[96,1024]{1,0:T(8,128)(2,1)S(1)}, bf16[96,1024]{1,0:T(8,128)(2,1)S(1)}, u32[]{:S(2)}, u32[]{:S(2)}) %collective-permute-start.2) | collective-permute-done | bytes 196640 | tf_op jit(solution)/shard_map/ppermute | solution.py:449
  24.9 0.3 gather_weights.1
  25.2 0.0 all-to-all-done
  25.2 0.6 pre_parts.1.mine_ref
  25.8 2.9 %collective-permute-start.3 = (f32[576,128]{1,0:T(8,128)S(1)}, f32[576,128]{1,0:T(8,128)S(1)}, u32[]{:S(2)}, u32[]{:S(2)}) collective-permute-start(f32[576,128]{1,0:T(8,128)S(1)} %pre_parts.1.mine_ref), channel_id=1, source_target_pairs={{0,2},{2,0},{1,3},{3,1},{4,6},{6,4},{5,7},{7,5},{8,10},{10,8},{9,1... | collective-permute-start | bytes 884744 | tf_op jit(solution)/shard_map/ppermute | solution.py:445
  28.7 6.0 %collective-permute-done.3.got_ref = f32[576,128]{1,0:T(8,128)S(1)} collective-permute-done((f32[576,128]{1,0:T(8,128)S(1)}, f32[576,128]{1,0:T(8,128)S(1)}, u32[]{:S(2)}, u32[]{:S(2)}) %collective-permute-start.3) | collective-permute-done | bytes 294944 | tf_op jit(solution)/shard_map/ppermute | solution.py:445
  34.7 0.5 units.1
  35.2 0.0 copy-start
  35.2 0.8 copy-done
  36.0 0.8 wgrads.1
  36.8 0.0 copy-start.3
  36.8 0.7 copy-done.3
  37.5 4.3 %collective-permute-start.4 = (f32[5,64,1024]{2,1,0:T(8,128)S(1)}, f32[5,64,1024]{2,1,0:T(8,128)S(1)}, u32[]{:S(2)}, u32[]{:S(2)}) collective-permute-start(f32[5,64,1024]{2,1,0:T(8,128)S(1)} %get-tuple-element.33.own_ref), channel_id=1, source_target_pairs={{0,1},{1,0},{2,3},{3,2},{4,5},{5,4},{6,7},{7,6},{8,9},{9,8},{10,11... | collective-permute-start | bytes 3932168 | tf_op jit(solution)/shard_map/ppermute | solution.py:449
  41.8 7.3 %all-to-all-start.1 = ((bf16[32,56,128]{2,1,0:T(8,128)(2,1)}), bf16[32,56,128]{2,1,0:T(8,128)(2,1)S(1)}, u32[]{:S(2)}, u32[]{:S(2)}) async-start(bf16[32,56,128]{2,1,0:T(8,128)(2,1)} %bitcast.30), calls=%async_computation.1 | async-start | bytes 917504 | tf_op jit(solution)/shard_map/all_to_all | solution.py:471
  49.1 0.0 collective-permute-done.4.got_ref
  49.1 0.0 copy-start.4
  49.1 0.9 %copy-done.4 = f32[64,1024]{1,0:T(8,128)S(1)} copy-done((f32[64,1024]{1,0:T(8,128)S(1)}, f32[64,1024]{1,0:T(8,128)}, u32[]{:S(2)}) %copy-start.4) | copy-done | bytes 262168
  50.1 0.3 totals.1
  50.3 0.0 copy-start.1
  50.3 0.8 copy-done.1
  51.1 0.7 copy-done.10
  51.8 2.2 %collective-permute-start.5 = (f32[2,1024]{1,0:T(2,128)S(1)}, f32[2,1024]{1,0:T(2,128)S(1)}, u32[]{:S(2)}, u32[]{:S(2)}) collective-permute-start(f32[2,1024]{1,0:T(2,128)S(1)} %get-tuple-element.35.norms_ref), channel_id=1, source_target_pairs={{0,2},{2,0},{1,3},{3,1},{4,6},{6,4},{5,7},{7,5},{8,10},{10,8},{9,1... | collective-permute-start | bytes 24584 | tf_op jit(solution)/shard_map/ppermute | solution.py:445
  54.0 5.9 %all-to-all-done.1 = bf16[32,56,128]{2,1,0:T(8,128)(2,1)S(1)} async-done(((bf16[32,56,128]{2,1,0:T(8,128)(2,1)}), bf16[32,56,128]{2,1,0:T(8,128)(2,1)S(1)}, u32[]{:S(2)}, u32[]{:S(2)}) %all-to-all-start.1) | async-done | bytes 458784 | tf_op jit(solution)/shard_map/all_to_all | solution.py:471
  59.9 0.0 collective-permute-done.5.got_ref
  59.9 0.0 copy-done.8
  59.9 1.1 %combine.1 = bf16[8,104,128]{2,1,0:T(8,128)(2,1)} custom-call(s32[1]{0:T(128)} %bitcast.place_ref, s32[2,128]{1,0:T(2,128)S(1)} %bitcast.35, bf16[16,2,56,128]{3,2,1,0:T(8,128)(2,1)S(1)} %bitcast.29, f32[2,1024]{1,0:T(2,128)S(1)} %get-tuple-element.35.norms_ref, f32[2,1024]{1,0:T(2,128)S(1)} %collective-permute-done.5.got_ref), custom_call_target="tpu_custom_call" | custom-call | tf_op jit(solution)/shard_map/combine/pallas_call | solution.py:407
  61.0 14.6 %all-to-all-start.2 = ((bf16[8,104,128]{2,1,0:T(8,128)(2,1)}), bf16[8,104,128]{2,1,0:T(8,128)(2,1)S(1)}, u32[]{:S(2)}, u32[]{:S(2)}) async-start(bf16[8,104,128]{2,1,0:T(8,128)(2,1)} %combine.1), calls=%async_computation.2 | async-start | bytes 425984 | tf_op jit(solution)/shard_map/all_to_all | solution.py:479
  75.6 2.6 %collective-permute-start.6 = (bf16[3,32,1024]{2,1,0:T(8,128)(2,1)}, bf16[3,32,1024]{2,1,0:T(8,128)(2,1)S(1)}, u32[]{:S(2)}, u32[]{:S(2)}) collective-permute-start(bf16[3,32,1024]{2,1,0:T(8,128)(2,1)} %copy-done.10), channel_id=1, source_target_pairs={{0,2},{2,0},{1,3},{3,1},{4,6},{6,4},{5,7},{7,5},{8,10},{10,8},{9,1... | collective-permute-start | bytes 589832 | tf_op jit(solution)/shard_map/ppermute | solution.py:445
  78.2 12.3 %collective-permute-done.6.got_ref = bf16[3,32,1024]{2,1,0:T(8,128)(2,1)S(1)} collective-permute-done((bf16[3,32,1024]{2,1,0:T(8,128)(2,1)}, bf16[3,32,1024]{2,1,0:T(8,128)(2,1)S(1)}, u32[]{:S(2)}, u32[]{:S(2)}) %collective-permute-start.6) | collective-permute-done | bytes 196640 | tf_op jit(solution)/shard_map/ppermute | solution.py:445
  90.6 0.0 copy-done.2
  90.6 0.9 %place_grads.1 = (f32[32,2048]{1,0:T(8,128)}, f32[32,2048]{1,0:T(8,128)}, f32[32,2048]{1,0:T(8,128)}, f32[1,128]{1,0:T(1,128)}) custom-call(s32[1]{0:T(128)} %bitcast.place_ref, f32[3,32,1024]{2,1,0:T(8,128)S(1)} %copy-done.2, bf16[3,32,1024]{2,1,0:T(8,128)(2,1)S(1)} %collective-permute-done.6.got_ref), custom_call_target="tpu_custom_call" | custom-call | tf_op jit(solution)/shard_map/place_grads/pallas_call | solution.py:338
  91.5 0.0 all-to-all-done.2.parts_ref
  91.5 0.0 copy-done.9
  91.5 0.6 finish.1
  (4 shorter events, 0.0 us)
Async XLA Ops:
  0.6 10.7 %copy-start.5 = (bf16[1,2048,32]{1,2,0:T(8,128)(2,1)S(1)}, bf16[1,2048,32]{1,2,0:T(8,128)(2,1)}, u32[]{:S(2)}) copy-start(bf16[1,2048,32]{1,2,0:T(8,128)(2,1)} %param.11) | copy-start | bytes 393220
  0.7 10.7 %copy-start.6 = (bf16[1,2048,32]{1,2,0:T(8,128)(2,1)S(1)}, bf16[1,2048,32]{1,2,0:T(8,128)(2,1)}, u32[]{:S(2)}) copy-start(bf16[1,2048,32]{1,2,0:T(8,128)(2,1)} %param.12) | copy-start | bytes 393220
  0.7 10.7 %copy-start.7 = (bf16[1,32,2048]{2,1,0:T(8,128)(2,1)S(1)}, bf16[1,32,2048]{2,1,0:T(8,128)(2,1)}, u32[]{:S(2)}) copy-start(bf16[1,32,2048]{2,1,0:T(8,128)(2,1)} %param.13) | copy-start | bytes 393220
  3.7 21.4 %all-to-all-start = ((bf16[16,24,1024]{2,1,0:T(8,128)(2,1)}), bf16[16,24,1024]{2,1,0:T(8,128)(2,1)S(1)}, u32[]{:S(2)}, u32[]{:S(2)}) async-start(bf16[16,24,1024]{2,1,0:T(8,128)(2,1)} %bitcast.38), calls=%async_computation | async-start | bytes 1572864 | tf_op jit(solution)/shard_map/all_to_all | solution.py:461
  11.5 6.8 %collective-permute-start = (bf16[96,1024]{1,0:T(8,128)(2,1)S(1)}, bf16[96,1024]{1,0:T(8,128)(2,1)S(1)}, u32[]{:S(2)}, u32[]{:S(2)}) collective-permute-start(bf16[96,1024]{1,0:T(8,128)(2,1)S(1)} %get-tuple-element.28), channel_id=1, source_target_pairs={{0,2},{2,0},{1,3},{3,1},{4,6},{6,4},{5,7},{7,5},{8,10},{10,8},{9,1... | collective-permute-start | bytes 589832 | tf_op jit(solution)/shard_map/ppermute | solution.py:445
  15.0 8.8 %collective-permute-start.1 = (bf16[96,1024]{1,0:T(8,128)(2,1)S(1)}, bf16[96,1024]{1,0:T(8,128)(2,1)S(1)}, u32[]{:S(2)}, u32[]{:S(2)}) collective-permute-start(bf16[96,1024]{1,0:T(8,128)(2,1)S(1)} %get-tuple-element.27.keep_ref), channel_id=1, source_target_pairs={{0,1},{1,0},{2,3},{3,2},{4,5},{5,4},{6,7},{7,6},{8,9},{9,8},{10,11... | collective-permute-start | bytes 589832 | tf_op jit(solution)/shard_map/ppermute | solution.py:449
  18.3 6.6 %collective-permute-start.2 = (bf16[96,1024]{1,0:T(8,128)(2,1)S(1)}, bf16[96,1024]{1,0:T(8,128)(2,1)S(1)}, u32[]{:S(2)}, u32[]{:S(2)}) collective-permute-start(bf16[96,1024]{1,0:T(8,128)(2,1)S(1)} %collective-permute-done.side_ref), channel_id=1, source_target_pairs={{0,1},{1,0},{2,3},{3,2},{4,5},{5,4},{6,7},{7,6},{8,9},{9,8},{10,11... | collective-permute-start | bytes 589832 | tf_op jit(solution)/shard_map/ppermute | solution.py:449
  25.8 8.9 %collective-permute-start.3 = (f32[576,128]{1,0:T(8,128)S(1)}, f32[576,128]{1,0:T(8,128)S(1)}, u32[]{:S(2)}, u32[]{:S(2)}) collective-permute-start(f32[576,128]{1,0:T(8,128)S(1)} %pre_parts.1.mine_ref), channel_id=1, source_target_pairs={{0,2},{2,0},{1,3},{3,1},{4,6},{6,4},{5,7},{7,5},{8,10},{10,8},{9,1... | collective-permute-start | bytes 884744 | tf_op jit(solution)/shard_map/ppermute | solution.py:445
  35.2 0.8 copy-start
  36.8 0.7 copy-start.3
  37.5 11.6 %collective-permute-start.4 = (f32[5,64,1024]{2,1,0:T(8,128)S(1)}, f32[5,64,1024]{2,1,0:T(8,128)S(1)}, u32[]{:S(2)}, u32[]{:S(2)}) collective-permute-start(f32[5,64,1024]{2,1,0:T(8,128)S(1)} %get-tuple-element.33.own_ref), channel_id=1, source_target_pairs={{0,1},{1,0},{2,3},{3,2},{4,5},{5,4},{6,7},{7,6},{8,9},{9,8},{10,11... | collective-permute-start | bytes 3932168 | tf_op jit(solution)/shard_map/ppermute | solution.py:449
  41.8 18.1 %all-to-all-start.1 = ((bf16[32,56,128]{2,1,0:T(8,128)(2,1)}), bf16[32,56,128]{2,1,0:T(8,128)(2,1)S(1)}, u32[]{:S(2)}, u32[]{:S(2)}) async-start(bf16[32,56,128]{2,1,0:T(8,128)(2,1)} %bitcast.30), calls=%async_computation.1 | async-start | bytes 917504 | tf_op jit(solution)/shard_map/all_to_all | solution.py:471
  49.1 1.0 %copy-start.4 = (f32[64,1024]{1,0:T(8,128)S(1)}, f32[64,1024]{1,0:T(8,128)}, u32[]{:S(2)}) copy-start(f32[64,1024]{1,0:T(8,128)} %copy-done.3) | copy-start | bytes 786436
  50.1 9.8 %copy-start.8 = (s32[128,2]{0,1:T(2,128)S(1)}, s32[128,2]{0,1:T(2,128)}, u32[]{:S(2)}) copy-start(s32[128,2]{0,1:T(2,128)} %param.8) | copy-start | bytes 3076
  50.3 0.8 copy-start.1
  51.1 0.7 copy-start.10
  51.8 39.7 %copy-start.9 = (f32[128,2]{0,1:T(2,128)S(1)}, f32[128,2]{0,1:T(2,128)}, u32[]{:S(2)}) copy-start(f32[128,2]{0,1:T(2,128)} %param.9) | copy-start | bytes 3076
  51.8 38.8 %copy-start.2 = (f32[3,32,1024]{2,1,0:T(8,128)S(1)}, f32[3,32,1024]{2,1,0:T(8,128)}, u32[]{:S(2)}) copy-start(f32[3,32,1024]{2,1,0:T(8,128)} %copy-done.1) | copy-start | bytes 1179652
  51.8 8.1 %collective-permute-start.5 = (f32[2,1024]{1,0:T(2,128)S(1)}, f32[2,1024]{1,0:T(2,128)S(1)}, u32[]{:S(2)}, u32[]{:S(2)}) collective-permute-start(f32[2,1024]{1,0:T(2,128)S(1)} %get-tuple-element.35.norms_ref), channel_id=1, source_target_pairs={{0,2},{2,0},{1,3},{3,1},{4,6},{6,4},{5,7},{7,5},{8,10},{10,8},{9,1... | collective-permute-start | bytes 24584 | tf_op jit(solution)/shard_map/ppermute | solution.py:445
  61.0 30.5 %all-to-all-start.2 = ((bf16[8,104,128]{2,1,0:T(8,128)(2,1)}), bf16[8,104,128]{2,1,0:T(8,128)(2,1)S(1)}, u32[]{:S(2)}, u32[]{:S(2)}) async-start(bf16[8,104,128]{2,1,0:T(8,128)(2,1)} %combine.1), calls=%async_computation.2 | async-start | bytes 425984 | tf_op jit(solution)/shard_map/all_to_all | solution.py:479
  75.6 15.0 %collective-permute-start.6 = (bf16[3,32,1024]{2,1,0:T(8,128)(2,1)}, bf16[3,32,1024]{2,1,0:T(8,128)(2,1)S(1)}, u32[]{:S(2)}, u32[]{:S(2)}) collective-permute-start(bf16[3,32,1024]{2,1,0:T(8,128)(2,1)} %copy-done.10), channel_id=1, source_target_pairs={{0,2},{2,0},{1,3},{3,1},{4,6},{6,4},{5,7},{7,5},{8,10},{10,8},{9,1... | collective-permute-start | bytes 589832 | tf_op jit(solution)/shard_map/ppermute | solution.py:445

commit v5 on v4

--- a/solution.py
+++ b/solution.py
@@ -262,7 +262,7 @@
     )(mine, got, wret)
 
 
-def wgrad_kernel(grads_ref, rows_ref, part_ref, down_ref):
+def wgrad_kernel(grads_ref, rows_ref, own_ref, down_ref, send_ref):
     step = min(512, rows_ref.shape[1])
 
     @pl.loop(0, rows_ref.shape[1] // step)
@@ -270,9 +270,10 @@
         cols = pl.ds(pl.multiple_of(n * step, step), step)
         part = tn(grads_ref[...], rows_ref[:, cols])
         for k in range(4):
-            part_ref[k, :, cols] = part[64 * k : 64 * k + 64, :]
+            own_ref[k, :, cols] = part[64 * k : 64 * k + 64, :]
+            send_ref[k, :, cols] = part[64 * k : 64 * k + 64, :].astype(bf16)
         down_ref[:, cols] = part[256:320, :]
-        part_ref[4, :, cols] = part[320:384, :]
+        send_ref[4, :, cols] = part[320:384, :].astype(bf16)
 
 
 def wgrads(grads, rows):
@@ -280,31 +281,34 @@
     return pl.pallas_call(
         wgrad_kernel,
         out_shape=(
-            jax.ShapeDtypeStruct((5, 64, width), f32),
+            jax.ShapeDtypeStruct((4, 64, width), f32),
             jax.ShapeDtypeStruct((64, width), f32),
+            jax.ShapeDtypeStruct((5, 64, width), bf16),
         ),
         in_specs=[VMEM, VMEM],
-        out_specs=(VMEM,) * 2,
+        out_specs=(VMEM,) * 3,
         compiler_params=pltpu.CompilerParams(vmem_limit_bytes=LIMIT),
         name="wgrads",
     )(grads, rows)
 
 
-def total_kernel(place_ref, own_ref, down_ref, got_ref, keep_ref, send_ref, norms_ref):
+def total_kernel(place_ref, own_ref, down_ref, sent_ref, got_ref, keep_ref, send_ref, norms_ref):
     side = place_ref[0]
     for k in range(3):
         if k < 2:
-            mine = own_ref[2 * k] + got_ref[2 * k + 1]
-            other = own_ref[2 * k + 1] + got_ref[2 * k]
-            norms_ref[k : k + 1, :] = jnp.sum(mine * mine + other * other, axis=0, keepdims=True)
+            first, second = got_ref[2 * k].astype(f32), got_ref[2 * k + 1].astype(f32)
+            one = sent_ref[2 * k].astype(f32) + second
+            two = sent_ref[2 * k + 1].astype(f32) + first
+            norms_ref[k : k + 1, :] = jnp.sum(one * one + two * two, axis=0, keepdims=True)
+            mine = own_ref[2 * k] + second
         else:
-            mine = down_ref[...] + got_ref[4]
+            mine = down_ref[...] + got_ref[4].astype(f32)
         low, high = mine[:32, :], mine[32:, :]
         keep_ref[k] = jnp.where(side == 0, low, high)
         send_ref[k] = jnp.where(side == 0, high, low).astype(bf16)
 
 
-def totals(place, own, down, got):
+def totals(place, own, down, sent, got):
     width = own.shape[2]
     return pl.pallas_call(
         total_kernel,
@@ -313,11 +317,11 @@
             jax.ShapeDtypeStruct((3, 32, width), bf16),
             jax.ShapeDtypeStruct((2, width), f32),
         ),
-        in_specs=[SMEM, VMEM, VMEM, VMEM],
+        in_specs=[SMEM] + [VMEM] * 4,
         out_specs=(VMEM,) * 3,
         compiler_params=pltpu.CompilerParams(vmem_limit_bytes=LIMIT),
         name="totals",
-    )(place, own, down, got)
+    )(place, own, down, sent, got)
 
 
 def place_kernel(place_ref, own_ref, got_ref, glu_ref, lin_ref, down_ref, norms_ref):
@@ -471,8 +475,8 @@
     back = lax.all_to_all(msg, ("ep", "core"), 0, 0, tiled=True)
     back = back.reshape(experts, 2, *msg.shape[1:])
 
-    part, down = wgrads(grads, rows)
-    own, other, norms = totals(place, part, down, over_core(part))
+    own, down, sent = wgrads(grads, rows)
+    own, other, norms = totals(place, own, down, sent, over_core(sent))
     norms_got = over_side(norms)
     msg = combine(place, routes_t, back, norms, norms_got, depth)
     turned = [(n + first_team(depth)) % depth for n in range(depth)]

time: 92.8 us -> 93 us (level)
  local copies, waits for them, and re-layouts: 3.86 us -> 2.16 us
  waiting for transfers between devices: 25.4 us -> 26.9 us
    unnamed x22 -> x20, local copies, waits for them, and re-layouts: 3.86 us -> 2.16 us
    all_to_all x1, waiting for transfers between devices: 5.91 us -> 7.51 us  [layer(): back = lax.all_to_all(msg, ('ep', 'core'), 0, 0, tiled=True)]
where the time goes in v5:
time: 93 us; the launch traced here: 92.4 us
  starting transfers between devices  54.1 us (58%)
  waiting for transfers between devices  26.9 us (29%)
  Pallas kernels  8.35 us (9%)
  local copies, waits for them, and re-layouts  2.16 us (2%)
    ppermute x4, waiting for transfers between devices, over_side(): return lax.ppermute(x, 'side', [(0, 1), (1, 0)])  18.3 us
    all_to_all x1, starting transfers between devices, layer(): lax.all_to_all(msg, 'team', 0, 0, axis_index_groups=[turned], tiled=True)  14.7 us
    ppermute x3, starting transfers between devices, over_core(): return lax.ppermute(x, 'core', [(0, 1), (1, 0)])  13 us
    ppermute x4, starting transfers between devices, over_side(): return lax.ppermute(x, 'side', [(0, 1), (1, 0)])  11.3 us
    all_to_all x1, starting transfers between devices, layer(): lax.all_to_all(packed.reshape(experts, ROWS, width // 2), 'ep', 0, 0, til...  7.71 us
    all_to_all x1, waiting for transfers between devices, layer(): back = lax.all_to_all(msg, ('ep', 'core'), 0, 0, tiled=True)  7.51 us
    all_to_all x1, starting transfers between devices, layer(): back = lax.all_to_all(msg, ('ep', 'core'), 0, 0, tiled=True)  7.46 us
    pallas_call x1, Pallas kernels, pack_rows(): pl.pallas_call(pack_kernel, out_shape=jax.ShapeDtypeStruct((experts * ROW...  3.01 us
  transfers between devices with their start and end apart: 10, of which 5 were waited for; matrix products, arithmetic and copies ran while one was open for 0% of the time, Pallas kernels for 2%

profile of v5, /device:TPU:1, one launch (start us, length us, event | category | flops | bytes accessed | tf_op | source)
XLA Modules:
  0.0 92.4 jit_solution(1668663577081714358)
XLA Ops:
  0.6 3.0 %pack_rows.1 = bf16[384,1024]{1,0:T(8,128)(2,1)} custom-call(s32[1]{0:T(128)} %bitcast.place_ref, s32[1]{0:T(128)} %bitcast.2.core_ref, s32[2,128]{1,0:T(2,128)} %bitcast.34, f32[2,128]{1,0:T(2,128)} %bitcast.36, bf16[128,2048]{1,0:T(8,128)(2,1)} %tok_ref.1, bf16[128,2048]{1,0:T(8,128)(2,1)} %cot_ref.1), custom_call_target="tpu_custom_call" | custom-call | tf_op jit(solution)/shard_map/pack_rows/pallas_call | solution.py:102
  3.6 0.0 copy-start.3
  3.7 0.0 copy-start.4
  3.7 0.0 copy-start.5
  3.7 7.7 %all-to-all-start = ((bf16[16,24,1024]{2,1,0:T(8,128)(2,1)}), bf16[16,24,1024]{2,1,0:T(8,128)(2,1)S(1)}, u32[]{:S(2)}, u32[]{:S(2)}) async-start(bf16[16,24,1024]{2,1,0:T(8,128)(2,1)} %bitcast.38), calls=%async_computation | async-start | bytes 1572864 | tf_op jit(solution)/shard_map/all_to_all | solution.py:465
  11.4 0.0 copy-done.3
  11.4 0.0 copy-done.4
  11.4 0.0 copy-done.5
  11.4 0.1 part_weights.1
  11.5 3.5 %collective-permute-start = (bf16[96,1024]{1,0:T(8,128)(2,1)S(1)}, bf16[96,1024]{1,0:T(8,128)(2,1)S(1)}, u32[]{:S(2)}, u32[]{:S(2)}) collective-permute-start(bf16[96,1024]{1,0:T(8,128)(2,1)S(1)} %get-tuple-element.29), channel_id=1, source_target_pairs={{0,2},{2,0},{1,3},{3,1},{4,6},{6,4},{5,7},{7,5},{8,10},{10,8},{9,1... | collective-permute-start | bytes 589832 | tf_op jit(solution)/shard_map/ppermute | solution.py:449
  15.1 3.2 %collective-permute-start.1 = (bf16[96,1024]{1,0:T(8,128)(2,1)S(1)}, bf16[96,1024]{1,0:T(8,128)(2,1)S(1)}, u32[]{:S(2)}, u32[]{:S(2)}) collective-permute-start(bf16[96,1024]{1,0:T(8,128)(2,1)S(1)} %get-tuple-element.28.keep_ref), channel_id=1, source_target_pairs={{0,1},{1,0},{2,3},{3,2},{4,5},{5,4},{6,7},{7,6},{8,9},{9,8},{10,11... | collective-permute-start | bytes 589832 | tf_op jit(solution)/shard_map/ppermute | solution.py:453
  18.2 0.1 collective-permute-done.side_ref
  18.3 5.5 %collective-permute-start.2 = (bf16[96,1024]{1,0:T(8,128)(2,1)S(1)}, bf16[96,1024]{1,0:T(8,128)(2,1)S(1)}, u32[]{:S(2)}, u32[]{:S(2)}) collective-permute-start(bf16[96,1024]{1,0:T(8,128)(2,1)S(1)} %collective-permute-done.side_ref), channel_id=1, source_target_pairs={{0,1},{1,0},{2,3},{3,2},{4,5},{5,4},{6,7},{7,6},{8,9},{9,8},{10,11... | collective-permute-start | bytes 589832 | tf_op jit(solution)/shard_map/ppermute | solution.py:453
  23.9 0.0 collective-permute-done.1.core_ref
  23.9 1.0 %collective-permute-done.2.cross_ref = bf16[96,1024]{1,0:T(8,128)(2,1)S(1)} collective-permute-done((bf16[96,1024]{1,0:T(8,128)(2,1)S(1)}, bf16[96,1024]{1,0:T(8,128)(2,1)S(1)}, u32[]{:S(2)}, u32[]{:S(2)}) %collective-permute-start.2) | collective-permute-done | bytes 196640 | tf_op jit(solution)/shard_map/ppermute | solution.py:453
  24.9 0.3 gather_weights.1
  25.2 0.0 all-to-all-done
  25.2 0.6 pre_parts.1.mine_ref
  25.8 2.9 %collective-permute-start.3 = (f32[576,128]{1,0:T(8,128)S(1)}, f32[576,128]{1,0:T(8,128)S(1)}, u32[]{:S(2)}, u32[]{:S(2)}) collective-permute-start(f32[576,128]{1,0:T(8,128)S(1)} %pre_parts.1.mine_ref), channel_id=1, source_target_pairs={{0,2},{2,0},{1,3},{3,1},{4,6},{6,4},{5,7},{7,5},{8,10},{10,8},{9,1... | collective-permute-start | bytes 884744 | tf_op jit(solution)/shard_map/ppermute | solution.py:449
  28.8 6.0 %collective-permute-done.3.got_ref = f32[576,128]{1,0:T(8,128)S(1)} collective-permute-done((f32[576,128]{1,0:T(8,128)S(1)}, f32[576,128]{1,0:T(8,128)S(1)}, u32[]{:S(2)}, u32[]{:S(2)}) %collective-permute-start.3) | collective-permute-done | bytes 294944 | tf_op jit(solution)/shard_map/ppermute | solution.py:449
  34.8 0.5 units.1
  35.3 0.0 copy-start
  35.3 0.8 copy-done
  36.0 0.8 wgrads.1
  36.8 0.0 copy-start.1
  36.8 0.7 copy-done.1
  37.5 4.3 %collective-permute-start.4 = (bf16[5,64,1024]{2,1,0:T(8,128)(2,1)S(1)}, bf16[5,64,1024]{2,1,0:T(8,128)(2,1)S(1)}, u32[]{:S(2)}, u32[]{:S(2)}) collective-permute-start(bf16[5,64,1024]{2,1,0:T(8,128)(2,1)S(1)} %get-tuple-element.36.sent_ref), channel_id=1, source_target_pairs={{0,1},{1,0},{2,3},{3,2},{4,5},{5,4},{6,7},{7,6},{8,9},{9,8},{10,11... | collective-permute-start | bytes 1966088 | tf_op jit(solution)/shard_map/ppermute | solution.py:453
  41.8 0.0 copy-start.2
  41.8 7.5 %all-to-all-start.1 = ((bf16[32,56,128]{2,1,0:T(8,128)(2,1)}), bf16[32,56,128]{2,1,0:T(8,128)(2,1)S(1)}, u32[]{:S(2)}, u32[]{:S(2)}) async-start(bf16[32,56,128]{2,1,0:T(8,128)(2,1)} %bitcast.30), calls=%async_computation.1 | async-start | bytes 917504 | tf_op jit(solution)/shard_map/all_to_all | solution.py:475
  49.3 0.0 collective-permute-done.4.got_ref
  49.3 0.0 copy-done.2
  49.3 0.4 totals.1
  49.7 0.0 copy-start.8
  49.7 0.7 copy-done.8
  50.4 0.0 copy-start.6
  50.4 2.2 %collective-permute-start.5 = (f32[2,1024]{1,0:T(2,128)S(1)}, f32[2,1024]{1,0:T(2,128)S(1)}, u32[]{:S(2)}, u32[]{:S(2)}) collective-permute-start(f32[2,1024]{1,0:T(2,128)S(1)} %get-tuple-element.37.norms_ref), channel_id=1, source_target_pairs={{0,2},{2,0},{1,3},{3,1},{4,6},{6,4},{5,7},{7,5},{8,10},{10,8},{9,1... | collective-permute-start | bytes 24584 | tf_op jit(solution)/shard_map/ppermute | solution.py:449
  52.6 7.5 %all-to-all-done.1 = bf16[32,56,128]{2,1,0:T(8,128)(2,1)S(1)} async-done(((bf16[32,56,128]{2,1,0:T(8,128)(2,1)}), bf16[32,56,128]{2,1,0:T(8,128)(2,1)S(1)}, u32[]{:S(2)}, u32[]{:S(2)}) %all-to-all-start.1) | async-done | bytes 458784 | tf_op jit(solution)/shard_map/all_to_all | solution.py:475
  60.1 0.0 collective-permute-done.5.got_ref
  60.1 0.0 copy-done.6
  60.1 1.1 %combine.1 = bf16[8,104,128]{2,1,0:T(8,128)(2,1)} custom-call(s32[1]{0:T(128)} %bitcast.place_ref, s32[2,128]{1,0:T(2,128)S(1)} %bitcast.35, bf16[16,2,56,128]{3,2,1,0:T(8,128)(2,1)S(1)} %bitcast.29, f32[2,1024]{1,0:T(2,128)S(1)} %get-tuple-element.37.norms_ref, f32[2,1024]{1,0:T(2,128)S(1)} %collective-permute-done.5.got_ref), custom_call_target="tpu_custom_call" | custom-call | tf_op jit(solution)/shard_map/combine/pallas_call | solution.py:411
  61.2 14.7 %all-to-all-start.2 = ((bf16[8,104,128]{2,1,0:T(8,128)(2,1)}), bf16[8,104,128]{2,1,0:T(8,128)(2,1)S(1)}, u32[]{:S(2)}, u32[]{:S(2)}) async-start(bf16[8,104,128]{2,1,0:T(8,128)(2,1)} %combine.1), calls=%async_computation.2 | async-start | bytes 425984 | tf_op jit(solution)/shard_map/all_to_all | solution.py:483
  75.9 0.0 copy-done.9
  75.9 2.6 %collective-permute-start.6 = (bf16[3,32,1024]{2,1,0:T(8,128)(2,1)S(1)}, bf16[3,32,1024]{2,1,0:T(8,128)(2,1)S(1)}, u32[]{:S(2)}, u32[]{:S(2)}) collective-permute-start(bf16[3,32,1024]{2,1,0:T(8,128)(2,1)S(1)} %copy-done.9), channel_id=1, source_target_pairs={{0,2},{2,0},{1,3},{3,1},{4,6},{6,4},{5,7},{7,5},{8,10},{10,8},{9,1... | collective-permute-start | bytes 589832 | tf_op jit(solution)/shard_map/ppermute | solution.py:449
  78.6 12.3 %collective-permute-done.6.got_ref = bf16[3,32,1024]{2,1,0:T(8,128)(2,1)S(1)} collective-permute-done((bf16[3,32,1024]{2,1,0:T(8,128)(2,1)S(1)}, bf16[3,32,1024]{2,1,0:T(8,128)(2,1)S(1)}, u32[]{:S(2)}, u32[]{:S(2)}) %collective-permute-start.6) | collective-permute-done | bytes 196640 | tf_op jit(solution)/shard_map/ppermute | solution.py:449
  90.8 0.9 place_grads.1
  91.7 0.0 all-to-all-done.2.parts_ref
  91.8 0.0 copy-done.7
  91.8 0.6 finish.1
  (2 shorter events, 0.0 us)
Async XLA Ops:
  3.6 7.7 %copy-start.3 = (bf16[1,2048,32]{1,2,0:T(8,128)(2,1)S(1)}, bf16[1,2048,32]{1,2,0:T(8,128)(2,1)}, u32[]{:S(2)}) copy-start(bf16[1,2048,32]{1,2,0:T(8,128)(2,1)} %param.11) | copy-start | bytes 393220
  3.7 7.7 %copy-start.4 = (bf16[1,2048,32]{1,2,0:T(8,128)(2,1)S(1)}, bf16[1,2048,32]{1,2,0:T(8,128)(2,1)}, u32[]{:S(2)}) copy-start(bf16[1,2048,32]{1,2,0:T(8,128)(2,1)} %param.12) | copy-start | bytes 393220
  3.7 7.7 %copy-start.5 = (bf16[1,32,2048]{2,1,0:T(8,128)(2,1)S(1)}, bf16[1,32,2048]{2,1,0:T(8,128)(2,1)}, u32[]{:S(2)}) copy-start(bf16[1,32,2048]{2,1,0:T(8,128)(2,1)} %param.13) | copy-start | bytes 393220
  3.7 21.6 %all-to-all-start = ((bf16[16,24,1024]{2,1,0:T(8,128)(2,1)}), bf16[16,24,1024]{2,1,0:T(8,128)(2,1)S(1)}, u32[]{:S(2)}, u32[]{:S(2)}) async-start(bf16[16,24,1024]{2,1,0:T(8,128)(2,1)} %bitcast.38), calls=%async_computation | async-start | bytes 1572864 | tf_op jit(solution)/shard_map/all_to_all | solution.py:465
  11.5 6.8 %collective-permute-start = (bf16[96,1024]{1,0:T(8,128)(2,1)S(1)}, bf16[96,1024]{1,0:T(8,128)(2,1)S(1)}, u32[]{:S(2)}, u32[]{:S(2)}) collective-permute-start(bf16[96,1024]{1,0:T(8,128)(2,1)S(1)} %get-tuple-element.29), channel_id=1, source_target_pairs={{0,2},{2,0},{1,3},{3,1},{4,6},{6,4},{5,7},{7,5},{8,10},{10,8},{9,1... | collective-permute-start | bytes 589832 | tf_op jit(solution)/shard_map/ppermute | solution.py:449
  15.1 8.8 %collective-permute-start.1 = (bf16[96,1024]{1,0:T(8,128)(2,1)S(1)}, bf16[96,1024]{1,0:T(8,128)(2,1)S(1)}, u32[]{:S(2)}, u32[]{:S(2)}) collective-permute-start(bf16[96,1024]{1,0:T(8,128)(2,1)S(1)} %get-tuple-element.28.keep_ref), channel_id=1, source_target_pairs={{0,1},{1,0},{2,3},{3,2},{4,5},{5,4},{6,7},{7,6},{8,9},{9,8},{10,11... | collective-permute-start | bytes 589832 | tf_op jit(solution)/shard_map/ppermute | solution.py:453
  18.3 6.6 %collective-permute-start.2 = (bf16[96,1024]{1,0:T(8,128)(2,1)S(1)}, bf16[96,1024]{1,0:T(8,128)(2,1)S(1)}, u32[]{:S(2)}, u32[]{:S(2)}) collective-permute-start(bf16[96,1024]{1,0:T(8,128)(2,1)S(1)} %collective-permute-done.side_ref), channel_id=1, source_target_pairs={{0,1},{1,0},{2,3},{3,2},{4,5},{5,4},{6,7},{7,6},{8,9},{9,8},{10,11... | collective-permute-start | bytes 589832 | tf_op jit(solution)/shard_map/ppermute | solution.py:453
  25.8 8.9 %collective-permute-start.3 = (f32[576,128]{1,0:T(8,128)S(1)}, f32[576,128]{1,0:T(8,128)S(1)}, u32[]{:S(2)}, u32[]{:S(2)}) collective-permute-start(f32[576,128]{1,0:T(8,128)S(1)} %pre_parts.1.mine_ref), channel_id=1, source_target_pairs={{0,2},{2,0},{1,3},{3,1},{4,6},{6,4},{5,7},{7,5},{8,10},{10,8},{9,1... | collective-permute-start | bytes 884744 | tf_op jit(solution)/shard_map/ppermute | solution.py:449
  35.3 0.8 copy-start
  36.8 0.7 copy-start.1
  37.5 11.8 %collective-permute-start.4 = (bf16[5,64,1024]{2,1,0:T(8,128)(2,1)S(1)}, bf16[5,64,1024]{2,1,0:T(8,128)(2,1)S(1)}, u32[]{:S(2)}, u32[]{:S(2)}) collective-permute-start(bf16[5,64,1024]{2,1,0:T(8,128)(2,1)S(1)} %get-tuple-element.36.sent_ref), channel_id=1, source_target_pairs={{0,1},{1,0},{2,3},{3,2},{4,5},{5,4},{6,7},{7,6},{8,9},{9,8},{10,11... | collective-permute-start | bytes 1966088 | tf_op jit(solution)/shard_map/ppermute | solution.py:453
  41.8 7.5 %copy-start.2 = (f32[64,1024]{1,0:T(8,128)S(1)}, f32[64,1024]{1,0:T(8,128)}, u32[]{:S(2)}) copy-start(f32[64,1024]{1,0:T(8,128)} %copy-done.1) | copy-start | bytes 786436
  41.8 18.2 %all-to-all-start.1 = ((bf16[32,56,128]{2,1,0:T(8,128)(2,1)}), bf16[32,56,128]{2,1,0:T(8,128)(2,1)S(1)}, u32[]{:S(2)}, u32[]{:S(2)}) async-start(bf16[32,56,128]{2,1,0:T(8,128)(2,1)} %bitcast.30), calls=%async_computation.1 | async-start | bytes 917504 | tf_op jit(solution)/shard_map/all_to_all | solution.py:475
  49.7 0.7 copy-start.8
  50.4 9.7 %copy-start.6 = (s32[128,2]{0,1:T(2,128)S(1)}, s32[128,2]{0,1:T(2,128)}, u32[]{:S(2)}) copy-start(s32[128,2]{0,1:T(2,128)} %param.8) | copy-start | bytes 3076
  50.4 9.7 %collective-permute-start.5 = (f32[2,1024]{1,0:T(2,128)S(1)}, f32[2,1024]{1,0:T(2,128)S(1)}, u32[]{:S(2)}, u32[]{:S(2)}) collective-permute-start(f32[2,1024]{1,0:T(2,128)S(1)} %get-tuple-element.37.norms_ref), channel_id=1, source_target_pairs={{0,2},{2,0},{1,3},{3,1},{4,6},{6,4},{5,7},{7,5},{8,10},{10,8},{9,1... | collective-permute-start | bytes 24584 | tf_op jit(solution)/shard_map/ppermute | solution.py:449
  61.2 14.7 %copy-start.9 = (bf16[3,32,1024]{2,1,0:T(8,128)(2,1)S(1)}, bf16[3,32,1024]{2,1,0:T(8,128)(2,1)}, u32[]{:S(2)}) copy-start(bf16[3,32,1024]{2,1,0:T(8,128)(2,1)} %copy-done.8) | copy-start | bytes 589828
  61.2 30.5 %all-to-all-start.2 = ((bf16[8,104,128]{2,1,0:T(8,128)(2,1)}), bf16[8,104,128]{2,1,0:T(8,128)(2,1)S(1)}, u32[]{:S(2)}, u32[]{:S(2)}) async-start(bf16[8,104,128]{2,1,0:T(8,128)(2,1)} %combine.1), calls=%async_computation.2 | async-start | bytes 425984 | tf_op jit(solution)/shard_map/all_to_all | solution.py:483
  75.9 14.9 %collective-permute-start.6 = (bf16[3,32,1024]{2,1,0:T(8,128)(2,1)S(1)}, bf16[3,32,1024]{2,1,0:T(8,128)(2,1)S(1)}, u32[]{:S(2)}, u32[]{:S(2)}) collective-permute-start(bf16[3,32,1024]{2,1,0:T(8,128)(2,1)S(1)} %copy-done.9), channel_id=1, source_target_pairs={{0,2},{2,0},{1,3},{3,1},{4,6},{6,4},{5,7},{7,5},{8,10},{10,8},{9,1... | collective-permute-start | bytes 589832 | tf_op jit(solution)/shard_map/ppermute | solution.py:449
  90.8 0.9 %copy-start.7 = (f32[128,2]{0,1:T(2,128)S(1)}, f32[128,2]{0,1:T(2,128)}, u32[]{:S(2)}) copy-start(f32[128,2]{0,1:T(2,128)} %param.9) | copy-start | bytes 3076

commit v6 on v5

--- a/solution.py
+++ b/solution.py
@@ -177,41 +177,52 @@
     )(place, keep, side, core, cross)
 
 
-def pre_kernel(rows_ref, wall_ref, out_ref):
-    count = rows_ref.shape[0]
+def paired(values):
+    groups = values.shape[0] // (2 * ROWS)
+    still = values.reshape(groups, 2, ROWS, 128)
+    moved = jnp.roll(values, HALF, axis=0).reshape(groups, 2, ROWS, 128)
+    top = iota((groups, ROWS, 128), 1) < HALF
+    return jnp.where(top, still[:, 0], moved[:, 1]).reshape(groups * ROWS, 128)
+
+
+def unpaired(values):
+    groups = values.shape[0] // ROWS
+    moved = jnp.roll(values, -HALF, axis=0).reshape(groups, 1, ROWS, 128)
+    both = jnp.concatenate([values.reshape(groups, 1, ROWS, 128), moved], axis=1)
+    return both.reshape(2 * values.shape[0], 128)
+
+
+def pre_kernel(rows_ref, wall_ref, up_ref, down_ref):
+    half = rows_ref.shape[0] // 2
     pre = nt(rows_ref[...], wall_ref[...])
-    upper = lax.rem(iota((count, 128), 0), ROWS) < HALF
-    out_ref[0:count, :] = jnp.where(upper, pre[:, :128], pre[:, 256:])
-    lin = pre[:, 128:256].reshape(count // (2 * ROWS), 2, ROWS, 128)
-    moved = jnp.roll(pre[:, 128:256], HALF, axis=0).reshape(lin.shape)
-    top = iota((count // (2 * ROWS), ROWS, 128), 1) < HALF
-    out_ref[count:, :] = jnp.where(top, lin[:, 0], moved[:, 1]).reshape(count // 2, 128)
+    up_ref[0:half, :] = paired(pre[:, :128])
+    up_ref[half:, :] = paired(pre[:, 128:256])
+    down_ref[...] = paired(jnp.roll(pre[:, 256:], -HALF, axis=0)).astype(bf16)
 
 
 def pre_parts(rows, wall):
     count = rows.shape[0]
     return pl.pallas_call(
         pre_kernel,
-        out_shape=jax.ShapeDtypeStruct((count + count // 2, 128), f32),
+        out_shape=(
+            jax.ShapeDtypeStruct((count, 128), f32),
+            jax.ShapeDtypeStruct((count // 2, 128), bf16),
+        ),
         in_specs=[VMEM, VMEM],
-        out_specs=VMEM,
+        out_specs=(VMEM,) * 2,
         compiler_params=pltpu.CompilerParams(vmem_limit_bytes=LIMIT),
         name="pre_parts",
     )(rows, wall)
 
 
-def unit_kernel(mine_ref, got_ref, wret_ref, grads_ref, msg_ref):
+def unit_kernel(up_ref, up_got_ref, down_ref, down_got_ref, wret_ref, grads_ref, msg_ref):
     count = grads_ref.shape[0]
     sources = count // ROWS
     units = 128
-    glu_pre = mine_ref[0:count, :] + got_ref[0:count, :]
-    hid_grad = jnp.roll(glu_pre, -HALF, axis=0)
-    lin = mine_ref[count:, :] + got_ref[count:, :]
-    moved = jnp.roll(lin, -HALF, axis=0)
-    lin_pre = jnp.concatenate(
-        [lin.reshape(sources // 2, 1, ROWS, units), moved.reshape(sources // 2, 1, ROWS, units)],
-        axis=1,
-    ).reshape(count, units)
+    half = count // 2
+    glu_pre = unpaired(up_ref[0:half, :] + up_got_ref[0:half, :])
+    lin_pre = unpaired(up_ref[half:, :] + up_got_ref[half:, :])
+    hid_grad = unpaired(down_ref[...].astype(f32) + down_got_ref[...].astype(f32))
     keep = lax.rem(iota((count, units), 0), ROWS) < HALF
     glu_clip = jnp.minimum(glu_pre, clamp_limit)
     lin_clip = jnp.clip(lin_pre, -clamp_limit, clamp_limit)
@@ -246,8 +257,8 @@
         msg_ref[:, core, blocks * ROWS :, :] = tail
 
 
-def units(mine, got, wret):
-    count = mine.shape[0] // 3 * 2
+def units(up, up_got, down, down_got, wret):
+    count = up.shape[0]
     height = wret.shape[2] // 128 * ROWS + 8
     return pl.pallas_call(
         unit_kernel,
@@ -255,11 +266,11 @@
             jax.ShapeDtypeStruct((count, 384), bf16),
             jax.ShapeDtypeStruct((count // ROWS, 2, height, 128), bf16),
         ),
-        in_specs=[VMEM, VMEM, VMEM],
+        in_specs=[VMEM] * 5,
         out_specs=(VMEM, VMEM),
         compiler_params=pltpu.CompilerParams(vmem_limit_bytes=LIMIT),
         name="units",
-    )(mine, got, wret)
+    )(up, up_got, down, down_got, wret)
 
 
 def wgrad_kernel(grads_ref, rows_ref, own_ref, down_ref, send_ref):
@@ -469,8 +480,10 @@
     got = over_side(send)
     wall, wret = gather_weights(place, keep, got, over_core(keep), over_core(got))
 
-    mine = pre_parts(rows, wall)
-    grads, msg = units(mine, over_side(mine), wret)
+    up, down = pre_parts(rows, wall)
+    up_got = over_side(up)
+    down_got = over_side(down)
+    grads, msg = units(up, up_got, down, down_got, wret)
     msg = msg.reshape(experts * 2, *msg.shape[2:])
     back = lax.all_to_all(msg, ("ep", "core"), 0, 0, tiled=True)
     back = back.reshape(experts, 2, *msg.shape[1:])

time: 93 us -> 92 us (0.989)
  waiting for transfers between devices: 26.9 us -> 24.2 us
  starting transfers between devices: 54.1 us -> 55.8 us
    ppermute x4 -> x5, waiting for transfers between devices: 18.3 us -> 15.6 us  [over_side(): return lax.ppermute(x, 'side', [(0, 1), (1, 0)])]
    ppermute x4 -> x5, starting transfers between devices: 11.3 us -> 13.6 us  [over_side(): return lax.ppermute(x, 'side', [(0, 1), (1, 0)])]
    all_to_all x1, starting transfers between devices: 7.46 us -> 6.3 us  [layer(): back = lax.all_to_all(msg, ('ep', 'core'), 0, 0, tiled=True)]
  transfers between devices with their start and end apart: 10 -> 11, of which waited for: 5 -> 5; matrix products, arithmetic and copies ran while one was open for 0% -> 0% of each run, Pallas kernels for 2% -> 2%
where the time goes in v6:
time: 92 us; the launch traced here: 91.4 us
  starting transfers between devices  55.8 us (61%)
  waiting for transfers between devices  24.2 us (26%)
  Pallas kernels  8.38 us (9%)
  local copies, waits for them, and re-layouts  2.16 us (2%)
    ppermute x5, waiting for transfers between devices, over_side(): return lax.ppermute(x, 'side', [(0, 1), (1, 0)])  15.6 us
    all_to_all x1, starting transfers between devices, layer(): lax.all_to_all(msg, 'team', 0, 0, axis_index_groups=[turned], tiled=True)  14.7 us
    ppermute x5, starting transfers between devices, over_side(): return lax.ppermute(x, 'side', [(0, 1), (1, 0)])  13.6 us
    ppermute x3, starting transfers between devices, over_core(): return lax.ppermute(x, 'core', [(0, 1), (1, 0)])  13.5 us
    all_to_all x1, starting transfers between devices, layer(): lax.all_to_all(packed.reshape(experts, ROWS, width // 2), 'ep', 0, 0, til...  7.71 us
    all_to_all x1, waiting for transfers between devices, layer(): back = lax.all_to_all(msg, ('ep', 'core'), 0, 0, tiled=True)  7.51 us
    all_to_all x1, starting transfers between devices, layer(): back = lax.all_to_all(msg, ('ep', 'core'), 0, 0, tiled=True)  6.3 us
    pallas_call x1, Pallas kernels, pack_rows(): pl.pallas_call(pack_kernel, out_shape=jax.ShapeDtypeStruct((experts * ROW...  3.02 us
  transfers between devices with their start and end apart: 11, of which 5 were waited for; matrix products, arithmetic and copies ran while one was open for 0% of the time, Pallas kernels for 2%

profile of v6, /device:TPU:1, one launch (start us, length us, event | category | flops | bytes accessed | tf_op | source)
XLA Modules:
  0.0 91.4 jit_solution(7466909964928887972)
XLA Ops:
  0.6 3.0 %pack_rows.1 = bf16[384,1024]{1,0:T(8,128)(2,1)} custom-call(s32[1]{0:T(128)} %bitcast.place_ref, s32[1]{0:T(128)} %bitcast.2.core_ref, s32[2,128]{1,0:T(2,128)} %bitcast.34, f32[2,128]{1,0:T(2,128)} %bitcast.36, bf16[128,2048]{1,0:T(8,128)(2,1)} %tok_ref.1, bf16[128,2048]{1,0:T(8,128)(2,1)} %cot_ref.1), custom_call_target="tpu_custom_call" | custom-call | tf_op jit(solution)/shard_map/pack_rows/pallas_call | solution.py:102
  3.7 0.0 copy-start.3
  3.7 0.0 copy-start.4
  3.7 7.7 %all-to-all-start = ((bf16[16,24,1024]{2,1,0:T(8,128)(2,1)}), bf16[16,24,1024]{2,1,0:T(8,128)(2,1)S(1)}, u32[]{:S(2)}, u32[]{:S(2)}) async-start(bf16[16,24,1024]{2,1,0:T(8,128)(2,1)} %bitcast.38), calls=%async_computation | async-start | bytes 1572864 | tf_op jit(solution)/shard_map/all_to_all | solution.py:476
  11.4 0.0 copy-done.3
  11.4 0.0 copy-done.4
  11.4 0.0 copy-done.5
  11.4 0.1 part_weights.1
  11.5 3.5 %collective-permute-start = (bf16[96,1024]{1,0:T(8,128)(2,1)S(1)}, bf16[96,1024]{1,0:T(8,128)(2,1)S(1)}, u32[]{:S(2)}, u32[]{:S(2)}) collective-permute-start(bf16[96,1024]{1,0:T(8,128)(2,1)S(1)} %get-tuple-element.31), channel_id=1, source_target_pairs={{0,2},{2,0},{1,3},{3,1},{4,6},{6,4},{5,7},{7,5},{8,10},{10,8},{9,1... | collective-permute-start | bytes 589832 | tf_op jit(solution)/shard_map/ppermute | solution.py:460
  15.1 3.2 %collective-permute-start.1 = (bf16[96,1024]{1,0:T(8,128)(2,1)S(1)}, bf16[96,1024]{1,0:T(8,128)(2,1)S(1)}, u32[]{:S(2)}, u32[]{:S(2)}) collective-permute-start(bf16[96,1024]{1,0:T(8,128)(2,1)S(1)} %get-tuple-element.30.keep_ref), channel_id=1, source_target_pairs={{0,1},{1,0},{2,3},{3,2},{4,5},{5,4},{6,7},{7,6},{8,9},{9,8},{10,11... | collective-permute-start | bytes 589832 | tf_op jit(solution)/shard_map/ppermute | solution.py:464
  18.3 0.1 collective-permute-done.side_ref
  18.3 5.5 %collective-permute-start.2 = (bf16[96,1024]{1,0:T(8,128)(2,1)S(1)}, bf16[96,1024]{1,0:T(8,128)(2,1)S(1)}, u32[]{:S(2)}, u32[]{:S(2)}) collective-permute-start(bf16[96,1024]{1,0:T(8,128)(2,1)S(1)} %collective-permute-done.side_ref), channel_id=1, source_target_pairs={{0,1},{1,0},{2,3},{3,2},{4,5},{5,4},{6,7},{7,6},{8,9},{9,8},{10,11... | collective-permute-start | bytes 589832 | tf_op jit(solution)/shard_map/ppermute | solution.py:464
  23.9 0.0 collective-permute-done.1.core_ref
  23.9 1.0 %collective-permute-done.2.cross_ref = bf16[96,1024]{1,0:T(8,128)(2,1)S(1)} collective-permute-done((bf16[96,1024]{1,0:T(8,128)(2,1)S(1)}, bf16[96,1024]{1,0:T(8,128)(2,1)S(1)}, u32[]{:S(2)}, u32[]{:S(2)}) %collective-permute-start.2) | collective-permute-done | bytes 196640 | tf_op jit(solution)/shard_map/ppermute | solution.py:464
  24.9 0.3 gather_weights.1
  25.2 0.0 all-to-all-done
  25.2 0.6 pre_parts.1
  25.8 2.9 %collective-permute-start.3 = (f32[384,128]{1,0:T(8,128)S(1)}, f32[384,128]{1,0:T(8,128)S(1)}, u32[]{:S(2)}, u32[]{:S(2)}) collective-permute-start(f32[384,128]{1,0:T(8,128)S(1)} %get-tuple-element.33.up_ref), channel_id=1, source_target_pairs={{0,2},{2,0},{1,3},{3,1},{4,6},{6,4},{5,7},{7,5},{8,10},{10,8},{9,1... | collective-permute-start | bytes 589832 | tf_op jit(solution)/shard_map/ppermute | solution.py:460
  28.8 2.4 %collective-permute-start.4 = (bf16[192,128]{1,0:T(8,128)(2,1)S(1)}, bf16[192,128]{1,0:T(8,128)(2,1)S(1)}, u32[]{:S(2)}, u32[]{:S(2)}) collective-permute-start(bf16[192,128]{1,0:T(8,128)(2,1)S(1)} %get-tuple-element.34.down_ref), channel_id=1, source_target_pairs={{0,2},{2,0},{1,3},{3,1},{4,6},{6,4},{5,7},{7,5},{8,10},{10,8},{9,1... | collective-permute-start | bytes 147464 | tf_op jit(solution)/shard_map/ppermute | solution.py:460
  31.1 3.3 %collective-permute-done.4.down_got_ref = bf16[192,128]{1,0:T(8,128)(2,1)S(1)} collective-permute-done((bf16[192,128]{1,0:T(8,128)(2,1)S(1)}, bf16[192,128]{1,0:T(8,128)(2,1)S(1)}, u32[]{:S(2)}, u32[]{:S(2)}) %collective-permute-start.4) | collective-permute-done | bytes 49184 | tf_op jit(solution)/shard_map/ppermute | solution.py:460
  34.4 0.0 collective-permute-done.3.up_got_ref
  34.4 0.5 units.1
  34.9 0.0 copy-start
  35.0 0.8 copy-done
  35.7 0.8 wgrads.1
  36.5 0.0 copy-start.1
  36.5 0.7 copy-done.1
  37.2 4.7 %collective-permute-start.5 = (bf16[5,64,1024]{2,1,0:T(8,128)(2,1)S(1)}, bf16[5,64,1024]{2,1,0:T(8,128)(2,1)S(1)}, u32[]{:S(2)}, u32[]{:S(2)}) collective-permute-start(bf16[5,64,1024]{2,1,0:T(8,128)(2,1)S(1)} %get-tuple-element.40.sent_ref), channel_id=1, source_target_pairs={{0,1},{1,0},{2,3},{3,2},{4,5},{5,4},{6,7},{7,6},{8,9},{9,8},{10,11... | collective-permute-start | bytes 1966088 | tf_op jit(solution)/shard_map/ppermute | solution.py:464
  42.0 0.0 copy-start.2
  42.0 6.3 %all-to-all-start.1 = ((bf16[32,56,128]{2,1,0:T(8,128)(2,1)}), bf16[32,56,128]{2,1,0:T(8,128)(2,1)S(1)}, u32[]{:S(2)}, u32[]{:S(2)}) async-start(bf16[32,56,128]{2,1,0:T(8,128)(2,1)} %bitcast.30), calls=%async_computation.1 | async-start | bytes 917504 | tf_op jit(solution)/shard_map/all_to_all | solution.py:488
  48.3 0.0 collective-permute-done.5.got_ref
  48.3 0.0 copy-done.2
  48.3 0.4 totals.1
  48.7 0.0 copy-start.8
  48.7 0.7 copy-done.8
  49.3 2.2 %collective-permute-start.6 = (f32[2,1024]{1,0:T(2,128)S(1)}, f32[2,1024]{1,0:T(2,128)S(1)}, u32[]{:S(2)}, u32[]{:S(2)}) collective-permute-start(f32[2,1024]{1,0:T(2,128)S(1)} %get-tuple-element.41.norms_ref), channel_id=1, source_target_pairs={{0,2},{2,0},{1,3},{3,1},{4,6},{6,4},{5,7},{7,5},{8,10},{10,8},{9,1... | collective-permute-start | bytes 24584 | tf_op jit(solution)/shard_map/ppermute | solution.py:460
  51.5 7.5 %all-to-all-done.1 = bf16[32,56,128]{2,1,0:T(8,128)(2,1)S(1)} async-done(((bf16[32,56,128]{2,1,0:T(8,128)(2,1)}), bf16[32,56,128]{2,1,0:T(8,128)(2,1)S(1)}, u32[]{:S(2)}, u32[]{:S(2)}) %all-to-all-start.1) | async-done | bytes 458784 | tf_op jit(solution)/shard_map/all_to_all | solution.py:488
  59.1 0.0 collective-permute-done.6.got_ref
  59.1 0.0 copy-done.6
  59.1 1.1 %combine.1 = bf16[8,104,128]{2,1,0:T(8,128)(2,1)} custom-call(s32[1]{0:T(128)} %bitcast.place_ref, s32[2,128]{1,0:T(2,128)S(1)} %bitcast.35, bf16[16,2,56,128]{3,2,1,0:T(8,128)(2,1)S(1)} %bitcast.29, f32[2,1024]{1,0:T(2,128)S(1)} %get-tuple-element.41.norms_ref, f32[2,1024]{1,0:T(2,128)S(1)} %collective-permute-done.6.got_ref), custom_call_target="tpu_custom_call" | custom-call | tf_op jit(solution)/shard_map/combine/pallas_call | solution.py:422
  60.2 14.7 %all-to-all-start.2 = ((bf16[8,104,128]{2,1,0:T(8,128)(2,1)}), bf16[8,104,128]{2,1,0:T(8,128)(2,1)S(1)}, u32[]{:S(2)}, u32[]{:S(2)}) async-start(bf16[8,104,128]{2,1,0:T(8,128)(2,1)} %combine.1), calls=%async_computation.2 | async-start | bytes 425984 | tf_op jit(solution)/shard_map/all_to_all | solution.py:496
  74.9 0.0 copy-done.9
  74.9 2.6 %collective-permute-start.7 = (bf16[3,32,1024]{2,1,0:T(8,128)(2,1)S(1)}, bf16[3,32,1024]{2,1,0:T(8,128)(2,1)S(1)}, u32[]{:S(2)}, u32[]{:S(2)}) collective-permute-start(bf16[3,32,1024]{2,1,0:T(8,128)(2,1)S(1)} %copy-done.9), channel_id=1, source_target_pairs={{0,2},{2,0},{1,3},{3,1},{4,6},{6,4},{5,7},{7,5},{8,10},{10,8},{9,1... | collective-permute-start | bytes 589832 | tf_op jit(solution)/shard_map/ppermute | solution.py:460
  77.5 12.3 %collective-permute-done.7.got_ref = bf16[3,32,1024]{2,1,0:T(8,128)(2,1)S(1)} collective-permute-done((bf16[3,32,1024]{2,1,0:T(8,128)(2,1)S(1)}, bf16[3,32,1024]{2,1,0:T(8,128)(2,1)S(1)}, u32[]{:S(2)}, u32[]{:S(2)}) %collective-permute-start.7) | collective-permute-done | bytes 196640 | tf_op jit(solution)/shard_map/ppermute | solution.py:460
  89.8 0.9 %place_grads.1 = (f32[32,2048]{1,0:T(8,128)}, f32[32,2048]{1,0:T(8,128)}, f32[32,2048]{1,0:T(8,128)}, f32[1,128]{1,0:T(1,128)}) custom-call(s32[1]{0:T(128)} %bitcast.place_ref, f32[3,32,1024]{2,1,0:T(8,128)S(1)} %get-tuple-element.44.own_ref, bf16[3,32,1024]{2,1,0:T(8,128)(2,1)S(1)} %collective-permute-done.7.got_ref), custom_call_target="tpu_custom_call" | custom-call | tf_op jit(solution)/shard_map/place_grads/pallas_call | solution.py:353
  90.7 0.0 all-to-all-done.2.parts_ref
  90.7 0.0 copy-done.7
  90.7 0.6 finish.1
  (4 shorter events, 0.0 us)
Async XLA Ops:
  3.7 7.7 %copy-start.3 = (bf16[1,2048,32]{1,2,0:T(8,128)(2,1)S(1)}, bf16[1,2048,32]{1,2,0:T(8,128)(2,1)}, u32[]{:S(2)}) copy-start(bf16[1,2048,32]{1,2,0:T(8,128)(2,1)} %param.11) | copy-start | bytes 393220
  3.7 7.7 %copy-start.4 = (bf16[1,2048,32]{1,2,0:T(8,128)(2,1)S(1)}, bf16[1,2048,32]{1,2,0:T(8,128)(2,1)}, u32[]{:S(2)}) copy-start(bf16[1,2048,32]{1,2,0:T(8,128)(2,1)} %param.12) | copy-start | bytes 393220
  3.7 7.7 %copy-start.5 = (bf16[1,32,2048]{2,1,0:T(8,128)(2,1)S(1)}, bf16[1,32,2048]{2,1,0:T(8,128)(2,1)}, u32[]{:S(2)}) copy-start(bf16[1,32,2048]{2,1,0:T(8,128)(2,1)} %param.13) | copy-start | bytes 393220
  3.7 21.6 %all-to-all-start = ((bf16[16,24,1024]{2,1,0:T(8,128)(2,1)}), bf16[16,24,1024]{2,1,0:T(8,128)(2,1)S(1)}, u32[]{:S(2)}, u32[]{:S(2)}) async-start(bf16[16,24,1024]{2,1,0:T(8,128)(2,1)} %bitcast.38), calls=%async_computation | async-start | bytes 1572864 | tf_op jit(solution)/shard_map/all_to_all | solution.py:476
  11.5 6.8 %collective-permute-start = (bf16[96,1024]{1,0:T(8,128)(2,1)S(1)}, bf16[96,1024]{1,0:T(8,128)(2,1)S(1)}, u32[]{:S(2)}, u32[]{:S(2)}) collective-permute-start(bf16[96,1024]{1,0:T(8,128)(2,1)S(1)} %get-tuple-element.31), channel_id=1, source_target_pairs={{0,2},{2,0},{1,3},{3,1},{4,6},{6,4},{5,7},{7,5},{8,10},{10,8},{9,1... | collective-permute-start | bytes 589832 | tf_op jit(solution)/shard_map/ppermute | solution.py:460
  15.1 8.8 %collective-permute-start.1 = (bf16[96,1024]{1,0:T(8,128)(2,1)S(1)}, bf16[96,1024]{1,0:T(8,128)(2,1)S(1)}, u32[]{:S(2)}, u32[]{:S(2)}) collective-permute-start(bf16[96,1024]{1,0:T(8,128)(2,1)S(1)} %get-tuple-element.30.keep_ref), channel_id=1, source_target_pairs={{0,1},{1,0},{2,3},{3,2},{4,5},{5,4},{6,7},{7,6},{8,9},{9,8},{10,11... | collective-permute-start | bytes 589832 | tf_op jit(solution)/shard_map/ppermute | solution.py:464
  18.3 6.6 %collective-permute-start.2 = (bf16[96,1024]{1,0:T(8,128)(2,1)S(1)}, bf16[96,1024]{1,0:T(8,128)(2,1)S(1)}, u32[]{:S(2)}, u32[]{:S(2)}) collective-permute-start(bf16[96,1024]{1,0:T(8,128)(2,1)S(1)} %collective-permute-done.side_ref), channel_id=1, source_target_pairs={{0,1},{1,0},{2,3},{3,2},{4,5},{5,4},{6,7},{7,6},{8,9},{9,8},{10,11... | collective-permute-start | bytes 589832 | tf_op jit(solution)/shard_map/ppermute | solution.py:464
  25.8 8.6 %collective-permute-start.3 = (f32[384,128]{1,0:T(8,128)S(1)}, f32[384,128]{1,0:T(8,128)S(1)}, u32[]{:S(2)}, u32[]{:S(2)}) collective-permute-start(f32[384,128]{1,0:T(8,128)S(1)} %get-tuple-element.33.up_ref), channel_id=1, source_target_pairs={{0,2},{2,0},{1,3},{3,1},{4,6},{6,4},{5,7},{7,5},{8,10},{10,8},{9,1... | collective-permute-start | bytes 589832 | tf_op jit(solution)/shard_map/ppermute | solution.py:460
  28.8 5.7 %collective-permute-start.4 = (bf16[192,128]{1,0:T(8,128)(2,1)S(1)}, bf16[192,128]{1,0:T(8,128)(2,1)S(1)}, u32[]{:S(2)}, u32[]{:S(2)}) collective-permute-start(bf16[192,128]{1,0:T(8,128)(2,1)S(1)} %get-tuple-element.34.down_ref), channel_id=1, source_target_pairs={{0,2},{2,0},{1,3},{3,1},{4,6},{6,4},{5,7},{7,5},{8,10},{10,8},{9,1... | collective-permute-start | bytes 147464 | tf_op jit(solution)/shard_map/ppermute | solution.py:460
  34.9 0.8 copy-start
  36.5 0.7 copy-start.1
  37.2 11.1 %collective-permute-start.5 = (bf16[5,64,1024]{2,1,0:T(8,128)(2,1)S(1)}, bf16[5,64,1024]{2,1,0:T(8,128)(2,1)S(1)}, u32[]{:S(2)}, u32[]{:S(2)}) collective-permute-start(bf16[5,64,1024]{2,1,0:T(8,128)(2,1)S(1)} %get-tuple-element.40.sent_ref), channel_id=1, source_target_pairs={{0,1},{1,0},{2,3},{3,2},{4,5},{5,4},{6,7},{7,6},{8,9},{9,8},{10,11... | collective-permute-start | bytes 1966088 | tf_op jit(solution)/shard_map/ppermute | solution.py:464
  42.0 6.3 %copy-start.2 = (f32[64,1024]{1,0:T(8,128)S(1)}, f32[64,1024]{1,0:T(8,128)}, u32[]{:S(2)}) copy-start(f32[64,1024]{1,0:T(8,128)} %copy-done.1) | copy-start | bytes 786436
  42.0 17.1 %all-to-all-start.1 = ((bf16[32,56,128]{2,1,0:T(8,128)(2,1)}), bf16[32,56,128]{2,1,0:T(8,128)(2,1)S(1)}, u32[]{:S(2)}, u32[]{:S(2)}) async-start(bf16[32,56,128]{2,1,0:T(8,128)(2,1)} %bitcast.30), calls=%async_computation.1 | async-start | bytes 917504 | tf_op jit(solution)/shard_map/all_to_all | solution.py:488
  48.7 0.7 copy-start.8
  49.3 9.7 %copy-start.6 = (s32[128,2]{0,1:T(2,128)S(1)}, s32[128,2]{0,1:T(2,128)}, u32[]{:S(2)}) copy-start(s32[128,2]{0,1:T(2,128)} %param.8) | copy-start | bytes 3076
  49.3 9.7 %collective-permute-start.6 = (f32[2,1024]{1,0:T(2,128)S(1)}, f32[2,1024]{1,0:T(2,128)S(1)}, u32[]{:S(2)}, u32[]{:S(2)}) collective-permute-start(f32[2,1024]{1,0:T(2,128)S(1)} %get-tuple-element.41.norms_ref), channel_id=1, source_target_pairs={{0,2},{2,0},{1,3},{3,1},{4,6},{6,4},{5,7},{7,5},{8,10},{10,8},{9,1... | collective-permute-start | bytes 24584 | tf_op jit(solution)/shard_map/ppermute | solution.py:460
  60.2 14.7 %copy-start.9 = (bf16[3,32,1024]{2,1,0:T(8,128)(2,1)S(1)}, bf16[3,32,1024]{2,1,0:T(8,128)(2,1)}, u32[]{:S(2)}) copy-start(bf16[3,32,1024]{2,1,0:T(8,128)(2,1)} %copy-done.8) | copy-start | bytes 589828
  60.2 30.5 %all-to-all-start.2 = ((bf16[8,104,128]{2,1,0:T(8,128)(2,1)}), bf16[8,104,128]{2,1,0:T(8,128)(2,1)S(1)}, u32[]{:S(2)}, u32[]{:S(2)}) async-start(bf16[8,104,128]{2,1,0:T(8,128)(2,1)} %combine.1), calls=%async_computation.2 | async-start | bytes 425984 | tf_op jit(solution)/shard_map/all_to_all | solution.py:496
  74.9 14.9 %collective-permute-start.7 = (bf16[3,32,1024]{2,1,0:T(8,128)(2,1)S(1)}, bf16[3,32,1024]{2,1,0:T(8,128)(2,1)S(1)}, u32[]{:S(2)}, u32[]{:S(2)}) collective-permute-start(bf16[3,32,1024]{2,1,0:T(8,128)(2,1)S(1)} %copy-done.9), channel_id=1, source_target_pairs={{0,2},{2,0},{1,3},{3,1},{4,6},{6,4},{5,7},{7,5},{8,10},{10,8},{9,1... | collective-permute-start | bytes 589832 | tf_op jit(solution)/shard_map/ppermute | solution.py:460
  89.8 0.9 %copy-start.7 = (f32[128,2]{0,1:T(2,128)S(1)}, f32[128,2]{0,1:T(2,128)}, u32[]{:S(2)}) copy-start(f32[128,2]{0,1:T(2,128)} %param.9) | copy-start | bytes 3076
